TPU v7x, 128 devices: a whole 4x4x4 slice. The times are simulated.
128 devices in a mesh: ep: 32 (over z, y, core), tp: 4 (over x).
Axes of the slice: x: 4, y: 4, z: 4, core: 2. Of those that a mesh axis runs over, the one named last changes fastest.
Arguments:
- tokens: bfloat16 [512, 2048], P('ep'), may hold values from -60 to 60
- mixer_gain: float32 [2048], replicated, may hold values from 0.1 to 1.9
- query_weight: bfloat16 [2048, 2048], P('ep', 'tp'), may hold values from -0.125 to 0.125
- key_weight: bfloat16 [2048, 2048], P('ep', 'tp'), may hold values from -0.125 to 0.125
- value_weight: bfloat16 [2048, 2048], P('ep', 'tp'), may hold values from -0.125 to 0.125
- outgate_weight: bfloat16 [2048, 2048], P('ep', 'tp'), may hold values from -0.125 to 0.125
- igate_weight: bfloat16 [4, 2048], P('tp'), may hold values from -0.125 to 0.125
- fgate_weight: bfloat16 [4, 2048], P('tp'), may hold values from -0.125 to 0.125
- memory: float32 [512, 4, 512, 512], P('ep', 'tp'), may hold values from -6 to 6
- stabilizer: float32 [512, 4], P('ep', 'tp'), may hold values from -6 to 6
- head_gain: float32 [2048], P('tp'), may hold values from 0.1 to 1.9
- down_weight: bfloat16 [2048, 2048], P(None, 'ep'), may hold values from -1 to 1
- mixed_gain: float32 [2048], P('ep'), may hold values from 0.1 to 1.9
- expert_gain: float32 [2048], P('ep'), may hold values from 0.1 to 1.9
- routes: int32 [512, 4], replicated, may hold values from 0 to 31, all different within a row; in each aligned block of 16 rows (0 to 15, 16 to 31, ...) at most 4 rows name the same one
- route_weights: float32 [512, 4], replicated, may hold values from 0.1 to 1
- gate_proj: bfloat16 [32, 2048, 2048], P('ep', None, 'tp'), may hold values from -0.5 to 0.5
- up_proj: bfloat16 [32, 2048, 2048], P('ep', None, 'tp'), may hold values from -0.5 to 0.5
- expert_down: bfloat16 [32, 2048, 2048], P('ep', 'tp'), may hold values from -1 to 1
- output_gain: float32 [2048], P('tp'), may hold values from 0.1 to 1.9
Outputs:
- layer_out: bfloat16 [512, 2048], P('ep', 'tp')
Inputs may be any that keep to these rules, and one draw needn't show every extreme that they name: `routes`: each row names 4 different experts; within the rows of one device (16 rows) no expert is named more than 4 times, a bound that some block reaches.
All inputs are finite; a program needn't handle non-finite values.
Results may differ from a plain program's by a relative error of at most 0.0095.
Values may be sent and summed in bfloat16 or wider, within the bound.
No kernel may reach another device: no remote copies, remote signals or barrier semaphores. Data moves between devices by JAX's collectives and lax.ppermute only.
A program may use at most 128 MiB of HBM per device.

v0:
```python
import jax
import jax.numpy as jnp
from jax import lax
from jax.experimental import pallas as pl
from jax.experimental.pallas import tpu as pltpu
from jax.sharding import PartitionSpec as P


NORM_EPS = 1e-06
CLAMP_LIMIT = 7.0
SIGMOID_SCALE = 1.702
BF = jnp.bfloat16
F32 = jnp.float32
Z, Y, C, TP = 4, 4, 2, 4
CAP = 4


def ep_at(z, y, c):
    return (z % Z) * (Y * C) + (y % Y) * C + c % C


def ep_moves(dz, dy, dc):
    return [
        (ep_at(z, y, c), ep_at(z + dz, y + dy, c + dc))
        for z in range(Z)
        for y in range(Y)
        for c in range(C)
    ]


def along_z(a, s):
    return lax.ppermute(a, "ep", ep_moves(s, 0, 0))


def along_y(a, s):
    return lax.ppermute(a, "ep", ep_moves(0, s, 0))


def other_core(a):
    return lax.ppermute(a, "ep", ep_moves(0, 0, 1))


def along_tp(a, s):
    return lax.ppermute(a, "tp", [(i, (i + s) % TP) for i in range(TP)])


def on_chip(*arrays):
    return [pltpu.with_memory_space_constraint(a, pltpu.VMEM) for a in arrays]


def kernel_room(mebibytes):
    return pltpu.CompilerParams(vmem_limit_bytes=mebibytes << 20)


def rms_scale(values):
    return lax.rsqrt(jnp.mean(values * values, axis=-1, keepdims=True) + NORM_EPS)


def join_kernel(q, k, v, o, w0, sems):
    loads = [
        pltpu.make_async_copy(r, w0.at[:, pl.ds(i * 512, 512)], sems.at[i])
        for i, r in enumerate((q, k, v, o))
    ]
    for load in loads:
        load.start()
    for load in loads:
        load.wait()


def join(weights):
    return pl.pallas_call(
        join_kernel,
        in_specs=[pl.BlockSpec(memory_space=pl.ANY)] * 4,
        out_specs=pl.BlockSpec(memory_space=pltpu.VMEM),
        out_shape=pltpu.VMEM((64, 2048), BF),
        scratch_shapes=[pltpu.SemaphoreType.DMA((4,))],
        name="join",
    )(*weights)


def prepare_kernel(
    at, x, gain, ig, fg, dw, mg, eg, stab, routes, weights, packed, gates, send, take
):
    xf = x[...].astype(F32)
    normed = (xf * rms_scale(xf) * gain[...]).astype(BF)
    for i in range(Z):
        packed[16 * i : 16 * i + 16, 640:1152] = normed[:, 512 * i : 512 * (i + 1)]
    nf = normed.astype(F32)
    log_input = jnp.sum(nf * ig[...].astype(F32), axis=1, keepdims=True)
    pre = jnp.sum(nf * fg[...].astype(F32), axis=1, keepdims=True)
    log_forget = jnp.minimum(pre, 0.0) - jnp.log1p(jnp.exp(-jnp.abs(pre)))
    small = lax.broadcasted_iota(jnp.int32, (16, 16), 0)
    across = lax.broadcasted_iota(jnp.int32, (16, 16), 1)
    stab_column = jnp.sum(jnp.where(small == across, stab[...], 0.0), axis=1, keepdims=True)
    lane = lax.broadcasted_iota(jnp.int32, (16, 128), 1)
    gates[...] = jnp.where(lane == 0, log_input, log_forget + stab_column)
    row = lax.broadcasted_iota(jnp.int32, (128, 64), 0)
    extra = jnp.zeros((128, 64), F32)
    for i, g in enumerate((mg, eg)):
        whole = g[...]
        high = whole.astype(BF).astype(F32)
        rest = whole - high
        mid = rest.astype(BF).astype(F32)
        for j, piece in enumerate((high, mid, rest - mid)):
            extra = jnp.where(row == 3 * i + j, piece, extra)
    eye = jnp.where(
        lax.broadcasted_iota(jnp.int32, (64, 64), 0) == lax.broadcasted_iota(jnp.int32, (64, 64), 1),
        1.0,
        0.0,
    ).astype(BF)
    turned = (((1,), (1,)), ((), ()))
    packed[:, 0:512] = dw[...]
    packed[:, 512:640] = lax.dot_general(
        eye, extra.astype(BF), turned, preferred_element_type=F32
    ).astype(BF)
    pick = jnp.where(
        lax.broadcasted_iota(jnp.int32, (16, 512), 1)
        == lax.broadcasted_iota(jnp.int32, (16, 512), 0) + at[1] * 16,
        1.0,
        0.0,
    )
    chosen = lax.dot_general(
        pick, routes[...].astype(F32), turned, precision=lax.Precision.HIGHEST,
        preferred_element_type=F32,
    )
    weight = lax.dot_general(
        pick, weights[...], turned, precision=lax.Precision.HIGHEST, preferred_element_type=F32
    )
    expert_of = (lane // CAP).astype(F32)
    named = jnp.zeros((16, 128), F32)
    weight_of = jnp.zeros((16, 128), F32)
    for k in range(4):
        hit = chosen[:, k : k + 1] == expert_of
        named = jnp.where(hit, 1.0, named)
        weight_of = jnp.where(hit, weight[:, k : k + 1], weight_of)
    before = jnp.dot(
        jnp.where(small > across, 1.0, 0.0).astype(BF), named.astype(BF),
        preferred_element_type=F32,
    )
    placed = (named > 0.5) & (before == (lane % CAP).astype(F32))
    send[...] = jnp.where(placed, 1.0, 0.0).astype(BF)
    take[...] = jnp.where(placed, weight_of, 0.0)


def prepare(at, tokens, mixer_gain, ig, fg, down_weight, mg, eg, stabilizer, routes, weights):
    def whole(a):
        return pl.BlockSpec(a.shape, lambda i, t: (0, 0))

    ins = [tokens, mixer_gain[None], ig, fg, down_weight.T, mg[None], eg[None]]
    ins += [stabilizer.T, routes.T, weights.T]
    specs = [whole(a) for a in ins]
    specs[4] = pl.BlockSpec((down_weight.shape[1], 512), lambda i, t: (0, t[0]))
    outs = [
        pltpu.VMEM((64, 1152), BF),
        pltpu.VMEM((16, 128), F32),
        pltpu.VMEM((16, 128), BF),
        pltpu.VMEM((16, 128), F32),
    ]
    return pl.pallas_call(
        prepare_kernel,
        grid_spec=pltpu.PrefetchScalarGridSpec(
            num_scalar_prefetch=1,
            grid=(1,),
            in_specs=specs,
            out_specs=[whole(a) for a in outs],
        ),
        out_shape=outs,
        name="prepare",
    )(at, *ins)


def project_kernel(
    at, n0, n1, n2, n3, w0, w1, w2, w3, p0, p1, p2, p3,
    own, t1, t2, t3,
):
    ep = at[1]
    z, y, c = ep // (Y * C), (ep // C) & 3, ep & 1
    col = pl.multiple_of(640 + y * 128, 128)
    rows = []
    for n in (n0, n1, n2, n3):
        chunks = []
        for s in range(Z):
            off = pl.multiple_of(((z + (Z - s)) & 3) * 16, 16)
            part = n[pl.ds(off, 16), pl.ds(col, 128)].astype(F32)
            chunks.append(jnp.where(c == 0, part, pltpu.roll(part, 64, 1)).astype(BF))
        rows.append(jnp.concatenate(chunks, axis=1))
    x = jnp.concatenate(rows, axis=0)
    pieces = [r for pair in zip((w0, w1, w2, w3), (p0, p1, p2, p3)) for r in pair]
    for i in range(4):
        at_i = slice(512 * i, 512 * (i + 1))
        w = jnp.concatenate([r[:, at_i] for r in pieces], axis=0)
        acc = jnp.dot(x, w, preferred_element_type=F32)
        own[:, at_i] = acc[0:16]
        for k, t in ((16, t1), (32, t2), (48, t3)):
            part = acc[k : k + 16]
            high = part.astype(BF)
            t[:, at_i] = high
            if i < 2:
                low = (part - high.astype(F32)).astype(BF)
                t[:, 2048 + 512 * i : 2048 + 512 * (i + 1)] = low


def project(at, packed_by_shift, weights, partner):
    rows, width = 16, weights[0].shape[1]
    vmem = pl.BlockSpec(memory_space=pltpu.VMEM)
    return pl.pallas_call(
        project_kernel,
        in_specs=[pl.BlockSpec(memory_space=pltpu.SMEM)] + [vmem] * 12,
        out_specs=[vmem] * 4,
        out_shape=[pltpu.VMEM((rows, width), F32)]
        + [pltpu.VMEM((rows, width + width // 2), BF)] * 3,
        compiler_params=kernel_room(8),
        name="project",
    )(at, *on_chip(*packed_by_shift, *weights, *partner))


def fetch_kernel(memory, out, sems):
    loads = [
        pltpu.make_async_copy(memory.at[n], out.at[n], sems.at[n]) for n in range(out.shape[0])
    ]
    for load in loads:
        load.start()
    for load in loads:
        load.wait()


def fetch(memory):
    return pl.pallas_call(
        fetch_kernel,
        in_specs=[pl.BlockSpec(memory_space=pltpu.HBM)],
        out_specs=pl.BlockSpec(memory_space=pltpu.VMEM),
        out_shape=pltpu.VMEM(memory.shape, F32),
        scratch_shapes=[pltpu.SemaphoreType.DMA((memory.shape[0],))],
        compiler_params=kernel_room(4),
        name="fetch",
    )(pltpu.with_memory_space_constraint(memory, pltpu.HBM))


def read_kernel(own, r1, r2, r3, gates, hg, mem, out):
    parts = []
    for i in range(4):
        at_i = slice(512 * i, 512 * (i + 1))
        total = own[:, at_i]
        for r in (r1, r2, r3):
            came = r[:, at_i].astype(F32)
            if i < 2:
                came = came + r[:, 2048 + 512 * i : 2048 + 512 * (i + 1)].astype(F32)
            total = total + came
        parts.append(total.astype(BF).astype(F32))
    query, key, value, outgate = parts
    query = query * 512 ** (-0.5)
    log_input, carry = gates[:, 0:1], gates[:, 1:2]
    peak = jnp.maximum(carry, log_input)
    within = jnp.exp(log_input - peak)
    carried = jnp.exp(carry - peak)
    score = jnp.sum(query * key, axis=1, keepdims=True) * within
    scaled = query * carried
    turned = jnp.concatenate([scaled, jnp.zeros((112, 512), F32)], axis=0).T
    read_rows = []
    for n in range(16):
        column = turned[:, n : n + 1]
        acc = jnp.zeros((8, 512), F32)
        for j in range(64):
            acc = acc + column[8 * j : 8 * j + 8] * mem[n, 0, 8 * j : 8 * j + 8, :]
        read_rows.append(jnp.sum(acc, axis=0, keepdims=True))
    read = score * value + jnp.concatenate(read_rows, axis=0)
    centered = read - jnp.mean(read, axis=1, keepdims=True)
    gated = centered * rms_scale(centered) * hg[...] * jax.nn.sigmoid(outgate)
    out[...] = gated.astype(BF)


def read(own, came, gates, head_gain, memory):
    vmem = pl.BlockSpec(memory_space=pltpu.VMEM)
    return pl.pallas_call(
        read_kernel,
        in_specs=[vmem] * 7,
        out_specs=vmem,
        out_shape=pltpu.VMEM((16, 512), BF),
        compiler_params=kernel_room(8),
        name="read",
    )(*on_chip(own, *came), gates, head_gain[None], memory)


def down_kernel(at, g, d0, d1, d2, d3, e0, e1, e2, e3, part, send, gains, full):
    ep = at[1]
    z, y, c = ep // (Y * C), (ep // C) & 3, ep & 1
    lane = lax.broadcasted_iota(jnp.int32, (16, 128), 1)
    row = lax.broadcasted_iota(jnp.int32, (16, 128), 0)
    eye = jnp.where(lane == row, 1.0, 0.0).astype(BF)
    a = jnp.concatenate(
        [
            jnp.concatenate([g[...], jnp.zeros((16, 128), BF)], axis=1),
            jnp.concatenate([jnp.zeros((16, 512), BF), eye], axis=1),
        ],
        axis=0,
    )
    low = lax.broadcasted_iota(jnp.int32, (32, 128), 1) < 64
    turn = (((1,), (1,)), ((), ()))
    for s, (d, e) in enumerate(zip((d0, d1, d2, d3), (e0, e1, e2, e3))):
        mine = lax.dot_general(a, d[...], turn, preferred_element_type=F32)
        other = lax.dot_general(a, e[...], turn, preferred_element_type=F32)
        for t in range(Y):
            j = t // 2 * 128
            m, o = mine[:, j : j + 128], other[:, j : j + 128]
            first = jnp.where(c == 0, m, o)
            second = jnp.where(c == 0, o, m)
            if t % 2 == 0:
                block = jnp.where(low, first, pltpu.roll(second, 64, 1))
            else:
                block = jnp.where(low, pltpu.roll(first, 64, 1), second)
            off = pl.multiple_of(((z + (Z - s)) & 3) * 512 + ((y + (Y - t)) & 3) * 128, 128)
            full[:, pl.ds(off, 128)] = block
    part[...] = full[0:16]
    send[...] = full[0:16].astype(BF)
    mixed_gain = full[16:17] + full[17:18] + full[18:19]
    expert_gain = full[19:20] + full[20:21] + full[21:22]
    gains[...] = jnp.concatenate(
        [mixed_gain, expert_gain, jnp.zeros((6, mixed_gain.shape[1]), F32)], axis=0
    )


def down_project(at, gated, own, partner):
    vmem = pl.BlockSpec(memory_space=pltpu.VMEM)
    return pl.pallas_call(
        down_kernel,
        in_specs=[pl.BlockSpec(memory_space=pltpu.SMEM)] + [vmem] * 9,
        out_specs=[vmem] * 3,
        out_shape=[
            pltpu.VMEM((16, 2048), F32),
            pltpu.VMEM((16, 2048), BF),
            pltpu.VMEM((8, 2048), F32),
        ],
        scratch_shapes=[pltpu.VMEM((32, 2048), F32)],
        compiler_params=kernel_room(8),
        name="down_project",
    )(at, gated, *on_chip(*own, *partner))


def layer(
    tokens,
    mixer_gain,
    query_weight,
    key_weight,
    value_weight,
    outgate_weight,
    igate_weight,
    fgate_weight,
    memory,
    stabilizer,
    head_gain,
    down_weight,
    mixed_gain,
    expert_gain,
    routes,
    route_weights,
    gate_proj,
    up_proj,
    expert_down,
    output_gain,
):
    ep_count = lax.axis_size("ep")
    tp_index = lax.axis_index("tp")
    at = jnp.stack([tp_index, lax.axis_index("ep")]).astype(jnp.int32)
    _, width = tokens.shape
    tp_width = output_gain.shape[0]

    tokens_float = tokens.astype(F32)
    w0 = join((query_weight, key_weight, value_weight, outgate_weight))
    by_z = [along_z(w0, s) for s in (2, 1, 3)]
    by_z = [w0, by_z[1], by_z[0], by_z[2]]
    packed, gates, send_from, take_with = prepare(
        at, tokens, mixer_gain, igate_weight, fgate_weight, down_weight, mixed_gain,
        expert_gain, stabilizer, routes, route_weights,
    )
    by_y = [along_y(packed, s) for s in (2, 1, 3)]
    by_y = [packed, by_y[1], by_y[0], by_y[2]]
    partner = [other_core(w) for w in by_z]
    down_y = jnp.concatenate([p[:, :640] for p in by_y], axis=0)
    down_z = [along_z(down_y, s) for s in (2, 1, 3)]
    down_z = [down_y, down_z[1], down_z[0], down_z[2]]
    own, t1, t2, t3 = project(at, by_y, by_z, partner)
    came = [along_y(t, -s) for s, t in ((2, t2), (1, t1), (3, t3))]
    down_partner = [other_core(d) for d in down_z]
    held = fetch(memory)
    gated = read(own, came, gates, head_gain, held)
    part, send, gains = down_project(at, gated, down_z, down_partner)
    mixed = part
    for s in (1, 2, 3):
        mixed = mixed + along_tp(send, s).astype(F32)

    residual_float = tokens_float + mixed * rms_scale(mixed) * gains[0]
    residual = lax.dynamic_slice_in_dim(residual_float.astype(BF), tp_index * tp_width, tp_width, 1)
    expert_in = (residual_float * rms_scale(residual_float) * gains[1]).astype(BF)
    outgoing = lax.dot_general(
        send_from.astype(BF), expert_in, (((0,), (0,)), ((), ())), preferred_element_type=F32
    ).astype(BF)
    arrived = lax.all_to_all(
        outgoing.reshape(ep_count, CAP, width), "ep", 0, 0, tiled=True
    ).reshape(ep_count * CAP, width)

    gate_pre = jnp.minimum(jnp.dot(arrived, gate_proj[0], preferred_element_type=F32), CLAMP_LIMIT)
    up_pre = jnp.clip(
        jnp.dot(arrived, up_proj[0], preferred_element_type=F32), -CLAMP_LIMIT, CLAMP_LIMIT
    )
    activation = ((up_pre + 1.0) * gate_pre * jax.nn.sigmoid(SIGMOID_SCALE * gate_pre)).astype(BF)
    partial_value = jnp.dot(activation, expert_down[0], preferred_element_type=F32)
    returned = lax.all_to_all(
        partial_value.astype(BF).reshape(ep_count, CAP, width), "ep", 0, 0, tiled=True
    ).reshape(ep_count * CAP, width)

    partial = jnp.dot(
        take_with, returned.astype(F32), precision=lax.Precision.HIGHEST,
        preferred_element_type=F32,
    )
    partial_sent = partial.astype(BF)
    combined = partial
    for s in (1, 2, 3):
        combined = combined + along_tp(partial_sent, s).astype(F32)
    scale = rms_scale(combined)
    combined_mine = lax.dynamic_slice_in_dim(combined, tp_index * tp_width, tp_width, 1)
    final_rows = residual.astype(F32) + combined_mine * scale * output_gain
    return final_rows.astype(BF)


def solution(mesh):
    placed = (
        P("ep", None),
        P(),
        P("ep", "tp"),
        P("ep", "tp"),
        P("ep", "tp"),
        P("ep", "tp"),
        P("tp", None),
        P("tp", None),
        P("ep", "tp", None, None),
        P("ep", "tp"),
        P("tp"),
        P(None, "ep"),
        P("ep"),
        P("ep"),
        P(),
        P(),
        P("ep", None, "tp"),
        P("ep", None, "tp"),
        P("ep", "tp", None),
        P("tp"),
    )
    return jax.shard_map(
        layer, mesh=mesh, in_specs=placed, out_specs=P("ep", "tp"), check_vma=False
    )
```

profile of v0, /device:TPU:0, one launch (start us, length us, event | category | flops | bytes accessed | tf_op | source)
XLA Modules:
  0.0 122.6 jit_solution(17465258205847865577)
XLA Ops:
  0.0 0.6 pad_add_fusion.at
  0.6 2.2 %prepare.1 = (bf16[64,1152]{1,0:T(8,128)(2,1)S(1)}, f32[16,128]{1,0:T(8,128)S(1)}, bf16[16,128]{1,0:T(8,128)(2,1)S(1)}, f32[16,128]{1,0:T(8,128)S(1)}) custom-call(s32[2]{0:T(128)} %pad_add_fusion.at, bf16[16,2048]{1,0:T(8,128)(2,1)} %x.1, f32[1,2048]{1,0:T(1,128)} %bitcast.44, bf16[1,2048]{1,0:T(2,128)(2,1)} %ig.1, bf16[1,2048]{1,0:T(2,128)(2,1)} %fg.1, ...), custom_call_target="tpu_custom_call" | custom-call | tf_op jit(solution)/shard_map/prepare/pallas_call | solution.py:159
  2.8 3.2 %collective-permute-start.2 = (bf16[64,1152]{1,0:T(8,128)(2,1)S(1)}, bf16[64,1152]{1,0:T(8,128)(2,1)S(1)}, u32[]{:S(2)}, u32[]{:S(2)}) collective-permute-start(bf16[64,1152]{1,0:T(8,128)(2,1)S(1)} %get-tuple-element.16.n0), channel_id=1, source_target_pairs={{0,24},{4,28},{8,0},{12,4},{16,8},{20,12},{24,16},{28,20},{32,56},... | collective-permute-start | bytes 442376 | tf_op jit(solution)/shard_map/ppermute | solution.py:36
  6.0 0.6 collective-permute-start.1
  6.6 1.0 collective-permute-start
  7.6 1.0 join.1.w0
  8.6 2.0 %collective-permute-start.3 = (bf16[64,2048]{1,0:T(8,128)(2,1)S(1)}, bf16[64,2048]{1,0:T(8,128)(2,1)S(1)}, u32[]{:S(2)}, u32[]{:S(2)}) collective-permute-start(bf16[64,2048]{1,0:T(8,128)(2,1)S(1)} %join.1.w0), channel_id=1, source_target_pairs={{0,32},{4,36},{8,40},{12,44},{16,48},{20,52},{24,56},{28,60},{32,6... | collective-permute-start | bytes 786440 | tf_op jit(solution)/shard_map/ppermute | solution.py:32
  10.6 3.6 %collective-permute-start.4 = (bf16[64,2048]{1,0:T(8,128)(2,1)S(1)}, bf16[64,2048]{1,0:T(8,128)(2,1)S(1)}, u32[]{:S(2)}, u32[]{:S(2)}) collective-permute-start(bf16[64,2048]{1,0:T(8,128)(2,1)S(1)} %join.1.w0), channel_id=1, source_target_pairs={{0,64},{4,68},{8,72},{12,76},{16,80},{20,84},{24,88},{28,92},{32,9... | collective-permute-start | bytes 786440 | tf_op jit(solution)/shard_map/ppermute | solution.py:32
  14.2 0.0 collective-permute-done.2.n3
  14.2 0.1 collective-permute-done.1.n2
  14.3 1.7 %collective-permute-done.n1 = bf16[64,1152]{1,0:T(8,128)(2,1)S(1)} collective-permute-done((bf16[64,1152]{1,0:T(8,128)(2,1)S(1)}, bf16[64,1152]{1,0:T(8,128)(2,1)S(1)}, u32[]{:S(2)}, u32[]{:S(2)}) %collective-permute-start) | collective-permute-done | bytes 147488 | tf_op jit(solution)/shard_map/ppermute | solution.py:36
  16.0 2.0 %collective-permute-start.13 = (bf16[256,640]{1,0:T(8,128)(2,1)S(1)}, bf16[256,640]{1,0:T(8,128)(2,1)S(1)}, u32[]{:S(2)}, u32[]{:S(2)}) collective-permute-start(bf16[256,640]{1,0:T(8,128)(2,1)S(1)} %pad_maximum_fusion.d0), channel_id=1, source_target_pairs={{0,32},{4,36},{8,40},{12,44},{16,48},{20,52},{24,56},{28,60},{32,6... | collective-permute-start | bytes 983048 | tf_op jit(solution)/shard_map/ppermute | solution.py:32
  18.0 2.2 %collective-permute-start.5 = (bf16[64,2048]{1,0:T(8,128)(2,1)S(1)}, bf16[64,2048]{1,0:T(8,128)(2,1)S(1)}, u32[]{:S(2)}, u32[]{:S(2)}) collective-permute-start(bf16[64,2048]{1,0:T(8,128)(2,1)S(1)} %join.1.w0), channel_id=1, source_target_pairs={{0,96},{4,100},{8,104},{12,108},{16,112},{20,116},{24,120},{28,124... | collective-permute-start | bytes 786440 | tf_op jit(solution)/shard_map/ppermute | solution.py:32
  20.2 0.0 collective-permute-start.6
  20.2 0.0 collective-permute-done.3.w1
  20.2 4.3 %collective-permute-start.14 = (bf16[256,640]{1,0:T(8,128)(2,1)S(1)}, bf16[256,640]{1,0:T(8,128)(2,1)S(1)}, u32[]{:S(2)}, u32[]{:S(2)}) collective-permute-start(bf16[256,640]{1,0:T(8,128)(2,1)S(1)} %pad_maximum_fusion.d0), channel_id=1, source_target_pairs={{0,64},{4,68},{8,72},{12,76},{16,80},{20,84},{24,88},{28,92},{32,9... | collective-permute-start | bytes 983048 | tf_op jit(solution)/shard_map/ppermute | solution.py:32
  24.5 2.5 %collective-permute-done.4.w2 = bf16[64,2048]{1,0:T(8,128)(2,1)S(1)} collective-permute-done((bf16[64,2048]{1,0:T(8,128)(2,1)S(1)}, bf16[64,2048]{1,0:T(8,128)(2,1)S(1)}, u32[]{:S(2)}, u32[]{:S(2)}) %collective-permute-start.4) | collective-permute-done | bytes 262176 | tf_op jit(solution)/shard_map/ppermute | solution.py:32
  27.0 0.0 collective-permute-start.15
  27.0 6.8 %collective-permute-done.5.w3 = bf16[64,2048]{1,0:T(8,128)(2,1)S(1)} collective-permute-done((bf16[64,2048]{1,0:T(8,128)(2,1)S(1)}, bf16[64,2048]{1,0:T(8,128)(2,1)S(1)}, u32[]{:S(2)}, u32[]{:S(2)}) %collective-permute-start.5) | collective-permute-done | bytes 262176 | tf_op jit(solution)/shard_map/ppermute | solution.py:32
  33.8 0.5 collective-permute-start.8
  34.3 0.1 collective-permute-start.9
  34.4 4.6 %collective-permute-done.14.d2 = bf16[256,640]{1,0:T(8,128)(2,1)S(1)} collective-permute-done((bf16[256,640]{1,0:T(8,128)(2,1)S(1)}, bf16[256,640]{1,0:T(8,128)(2,1)S(1)}, u32[]{:S(2)}, u32[]{:S(2)}) %collective-permute-start.14) | collective-permute-done | bytes 327712 | tf_op jit(solution)/shard_map/ppermute | solution.py:32
  39.0 1.2 collective-permute-done.15.d3
  40.2 0.5 collective-permute-start.18
  40.8 0.1 collective-permute-start.19
  40.8 0.0 collective-permute-done.9.p3
  40.8 1.1 project.1
  41.9 1.5 %collective-permute-start.10 = (bf16[16,3072]{1,0:T(8,128)(2,1)S(1)}, bf16[16,3072]{1,0:T(8,128)(2,1)S(1)}, u32[]{:S(2)}, u32[]{:S(2)}) collective-permute-start(bf16[16,3072]{1,0:T(8,128)(2,1)S(1)} %get-tuple-element.18), channel_id=1, source_target_pairs={{0,16},{4,20},{8,24},{12,28},{16,0},{20,4},{24,8},{28,12},{32,48},... | collective-permute-start | bytes 294920 | tf_op jit(solution)/shard_map/ppermute | solution.py:36
  43.5 5.2 %collective-permute-done.10.r1 = bf16[16,3072]{1,0:T(8,128)(2,1)S(1)} collective-permute-done((bf16[16,3072]{1,0:T(8,128)(2,1)S(1)}, bf16[16,3072]{1,0:T(8,128)(2,1)S(1)}, u32[]{:S(2)}, u32[]{:S(2)}) %collective-permute-start.10) | collective-permute-done | bytes 98336 | tf_op jit(solution)/shard_map/ppermute | solution.py:36
  48.7 1.2 collective-permute-start.11
  49.8 3.5 %collective-permute-done.11.r2 = bf16[16,3072]{1,0:T(8,128)(2,1)S(1)} collective-permute-done((bf16[16,3072]{1,0:T(8,128)(2,1)S(1)}, bf16[16,3072]{1,0:T(8,128)(2,1)S(1)}, u32[]{:S(2)}, u32[]{:S(2)}) %collective-permute-start.11) | collective-permute-done | bytes 98336 | tf_op jit(solution)/shard_map/ppermute | solution.py:36
  53.3 0.8 collective-permute-start.12
  54.1 5.9 %fetch.1.mem = f32[16,1,512,512]{3,2,1,0:T(8,128)S(1)} custom-call(f32[16,1,512,512]{3,2,1,0:T(8,128)} %memory.1), custom_call_target="tpu_custom_call" | custom-call | tf_op jit(solution)/shard_map/fetch/pallas_call | solution.py:228
  60.0 1.8 %read.1.g = bf16[16,512]{1,0:T(8,128)(2,1)S(1)} custom-call(f32[16,2048]{1,0:T(8,128)S(1)} %get-tuple-element.17.own, bf16[16,3072]{1,0:T(8,128)(2,1)S(1)} %collective-permute-done.10.r1, bf16[16,3072]{1,0:T(8,128)(2,1)S(1)} %collective-permute-done.11.r2, bf16[16,3072]{1,0:T(8,128)(2,1)S(1)} %collective-permute-done.12.r3, ...), custom_call_target="tpu_custom_call" | custom-call | tf_op jit(solution)/shard_map/read/pallas_call | solution.py:274
  61.8 0.0 copy-start.3
  61.8 0.0 collective-permute-done.16.e0
  61.8 0.0 collective-permute-done.17.e1
  61.9 1.6 %down_project.1 = (f32[16,2048]{1,0:T(8,128)S(1)}, bf16[16,2048]{1,0:T(8,128)(2,1)S(1)}, f32[8,2048]{1,0:T(8,128)S(1)}) custom-call(s32[2]{0:T(128)S(1)} %copy-done.1, bf16[16,512]{1,0:T(8,128)(2,1)S(1)} %read.1.g, bf16[256,640]{1,0:T(8,128)(2,1)S(1)} %pad_maximum_fusion.d0, bf16[256,640]{1,0:T(8,128)(2,1)S(1)} %collective-permute-done.13.d1, ...), custom_call_target="tpu_custom_call" | custom-call | tf_op jit(solution)/shard_map/down_project/pallas_call | solution.py:324
  63.4 2.8 %collective-permute-start.22 = (bf16[16,2048]{1,0:T(8,128)(2,1)S(1)}, bf16[16,2048]{1,0:T(8,128)(2,1)S(1)}, u32[]{:S(2)}, u32[]{:S(2)}) collective-permute-start(bf16[16,2048]{1,0:T(8,128)(2,1)S(1)} %get-tuple-element.23), channel_id=1, source_target_pairs={{0,3},{1,0},{2,1},{3,2},{4,7},{5,4},{6,5},{7,6},{8,11},{9,8},{10,9... | collective-permute-start | bytes 196616 | tf_op jit(solution)/shard_map/ppermute | solution.py:44
  66.3 0.8 collective-permute-start.21
  67.1 0.9 collective-permute-start.20
  68.0 0.2 collective-permute-done.22
  68.2 3.9 %collective-permute-done.21 = bf16[16,2048]{1,0:T(8,128)(2,1)S(1)} collective-permute-done((bf16[16,2048]{1,0:T(8,128)(2,1)S(1)}, bf16[16,2048]{1,0:T(8,128)(2,1)S(1)}, u32[]{:S(2)}, u32[]{:S(2)}) %collective-permute-start.21) | collective-permute-done | bytes 65568 | tf_op jit(solution)/shard_map/ppermute | solution.py:44
  72.1 0.7 collective-permute-done.20
  72.7 0.1 multiply_reduce_fusion.2
  72.9 0.2 multiply_reduce_fusion.1
  73.1 0.3 convolution_convert_fusion.1
  73.5 0.2 reshape.37
  73.7 18.4 %all_to_all.10 = bf16[32,4,2048]{2,1,0:T(4,128)(2,1)S(1)} all-to-all(bf16[32,4,2048]{2,1,0:T(4,128)(2,1)S(1)} %reshape.37), channel_id=1, replica_groups=mesh['ep'=32,'tp'=4] {'ep'}, dimensions={0} | all-to-all | bytes 1048576 | tf_op jit(solution)/shard_map/all_to_all | solution.py:397
  92.1 0.1 reshape.38
  92.2 2.1 %fusion.8 = f32[128,512]{1,0:T(8,128)S(1)} fusion(bf16[128,2048]{1,0:T(8,128)(2,1)S(1)} %reshape.38, bf16[1,2048,512]{2,1,0:T(8,128)(2,1)} %param.36), kind=kOutput, calls=%fused_computation.8 | convolution fusion | flops 268500992 | bytes 2883584 | tf_op jit(solution)/shard_map/dot_general | solution.py:401
  94.3 3.3 %convolution_convert_fusion = bf16[128,2048]{1,0:T(8,128)(2,1)} fusion(bf16[1,512,2048]{2,1,0:T(8,128)(2,1)S(1)} %copy-done, f32[128,512]{1,0:T(8,128)S(1)} %fusion.8, bf16[128,2048]{1,0:T(8,128)(2,1)S(1)} %reshape.38, bf16[1,2048,512]{2,1,0:T(8,128)(2,1)} %param.37), kind=kOutput, calls=%fused_computation | convolution fusion | flops 537722880 | bytes 5505024 | tf_op jit(solution)/shard_map/dot_general | solution.py:406
  97.6 1.2 %reshape.39 = bf16[32,4,2048]{2,1,0:T(4,128)(2,1)S(1)} reshape(bf16[128,2048]{1,0:T(8,128)(2,1)} %convolution_convert_fusion) | data formatting | bytes 1048576 | tf_op jit(solution)/shard_map/reshape | solution.py:408
  98.9 15.1 %all_to_all.11 = bf16[32,4,2048]{2,1,0:T(4,128)(2,1)S(1)} all-to-all(bf16[32,4,2048]{2,1,0:T(4,128)(2,1)S(1)} %reshape.39), channel_id=1, replica_groups=mesh['ep'=32,'tp'=4] {'ep'}, dimensions={0} | all-to-all | bytes 1048576 | tf_op jit(solution)/shard_map/all_to_all | solution.py:407
  113.9 0.1 reshape.40
  114.0 0.3 fusion.41
  114.4 0.6 collective-permute-start.25
  115.0 1.0 collective-permute-start.24
  116.0 1.2 collective-permute-start.23
  117.2 2.1 %collective-permute-done.25 = bf16[16,2048]{1,0:T(8,128)(2,1)S(1)} collective-permute-done((bf16[16,2048]{1,0:T(8,128)(2,1)S(1)}, bf16[16,2048]{1,0:T(8,128)(2,1)S(1)}, u32[]{:S(2)}, u32[]{:S(2)}) %collective-permute-start.25) | collective-permute-done | bytes 65568 | tf_op jit(solution)/shard_map/ppermute | solution.py:44
  119.2 1.6 %collective-permute-done.24 = bf16[16,2048]{1,0:T(8,128)(2,1)S(1)} collective-permute-done((bf16[16,2048]{1,0:T(8,128)(2,1)S(1)}, bf16[16,2048]{1,0:T(8,128)(2,1)S(1)}, u32[]{:S(2)}, u32[]{:S(2)}) %collective-permute-start.24) | collective-permute-done | bytes 65568 | tf_op jit(solution)/shard_map/ppermute | solution.py:44
  120.8 0.9 collective-permute-done.23
  121.7 0.1 multiply_reduce_fusion
  121.9 0.7 add_convert_fusion
  (28 shorter events, 0.1 us)
Async XLA Ops:
  0.0 94.3 %copy-start = (bf16[1,512,2048]{2,1,0:T(8,128)(2,1)S(1)}, bf16[1,512,2048]{2,1,0:T(8,128)(2,1)}, u32[]{:S(2)}) copy-start(bf16[1,512,2048]{2,1,0:T(8,128)(2,1)} %param.38) | copy-start | bytes 6291460
  0.6 40.2 %copy-start.1 = (s32[2]{0:T(128)S(1)}, s32[2]{0:T(128)}, u32[]{:S(2)}) copy-start(s32[2]{0:T(128)} %pad_add_fusion.at) | copy-start | bytes 28
  2.8 11.4 %collective-permute-start.2 = (bf16[64,1152]{1,0:T(8,128)(2,1)S(1)}, bf16[64,1152]{1,0:T(8,128)(2,1)S(1)}, u32[]{:S(2)}, u32[]{:S(2)}) collective-permute-start(bf16[64,1152]{1,0:T(8,128)(2,1)S(1)} %get-tuple-element.16.n0), channel_id=1, source_target_pairs={{0,24},{4,28},{8,0},{12,4},{16,8},{20,12},{24,16},{28,20},{32,56},... | collective-permute-start | bytes 442376 | tf_op jit(solution)/shard_map/ppermute | solution.py:36
  6.0 8.2 %collective-permute-start.1 = (bf16[64,1152]{1,0:T(8,128)(2,1)S(1)}, bf16[64,1152]{1,0:T(8,128)(2,1)S(1)}, u32[]{:S(2)}, u32[]{:S(2)}) collective-permute-start(bf16[64,1152]{1,0:T(8,128)(2,1)S(1)} %get-tuple-element.16.n0), channel_id=1, source_target_pairs={{0,16},{4,20},{8,24},{12,28},{16,0},{20,4},{24,8},{28,12},{32,48},... | collective-permute-start | bytes 442376 | tf_op jit(solution)/shard_map/ppermute | solution.py:36
  6.6 9.3 %collective-permute-start = (bf16[64,1152]{1,0:T(8,128)(2,1)S(1)}, bf16[64,1152]{1,0:T(8,128)(2,1)S(1)}, u32[]{:S(2)}, u32[]{:S(2)}) collective-permute-start(bf16[64,1152]{1,0:T(8,128)(2,1)S(1)} %get-tuple-element.16.n0), channel_id=1, source_target_pairs={{0,8},{4,12},{8,16},{12,20},{16,24},{20,28},{24,0},{28,4},{32,40},... | collective-permute-start | bytes 442376 | tf_op jit(solution)/shard_map/ppermute | solution.py:36
  8.6 11.6 %collective-permute-start.3 = (bf16[64,2048]{1,0:T(8,128)(2,1)S(1)}, bf16[64,2048]{1,0:T(8,128)(2,1)S(1)}, u32[]{:S(2)}, u32[]{:S(2)}) collective-permute-start(bf16[64,2048]{1,0:T(8,128)(2,1)S(1)} %join.1.w0), channel_id=1, source_target_pairs={{0,32},{4,36},{8,40},{12,44},{16,48},{20,52},{24,56},{28,60},{32,6... | collective-permute-start | bytes 786440 | tf_op jit(solution)/shard_map/ppermute | solution.py:32
  10.6 16.4 %collective-permute-start.4 = (bf16[64,2048]{1,0:T(8,128)(2,1)S(1)}, bf16[64,2048]{1,0:T(8,128)(2,1)S(1)}, u32[]{:S(2)}, u32[]{:S(2)}) collective-permute-start(bf16[64,2048]{1,0:T(8,128)(2,1)S(1)} %join.1.w0), channel_id=1, source_target_pairs={{0,64},{4,68},{8,72},{12,76},{16,80},{20,84},{24,88},{28,92},{32,9... | collective-permute-start | bytes 786440 | tf_op jit(solution)/shard_map/ppermute | solution.py:32
  16.0 18.3 %collective-permute-start.13 = (bf16[256,640]{1,0:T(8,128)(2,1)S(1)}, bf16[256,640]{1,0:T(8,128)(2,1)S(1)}, u32[]{:S(2)}, u32[]{:S(2)}) collective-permute-start(bf16[256,640]{1,0:T(8,128)(2,1)S(1)} %pad_maximum_fusion.d0), channel_id=1, source_target_pairs={{0,32},{4,36},{8,40},{12,44},{16,48},{20,52},{24,56},{28,60},{32,6... | collective-permute-start | bytes 983048 | tf_op jit(solution)/shard_map/ppermute | solution.py:32
  18.0 15.8 %collective-permute-start.5 = (bf16[64,2048]{1,0:T(8,128)(2,1)S(1)}, bf16[64,2048]{1,0:T(8,128)(2,1)S(1)}, u32[]{:S(2)}, u32[]{:S(2)}) collective-permute-start(bf16[64,2048]{1,0:T(8,128)(2,1)S(1)} %join.1.w0), channel_id=1, source_target_pairs={{0,96},{4,100},{8,104},{12,108},{16,112},{20,116},{24,120},{28,124... | collective-permute-start | bytes 786440 | tf_op jit(solution)/shard_map/ppermute | solution.py:32
  20.2 13.6 %collective-permute-start.6 = (bf16[64,2048]{1,0:T(8,128)(2,1)S(1)}, bf16[64,2048]{1,0:T(8,128)(2,1)S(1)}, u32[]{:S(2)}, u32[]{:S(2)}) collective-permute-start(bf16[64,2048]{1,0:T(8,128)(2,1)S(1)} %join.1.w0), channel_id=1, source_target_pairs={{0,4},{4,0},{8,12},{12,8},{16,20},{20,16},{24,28},{28,24},{32,36},... | collective-permute-start | bytes 786440 | tf_op jit(solution)/shard_map/ppermute | solution.py:40
  20.2 18.8 %collective-permute-start.14 = (bf16[256,640]{1,0:T(8,128)(2,1)S(1)}, bf16[256,640]{1,0:T(8,128)(2,1)S(1)}, u32[]{:S(2)}, u32[]{:S(2)}) collective-permute-start(bf16[256,640]{1,0:T(8,128)(2,1)S(1)} %pad_maximum_fusion.d0), channel_id=1, source_target_pairs={{0,64},{4,68},{8,72},{12,76},{16,80},{20,84},{24,88},{28,92},{32,9... | collective-permute-start | bytes 983048 | tf_op jit(solution)/shard_map/ppermute | solution.py:32
  27.0 13.3 %collective-permute-start.15 = (bf16[256,640]{1,0:T(8,128)(2,1)S(1)}, bf16[256,640]{1,0:T(8,128)(2,1)S(1)}, u32[]{:S(2)}, u32[]{:S(2)}) collective-permute-start(bf16[256,640]{1,0:T(8,128)(2,1)S(1)} %pad_maximum_fusion.d0), channel_id=1, source_target_pairs={{0,96},{4,100},{8,104},{12,108},{16,112},{20,116},{24,120},{28,124... | collective-permute-start | bytes 983048 | tf_op jit(solution)/shard_map/ppermute | solution.py:32
  33.8 6.4 %collective-permute-start.7 = (bf16[64,2048]{1,0:T(8,128)(2,1)S(1)}, bf16[64,2048]{1,0:T(8,128)(2,1)S(1)}, u32[]{:S(2)}, u32[]{:S(2)}) collective-permute-start(bf16[64,2048]{1,0:T(8,128)(2,1)S(1)} %collective-permute-done.3.w1), channel_id=1, source_target_pairs={{0,4},{4,0},{8,12},{12,8},{16,20},{20,16},{24,28},{28,24},{32,36},... | collective-permute-start | bytes 786440 | tf_op jit(solution)/shard_map/ppermute | solution.py:40
  33.8 6.9 %collective-permute-start.8 = (bf16[64,2048]{1,0:T(8,128)(2,1)S(1)}, bf16[64,2048]{1,0:T(8,128)(2,1)S(1)}, u32[]{:S(2)}, u32[]{:S(2)}) collective-permute-start(bf16[64,2048]{1,0:T(8,128)(2,1)S(1)} %collective-permute-done.4.w2), channel_id=1, source_target_pairs={{0,4},{4,0},{8,12},{12,8},{16,20},{20,16},{24,28},{28,24},{32,36},... | collective-permute-start | bytes 786440 | tf_op jit(solution)/shard_map/ppermute | solution.py:40
  34.3 6.5 %collective-permute-start.9 = (bf16[64,2048]{1,0:T(8,128)(2,1)S(1)}, bf16[64,2048]{1,0:T(8,128)(2,1)S(1)}, u32[]{:S(2)}, u32[]{:S(2)}) collective-permute-start(bf16[64,2048]{1,0:T(8,128)(2,1)S(1)} %collective-permute-done.5.w3), channel_id=1, source_target_pairs={{0,4},{4,0},{8,12},{12,8},{16,20},{20,16},{24,28},{28,24},{32,36},... | collective-permute-start | bytes 786440 | tf_op jit(solution)/shard_map/ppermute | solution.py:40
  39.0 22.8 %collective-permute-start.16 = (bf16[256,640]{1,0:T(8,128)(2,1)S(1)}, bf16[256,640]{1,0:T(8,128)(2,1)S(1)}, u32[]{:S(2)}, u32[]{:S(2)}) collective-permute-start(bf16[256,640]{1,0:T(8,128)(2,1)S(1)} %pad_maximum_fusion.d0), channel_id=1, source_target_pairs={{0,4},{4,0},{8,12},{12,8},{16,20},{20,16},{24,28},{28,24},{32,36},... | collective-permute-start | bytes 983048 | tf_op jit(solution)/shard_map/ppermute | solution.py:40
  40.2 21.6 %collective-permute-start.17 = (bf16[256,640]{1,0:T(8,128)(2,1)S(1)}, bf16[256,640]{1,0:T(8,128)(2,1)S(1)}, u32[]{:S(2)}, u32[]{:S(2)}) collective-permute-start(bf16[256,640]{1,0:T(8,128)(2,1)S(1)} %collective-permute-done.13.d1), channel_id=1, source_target_pairs={{0,4},{4,0},{8,12},{12,8},{16,20},{20,16},{24,28},{28,24},{32,36},... | collective-permute-start | bytes 983048 | tf_op jit(solution)/shard_map/ppermute | solution.py:40
  40.2 21.6 %collective-permute-start.18 = (bf16[256,640]{1,0:T(8,128)(2,1)S(1)}, bf16[256,640]{1,0:T(8,128)(2,1)S(1)}, u32[]{:S(2)}, u32[]{:S(2)}) collective-permute-start(bf16[256,640]{1,0:T(8,128)(2,1)S(1)} %collective-permute-done.14.d2), channel_id=1, source_target_pairs={{0,4},{4,0},{8,12},{12,8},{16,20},{20,16},{24,28},{28,24},{32,36},... | collective-permute-start | bytes 983048 | tf_op jit(solution)/shard_map/ppermute | solution.py:40
  40.8 21.1 %collective-permute-start.19 = (bf16[256,640]{1,0:T(8,128)(2,1)S(1)}, bf16[256,640]{1,0:T(8,128)(2,1)S(1)}, u32[]{:S(2)}, u32[]{:S(2)}) collective-permute-start(bf16[256,640]{1,0:T(8,128)(2,1)S(1)} %collective-permute-done.15.d3), channel_id=1, source_target_pairs={{0,4},{4,0},{8,12},{12,8},{16,20},{20,16},{24,28},{28,24},{32,36},... | collective-permute-start | bytes 983048 | tf_op jit(solution)/shard_map/ppermute | solution.py:40
  41.9 6.7 %collective-permute-start.10 = (bf16[16,3072]{1,0:T(8,128)(2,1)S(1)}, bf16[16,3072]{1,0:T(8,128)(2,1)S(1)}, u32[]{:S(2)}, u32[]{:S(2)}) collective-permute-start(bf16[16,3072]{1,0:T(8,128)(2,1)S(1)} %get-tuple-element.18), channel_id=1, source_target_pairs={{0,16},{4,20},{8,24},{12,28},{16,0},{20,4},{24,8},{28,12},{32,48},... | collective-permute-start | bytes 294920 | tf_op jit(solution)/shard_map/ppermute | solution.py:36
  48.7 4.6 %collective-permute-start.11 = (bf16[16,3072]{1,0:T(8,128)(2,1)S(1)}, bf16[16,3072]{1,0:T(8,128)(2,1)S(1)}, u32[]{:S(2)}, u32[]{:S(2)}) collective-permute-start(bf16[16,3072]{1,0:T(8,128)(2,1)S(1)} %get-tuple-element.19), channel_id=1, source_target_pairs={{0,24},{4,28},{8,0},{12,4},{16,8},{20,12},{24,16},{28,20},{32,56},... | collective-permute-start | bytes 294920 | tf_op jit(solution)/shard_map/ppermute | solution.py:36
  53.3 6.7 %copy-start.2 = (f32[512]{0:T(512)S(1)}, f32[512]{0:T(512)}, u32[]{:S(2)}) copy-start(f32[512]{0:T(512)} %param.30) | copy-start | bytes 6148
  53.3 6.7 %collective-permute-start.12 = (bf16[16,3072]{1,0:T(8,128)(2,1)S(1)}, bf16[16,3072]{1,0:T(8,128)(2,1)S(1)}, u32[]{:S(2)}, u32[]{:S(2)}) collective-permute-start(bf16[16,3072]{1,0:T(8,128)(2,1)S(1)} %get-tuple-element.20), channel_id=1, source_target_pairs={{0,8},{4,12},{8,16},{12,20},{16,24},{20,28},{24,0},{28,4},{32,40},... | collective-permute-start | bytes 294920 | tf_op jit(solution)/shard_map/ppermute | solution.py:36
  61.8 11.1 %copy-start.3 = (bf16[16,2048]{1,0:T(8,128)(2,1)S(1)}, bf16[16,2048]{1,0:T(8,128)(2,1)}, u32[]{:S(2)}) copy-start(bf16[16,2048]{1,0:T(8,128)(2,1)} %x.1) | copy-start | bytes 196612
  63.4 4.7 %collective-permute-start.22 = (bf16[16,2048]{1,0:T(8,128)(2,1)S(1)}, bf16[16,2048]{1,0:T(8,128)(2,1)S(1)}, u32[]{:S(2)}, u32[]{:S(2)}) collective-permute-start(bf16[16,2048]{1,0:T(8,128)(2,1)S(1)} %get-tuple-element.23), channel_id=1, source_target_pairs={{0,3},{1,0},{2,1},{3,2},{4,7},{5,4},{6,5},{7,6},{8,11},{9,8},{10,9... | collective-permute-start | bytes 196616 | tf_op jit(solution)/shard_map/ppermute | solution.py:44
  66.3 5.8 %collective-permute-start.21 = (bf16[16,2048]{1,0:T(8,128)(2,1)S(1)}, bf16[16,2048]{1,0:T(8,128)(2,1)S(1)}, u32[]{:S(2)}, u32[]{:S(2)}) collective-permute-start(bf16[16,2048]{1,0:T(8,128)(2,1)S(1)} %get-tuple-element.23), channel_id=1, source_target_pairs={{0,2},{1,3},{2,0},{3,1},{4,6},{5,7},{6,4},{7,5},{8,10},{9,11},{10,... | collective-permute-start | bytes 196616 | tf_op jit(solution)/shard_map/ppermute | solution.py:44
  67.1 5.7 %collective-permute-start.20 = (bf16[16,2048]{1,0:T(8,128)(2,1)S(1)}, bf16[16,2048]{1,0:T(8,128)(2,1)S(1)}, u32[]{:S(2)}, u32[]{:S(2)}) collective-permute-start(bf16[16,2048]{1,0:T(8,128)(2,1)S(1)} %get-tuple-element.23), channel_id=1, source_target_pairs={{0,1},{1,2},{2,3},{3,0},{4,5},{5,6},{6,7},{7,4},{8,9},{9,10},{10,1... | collective-permute-start | bytes 196616 | tf_op jit(solution)/shard_map/ppermute | solution.py:44
  97.6 24.3 %copy-start.4 = (f32[512]{0:T(512)S(1)}, f32[512]{0:T(512)}, u32[]{:S(2)}) copy-start(f32[512]{0:T(512)} %param.39) | copy-start | bytes 6148
  114.4 4.9 %collective-permute-start.25 = (bf16[16,2048]{1,0:T(8,128)(2,1)S(1)}, bf16[16,2048]{1,0:T(8,128)(2,1)S(1)}, u32[]{:S(2)}, u32[]{:S(2)}) collective-permute-start(bf16[16,2048]{1,0:T(8,128)(2,1)S(1)} %get-tuple-element.33), channel_id=1, source_target_pairs={{0,3},{1,0},{2,1},{3,2},{4,7},{5,4},{6,5},{7,6},{8,11},{9,8},{10,9... | collective-permute-start | bytes 196616 | tf_op jit(solution)/shard_map/ppermute | solution.py:44
  115.0 5.8 %collective-permute-start.24 = (bf16[16,2048]{1,0:T(8,128)(2,1)S(1)}, bf16[16,2048]{1,0:T(8,128)(2,1)S(1)}, u32[]{:S(2)}, u32[]{:S(2)}) collective-permute-start(bf16[16,2048]{1,0:T(8,128)(2,1)S(1)} %get-tuple-element.33), channel_id=1, source_target_pairs={{0,2},{1,3},{2,0},{3,1},{4,6},{5,7},{6,4},{7,5},{8,10},{9,11},{10,... | collective-permute-start | bytes 196616 | tf_op jit(solution)/shard_map/ppermute | solution.py:44
  116.0 5.8 %collective-permute-start.23 = (bf16[16,2048]{1,0:T(8,128)(2,1)S(1)}, bf16[16,2048]{1,0:T(8,128)(2,1)S(1)}, u32[]{:S(2)}, u32[]{:S(2)}) collective-permute-start(bf16[16,2048]{1,0:T(8,128)(2,1)S(1)} %get-tuple-element.33), channel_id=1, source_target_pairs={{0,1},{1,2},{2,3},{3,0},{4,5},{5,6},{6,7},{7,4},{8,9},{9,10},{10,1... | collective-permute-start | bytes 196616 | tf_op jit(solution)/shard_map/ppermute | solution.py:44
where the time goes:
time: 123 us
  waiting for transfers between devices  34.9 us (28%)
  blocking collectives  33.5 us (27%)
  starting transfers between devices  30.8 us (25%)
  Pallas kernels  13.5 us (11%)
  matrix products  6.03 us (5%)
  other arithmetic  1.86 us (2%)
  local copies, waits for them, and re-layouts  1.75 us (1%)
    all_to_all x1, blocking collectives, layer(): lax.all_to_all(outgoing.reshape(ep_count, CAP, width), 'ep', 0, 0, tiled=...  18.4 us
    ppermute x6, waiting for transfers between devices, along_z(): return lax.ppermute(a, 'ep', ep_moves(s, 0, 0))  15.1 us
    all_to_all x1, blocking collectives, layer(): lax.all_to_all(partial_value.astype(BF).reshape(ep_count, CAP, width), 'e...  15.1 us
    ppermute x6, starting transfers between devices, along_z(): return lax.ppermute(a, 'ep', ep_moves(s, 0, 0))  14 us
    ppermute x6, waiting for transfers between devices, along_y(): return lax.ppermute(a, 'ep', ep_moves(0, s, 0))  10.4 us
    ppermute x6, waiting for transfers between devices, along_tp(): return lax.ppermute(a, 'tp', [(i, (i + s) % TP) for i in range(TP)])  9.34 us
    ppermute x6, starting transfers between devices, along_y(): return lax.ppermute(a, 'ep', ep_moves(0, s, 0))  8.28 us
    ppermute x6, starting transfers between devices, along_tp(): return lax.ppermute(a, 'tp', [(i, (i + s) % TP) for i in range(TP)])  7.32 us
  transfers between devices with their start and end apart: 26, of which 14 were waited for; matrix products, arithmetic and copies ran while one was open for 0% of the time, Pallas kernels for 8%

commit v1 on v0

v1 whole, which is shorter than its diff:
```python
import jax
import jax.numpy as jnp
from jax import lax
from jax.experimental import pallas as pl
from jax.experimental.pallas import tpu as pltpu
from jax.sharding import PartitionSpec as P


NORM_EPS = 1e-06
CLAMP_LIMIT = 7.0
SIGMOID_SCALE = 1.702
BF = jnp.bfloat16
F32 = jnp.float32
Z, Y, C, TP = 4, 4, 2, 4


def ep_at(z, y, c):
    return (z % Z) * (Y * C) + (y % Y) * C + c % C


def ep_moves(dz, dy, dc):
    return [
        (ep_at(z, y, c), ep_at(z + dz, y + dy, c + dc))
        for z in range(Z)
        for y in range(Y)
        for c in range(C)
    ]


def along_z(a, s):
    return lax.ppermute(a, "ep", ep_moves(s, 0, 0))


def along_y(a, s):
    return lax.ppermute(a, "ep", ep_moves(0, s, 0))


def other_core(a):
    return lax.ppermute(a, "ep", ep_moves(0, 0, 1))


def along_tp(a, s):
    return lax.ppermute(a, "tp", [(i, (i + s) % TP) for i in range(TP)])


def on_chip(*arrays):
    return [pltpu.with_memory_space_constraint(a, pltpu.VMEM) for a in arrays]


def kernel_room(mebibytes):
    return pltpu.CompilerParams(vmem_limit_bytes=mebibytes << 20)


def rms_scale(values):
    return lax.rsqrt(jnp.mean(values * values, axis=-1, keepdims=True) + NORM_EPS)


def join_kernel(q, k, v, o, w0, sems):
    loads = [
        pltpu.make_async_copy(r, w0.at[:, pl.ds(i * 512, 512)], sems.at[i])
        for i, r in enumerate((q, k, v, o))
    ]
    for load in loads:
        load.start()
    for load in loads:
        load.wait()


def join(weights):
    return pl.pallas_call(
        join_kernel,
        in_specs=[pl.BlockSpec(memory_space=pl.ANY)] * 4,
        out_specs=pl.BlockSpec(memory_space=pltpu.VMEM),
        out_shape=pltpu.VMEM((64, 2048), BF),
        scratch_shapes=[pltpu.SemaphoreType.DMA((4,))],
        name="join",
    )(*weights)


def normed_of(x, gain):
    xf = x[...].astype(F32)
    return (xf * rms_scale(xf) * gain[...]).astype(BF)


def split_in_three(whole):
    high = whole.astype(BF).astype(F32)
    rest = whole - high
    mid = rest.astype(BF).astype(F32)
    return high, mid, rest - mid


TURNED = (((1,), (1,)), ((), ()))


def prepare_kernel(x, gain, dw, mg, eg, out0, out1, out2, out3, normed, down, sem):
    y = (lax.axis_index("ep") // C) & 3
    col = pl.multiple_of(lax.axis_index("tp") * 512, 128)
    load = pltpu.make_async_copy(dw.at[:, pl.ds(col, 512)], down, sem)
    load.start()
    normed[...] = normed_of(x, gain)
    row = lax.broadcasted_iota(jnp.int32, (8, 64), 0)
    extra = jnp.zeros((8, 64), F32)
    for i, g in enumerate((mg, eg)):
        for j, piece in enumerate(split_in_three(g[...])):
            extra = jnp.where(row == 3 * i + j, piece, extra)
    extra = jnp.concatenate([extra, jnp.zeros((8, 576), F32)], axis=1).astype(BF)
    load.wait()
    for s, out in enumerate((out0, out1, out2, out3)):
        out[0:64, 0:512] = down[...]
        out[64:72] = extra
        target = (y + s) & 3
        for i in range(Z):
            off = pl.multiple_of(512 * i + target * 128, 128)
            out[16 * i : 16 * i + 16, 512:640] = normed[:, pl.ds(off, 128)]


def prepare(tokens, mixer_gain, down_weight, mg, eg):
    vmem = pl.BlockSpec(memory_space=pltpu.VMEM)
    return pl.pallas_call(
        prepare_kernel,
        in_specs=[vmem, vmem, pl.BlockSpec(memory_space=pl.ANY), vmem, vmem],
        out_specs=[vmem] * 4,
        out_shape=[pltpu.VMEM((72, 640), BF)] * 4,
        scratch_shapes=[
            pltpu.VMEM((16, 2048), BF),
            pltpu.VMEM((64, 512), BF),
            pltpu.SemaphoreType.DMA,
        ],
        name="prepare",
    )(tokens, mixer_gain[None], down_weight.T, mg[None], eg[None])


def route_kernel(x, gain, ig, fg, stab, routes, weights, gates, send, take):
    nf = normed_of(x, gain).astype(F32)
    log_input = jnp.sum(nf * ig[...].astype(F32), axis=1, keepdims=True)
    pre = jnp.sum(nf * fg[...].astype(F32), axis=1, keepdims=True)
    log_forget = jnp.minimum(pre, 0.0) - jnp.log1p(jnp.exp(-jnp.abs(pre)))
    small = lax.broadcasted_iota(jnp.int32, (16, 16), 0)
    across = lax.broadcasted_iota(jnp.int32, (16, 16), 1)
    stab_column = jnp.sum(jnp.where(small == across, stab[...], 0.0), axis=1, keepdims=True)
    first = lax.broadcasted_iota(jnp.int32, (16, 128), 1)
    gates[...] = jnp.where(first == 0, log_input, log_forget + stab_column)
    pick = jnp.where(
        lax.broadcasted_iota(jnp.int32, (16, 512), 1)
        == lax.broadcasted_iota(jnp.int32, (16, 512), 0) + lax.axis_index("ep") * 16,
        1.0,
        0.0,
    )
    chosen = lax.dot_general(
        pick, routes[...].astype(F32), TURNED, precision=lax.Precision.HIGHEST,
        preferred_element_type=F32,
    )
    weight = lax.dot_general(
        pick, weights[...], TURNED, precision=lax.Precision.HIGHEST, preferred_element_type=F32
    )
    lane = lax.broadcasted_iota(jnp.int32, (16, 256), 1)
    expert_of = (lane >> 3).astype(F32)
    named = jnp.zeros((16, 256), F32)
    weight_of = jnp.zeros((16, 256), F32)
    for k in range(4):
        hit = chosen[:, k : k + 1] == expert_of
        named = jnp.where(hit, 1.0, named)
        weight_of = jnp.where(hit, weight[:, k : k + 1], weight_of)
    before = jnp.dot(
        jnp.where(small > across, 1.0, 0.0).astype(BF), named.astype(BF),
        preferred_element_type=F32,
    )
    placed = (named > 0.5) & (before == (lane & 3).astype(F32))
    for h in range(2):
        half = placed & (((lane >> 2) & 1) == h)
        send[16 * h : 16 * h + 16] = jnp.where(half, 1.0, 0.0).astype(BF)
        taken = jnp.where(half, weight_of, 0.0)
        for j, piece in enumerate(split_in_three(taken)):
            at = 48 * h + 16 * j
            take[at : at + 16] = piece.astype(BF)


def route(tokens, mixer_gain, ig, fg, stabilizer, routes, weights):
    vmem = pl.BlockSpec(memory_space=pltpu.VMEM)
    return pl.pallas_call(
        route_kernel,
        in_specs=[vmem] * 7,
        out_specs=[vmem] * 3,
        out_shape=[
            pltpu.VMEM((16, 128), F32),
            pltpu.VMEM((32, 256), BF),
            pltpu.VMEM((96, 256), BF),
        ],
        name="route",
    )(tokens, mixer_gain[None], ig, fg, stabilizer.T, routes.T, weights.T)


def stack_kernel(a0, a1, a2, a3, out):
    for i, a in enumerate((a0, a1, a2, a3)):
        out[64 * i : 64 * i + 64] = a[0:64, 0:512]
        out[256 + 8 * i : 264 + 8 * i] = a[64:72, 0:512]


def stack_down(pieces):
    vmem = pl.BlockSpec(memory_space=pltpu.VMEM)
    return pl.pallas_call(
        stack_kernel,
        in_specs=[vmem] * 4,
        out_specs=vmem,
        out_shape=pltpu.VMEM((288, 512), BF),
        compiler_params=kernel_room(4),
        name="stack_down",
    )(*on_chip(*pieces))


def project_kernel(
    n0, n1, n2, n3, w0, w1, w2, w3, p0, p1, p2, p3, own, t1, t2, t3
):
    ep = lax.axis_index("ep")
    z, c = ep // (Y * C), ep & 1
    rows = []
    for n in (n0, n1, n2, n3):
        chunks = []
        for s in range(Z):
            off = pl.multiple_of(((z + (Z - s)) & 3) * 16, 16)
            part = n[pl.ds(off, 16), 512:640].astype(F32)
            chunks.append(jnp.where(c == 0, part, pltpu.roll(part, 64, 1)).astype(BF))
        rows.append(jnp.concatenate(chunks, axis=1))
    x = jnp.concatenate(rows, axis=0)
    pieces = [r for pair in zip((w0, w1, w2, w3), (p0, p1, p2, p3)) for r in pair]
    for i in range(4):
        at_i = slice(512 * i, 512 * (i + 1))
        w = jnp.concatenate([r[:, at_i] for r in pieces], axis=0)
        acc = jnp.dot(x, w, preferred_element_type=F32)
        own[:, at_i] = acc[0:16]
        for k, t in ((16, t1), (32, t2), (48, t3)):
            part = acc[k : k + 16]
            high = part.astype(BF)
            t[:, at_i] = high
            if i < 2:
                low = (part - high.astype(F32)).astype(BF)
                t[:, 2048 + 512 * i : 2048 + 512 * (i + 1)] = low


def project(packed_by_shift, weights, partner):
    rows, width = 16, weights[0].shape[1]
    vmem = pl.BlockSpec(memory_space=pltpu.VMEM)
    return pl.pallas_call(
        project_kernel,
        in_specs=[vmem] * 12,
        out_specs=[vmem] * 4,
        out_shape=[pltpu.VMEM((rows, width), F32)]
        + [pltpu.VMEM((rows, width + width // 2), BF)] * 3,
        compiler_params=kernel_room(8),
        name="project",
    )(*on_chip(*packed_by_shift, *weights, *partner))


def fetch_kernel(memory, out, sems):
    loads = [
        pltpu.make_async_copy(memory.at[n], out.at[n], sems.at[n]) for n in range(out.shape[0])
    ]
    for load in loads:
        load.start()
    for load in loads:
        load.wait()


def fetch(memory):
    return pl.pallas_call(
        fetch_kernel,
        in_specs=[pl.BlockSpec(memory_space=pltpu.HBM)],
        out_specs=pl.BlockSpec(memory_space=pltpu.VMEM),
        out_shape=pltpu.VMEM(memory.shape, F32),
        scratch_shapes=[pltpu.SemaphoreType.DMA((memory.shape[0],))],
        compiler_params=kernel_room(4),
        name="fetch",
    )(pltpu.with_memory_space_constraint(memory, pltpu.HBM))


def read_kernel(own, r1, r2, r3, gates, hg, mem, out):
    parts = []
    for i in range(4):
        at_i = slice(512 * i, 512 * (i + 1))
        total = own[:, at_i]
        for r in (r1, r2, r3):
            came = r[:, at_i].astype(F32)
            if i < 2:
                came = came + r[:, 2048 + 512 * i : 2048 + 512 * (i + 1)].astype(F32)
            total = total + came
        parts.append(total.astype(BF).astype(F32))
    query, key, value, outgate = parts
    query = query * 512 ** (-0.5)
    log_input, carry = gates[:, 0:1], gates[:, 1:2]
    peak = jnp.maximum(carry, log_input)
    within = jnp.exp(log_input - peak)
    carried = jnp.exp(carry - peak)
    score = jnp.sum(query * key, axis=1, keepdims=True) * within
    scaled = query * carried
    turned = jnp.concatenate([scaled, jnp.zeros((112, 512), F32)], axis=0).T
    read_rows = []
    for n in range(16):
        column = turned[:, n : n + 1]
        acc = jnp.zeros((8, 512), F32)
        for j in range(64):
            acc = acc + column[8 * j : 8 * j + 8] * mem[n, 0, 8 * j : 8 * j + 8, :]
        read_rows.append(jnp.sum(acc, axis=0, keepdims=True))
    read = score * value + jnp.concatenate(read_rows, axis=0)
    centered = read - jnp.mean(read, axis=1, keepdims=True)
    gated = centered * rms_scale(centered) * hg[...] * jax.nn.sigmoid(outgate)
    out[...] = gated.astype(BF)


def read(own, came, gates, head_gain, memory):
    vmem = pl.BlockSpec(memory_space=pltpu.VMEM)
    return pl.pallas_call(
        read_kernel,
        in_specs=[vmem] * 7,
        out_specs=vmem,
        out_shape=pltpu.VMEM((16, 512), BF),
        compiler_params=kernel_room(8),
        name="read",
    )(*on_chip(own, *came), gates, head_gain[None], memory)


def paired(mine, other, c, odd):
    first = jnp.where(c == 0, mine, other)
    second = jnp.where(c == 0, other, mine)
    low = lax.broadcasted_iota(jnp.int32, mine.shape, 1) < 64
    if odd:
        return jnp.where(low, pltpu.roll(first, 64, 1), second)
    return jnp.where(low, first, pltpu.roll(second, 64, 1))


def down_kernel(g, d0, d1, d2, d3, e0, e1, e2, e3, part, send, gains, factors):
    ep = lax.axis_index("ep")
    z, y, c = ep // (Y * C), (ep // C) & 3, ep & 1
    gated = g[...]
    for s, (d, e) in enumerate(zip((d0, d1, d2, d3), (e0, e1, e2, e3))):
        mine = lax.dot_general(gated, d[0:256], TURNED, preferred_element_type=F32)
        other = lax.dot_general(gated, e[0:256], TURNED, preferred_element_type=F32)
        my_gains = d[256:288, 0:128].astype(F32)
        other_gains = e[256:288, 0:128].astype(F32)
        for t in range(Y):
            at = slice(t // 2 * 128, t // 2 * 128 + 128)
            block = paired(mine[:, at], other[:, at], c, t % 2 == 1)
            off = pl.multiple_of(((z + (Z - s)) & 3) * 512 + ((y + (Y - t)) & 3) * 128, 128)
            part[:, pl.ds(off, 128)] = block
            send[:, pl.ds(off, 128)] = block.astype(BF)
            at = slice(8 * t, 8 * t + 8)
            factors[:, pl.ds(off, 128)] = paired(my_gains[at], other_gains[at], c, False)
    gains[0:1] = factors[0:1] + factors[1:2] + factors[2:3]
    gains[1:2] = factors[3:4] + factors[4:5] + factors[5:6]


def down_project(gated, own, partner):
    vmem = pl.BlockSpec(memory_space=pltpu.VMEM)
    return pl.pallas_call(
        down_kernel,
        in_specs=[vmem] * 9,
        out_specs=[vmem] * 3,
        out_shape=[
            pltpu.VMEM((16, 2048), F32),
            pltpu.VMEM((16, 2048), BF),
            pltpu.VMEM((8, 2048), F32),
        ],
        scratch_shapes=[pltpu.VMEM((8, 2048), F32)],
        compiler_params=kernel_room(8),
        name="down_project",
    )(gated, *on_chip(*own, *partner))


def fetch_experts_kernel(g, u, d, gate, up, down, sems):
    loads = [
        pltpu.make_async_copy(r.at[0], o, sems.at[i])
        for i, (r, o) in enumerate(((g, gate), (u, up), (d, down)))
    ]
    for load in loads:
        load.start()
    for load in loads:
        load.wait()


def fetch_experts(*arrays):
    return pl.pallas_call(
        fetch_experts_kernel,
        in_specs=[pl.BlockSpec(memory_space=pltpu.HBM)] * 3,
        out_specs=[pl.BlockSpec(memory_space=pltpu.VMEM)] * 3,
        out_shape=[pltpu.VMEM(a.shape[1:], BF) for a in arrays],
        scratch_shapes=[pltpu.SemaphoreType.DMA((3,))],
        compiler_params=kernel_room(4),
        name="fetch_experts",
    )(*[pltpu.with_memory_space_constraint(a, pltpu.HBM) for a in arrays])


def dispatch_kernel(x, part, r1, r2, r3, gains, send, residual, outgoing):
    mixed = part[...] + r1[...].astype(F32) + r2[...].astype(F32) + r3[...].astype(F32)
    total = x[...].astype(F32) + mixed * rms_scale(mixed) * gains[0:1]
    residual[...] = total.astype(BF)
    expert_in = (total * rms_scale(total) * gains[1:2]).astype(BF)
    halves = jnp.concatenate([expert_in[:, 0:1024], expert_in[:, 1024:2048]], axis=0)
    outgoing[...] = lax.dot_general(
        send[...], halves, (((0,), (0,)), ((), ())), preferred_element_type=F32
    ).astype(BF)


def dispatch(tokens, part, came, gains, send_from):
    vmem = pl.BlockSpec(memory_space=pltpu.VMEM)
    return pl.pallas_call(
        dispatch_kernel,
        in_specs=[vmem] * 7,
        out_specs=[vmem] * 2,
        out_shape=[pltpu.VMEM((16, 2048), BF), pltpu.VMEM((256, 1024), BF)],
        compiler_params=kernel_room(8),
        name="dispatch",
    )(tokens, part, *on_chip(*came), gains, send_from)


def experts_kernel(arrived, gate_w, up_w, down_w, out):
    row = lax.broadcasted_iota(jnp.int32, (128, 256), 0)
    lane = lax.broadcasted_iota(jnp.int32, (128, 256), 1)
    place = ((row >> 2) << 3) + (row & 3)
    rows = jnp.concatenate(
        [
            jnp.dot(
                jnp.where(lane == place + 4 * h, 1.0, 0.0).astype(BF), arrived[...],
                preferred_element_type=F32,
            ).astype(BF)
            for h in range(2)
        ],
        axis=1,
    )
    gate = jnp.minimum(jnp.dot(rows, gate_w[...], preferred_element_type=F32), CLAMP_LIMIT)
    up = jnp.clip(
        jnp.dot(rows, up_w[...], preferred_element_type=F32), -CLAMP_LIMIT, CLAMP_LIMIT
    )
    activation = ((up + 1.0) * gate * jax.nn.sigmoid(SIGMOID_SCALE * gate)).astype(BF)
    value = jnp.dot(activation, down_w[...], preferred_element_type=F32).astype(BF)
    both = jnp.concatenate([value[:, 0:1024], value[:, 1024:2048]], axis=0)
    goes = lax.broadcasted_iota(jnp.int32, (256, 256), 0)
    source = lax.broadcasted_iota(jnp.int32, (256, 256), 1)
    wanted = ((goes >> 2) & 1) * 128 + ((goes >> 3) << 2) + (goes & 3)
    out[...] = jnp.dot(
        jnp.where(source == wanted, 1.0, 0.0).astype(BF), both, preferred_element_type=F32
    ).astype(BF)


def run_experts(arrived, weights):
    vmem = pl.BlockSpec(memory_space=pltpu.VMEM)
    return pl.pallas_call(
        experts_kernel,
        in_specs=[vmem] * 4,
        out_specs=vmem,
        out_shape=pltpu.VMEM(arrived.shape, BF),
        compiler_params=kernel_room(16),
        name="experts",
    )(*on_chip(arrived), *weights)


def combine_kernel(take, returned, part, send):
    sums = jnp.dot(take[...], returned[...], preferred_element_type=F32)
    for h in range(2):
        at = 48 * h
        half = sums[at : at + 16] + sums[at + 16 : at + 32] + sums[at + 32 : at + 48]
        part[:, 1024 * h : 1024 * (h + 1)] = half
        send[:, 1024 * h : 1024 * (h + 1)] = half.astype(BF)


def combine(take_with, returned):
    vmem = pl.BlockSpec(memory_space=pltpu.VMEM)
    return pl.pallas_call(
        combine_kernel,
        in_specs=[vmem] * 2,
        out_specs=[vmem] * 2,
        out_shape=[pltpu.VMEM((16, 2048), F32), pltpu.VMEM((16, 2048), BF)],
        compiler_params=kernel_room(8),
        name="combine",
    )(take_with, *on_chip(returned))


def finish_kernel(part, r1, r2, r3, residual, gain, out, total):
    combined = part[...] + r1[...].astype(F32) + r2[...].astype(F32) + r3[...].astype(F32)
    scale = rms_scale(combined)
    total[...] = combined
    col = pl.multiple_of(lax.axis_index("tp") * 512, 128)
    mine = total[:, pl.ds(col, 512)]
    out[...] = (residual[:, pl.ds(col, 512)].astype(F32) + mine * scale * gain[...]).astype(BF)


def finish(part, came, residual, output_gain):
    vmem = pl.BlockSpec(memory_space=pltpu.VMEM)
    return pl.pallas_call(
        finish_kernel,
        in_specs=[vmem] * 6,
        out_specs=vmem,
        out_shape=jax.ShapeDtypeStruct((16, 512), BF),
        scratch_shapes=[pltpu.VMEM((16, 2048), F32)],
        compiler_params=kernel_room(8),
        name="finish",
    )(part, *on_chip(*came), residual, output_gain[None])


def layer(
    tokens,
    mixer_gain,
    query_weight,
    key_weight,
    value_weight,
    outgate_weight,
    igate_weight,
    fgate_weight,
    memory,
    stabilizer,
    head_gain,
    down_weight,
    mixed_gain,
    expert_gain,
    routes,
    route_weights,
    gate_proj,
    up_proj,
    expert_down,
    output_gain,
):
    ep_count = lax.axis_size("ep")
    packed = prepare(tokens, mixer_gain, down_weight, mixed_gain, expert_gain)
    by_y = [along_y(packed[s], s) for s in (2, 1, 3)]
    by_y = [packed[0], by_y[1], by_y[0], by_y[2]]
    w0 = join((query_weight, key_weight, value_weight, outgate_weight))
    by_z = [along_z(w0, s) for s in (2, 1, 3)]
    by_z = [w0, by_z[1], by_z[0], by_z[2]]
    gates, send_from, take_with = route(
        tokens, mixer_gain, igate_weight, fgate_weight, stabilizer, routes, route_weights
    )
    down_y = stack_down(by_y)
    down_z = [along_z(down_y, s) for s in (2, 1, 3)]
    down_z = [down_y, down_z[1], down_z[0], down_z[2]]
    held = fetch(memory)
    partner = [other_core(w) for w in by_z]
    own, t1, t2, t3 = project(by_y, by_z, partner)
    came = [along_y(t, -s) for s, t in ((2, t2), (1, t1), (3, t3))]
    down_partner = [other_core(d) for d in down_z]
    gated = read(own, came, gates, head_gain, held)
    part, send, gains = down_project(gated, down_z, down_partner)
    mixed = [along_tp(send, s) for s in (2, 1, 3)]
    weights = fetch_experts(gate_proj, up_proj, expert_down)
    residual, outgoing = dispatch(tokens, part, mixed, gains, send_from)
    arrived = lax.all_to_all(
        outgoing.reshape(ep_count, 8, 1024), "ep", 0, 0, tiled=True
    ).reshape(256, 1024)
    value = run_experts(arrived, weights)
    returned = lax.all_to_all(
        value.reshape(ep_count, 8, 1024), "ep", 0, 0, tiled=True
    ).reshape(256, 1024)
    own_sum, sent = combine(take_with, returned)
    others = [along_tp(sent, s) for s in (2, 1, 3)]
    return finish(own_sum, others, residual, output_gain)


def solution(mesh):
    placed = (
        P("ep", None),
        P(),
        P("ep", "tp"),
        P("ep", "tp"),
        P("ep", "tp"),
        P("ep", "tp"),
        P("tp", None),
        P("tp", None),
        P("ep", "tp", None, None),
        P("ep", "tp"),
        P("tp"),
        P(None, "ep"),
        P("ep"),
        P("ep"),
        P(),
        P(),
        P("ep", None, "tp"),
        P("ep", None, "tp"),
        P("ep", "tp", None),
        P("tp"),
    )
    return jax.shard_map(
        layer, mesh=mesh, in_specs=placed, out_specs=P("ep", "tp"), check_vma=False
    )
```

time: 123 us -> 132 us (1.073)
  starting transfers between devices: 30.8 us -> 52.3 us
  blocking collectives: 33.5 us -> 15.1 us
  local copies, waits for them, and re-layouts: 1.75 us -> 17.4 us
  waiting for transfers between devices: 34.9 us -> 26.2 us
  Pallas kernels: 13.5 us -> 20.2 us
  matrix products: 6.03 us -> 0 us
  other arithmetic: 1.86 us -> 0 us
    all_to_all x2 -> x1, blocking collectives: 33.5 us -> 15.1 us  [layer(): lax.all_to_all(value.reshape(ep_count, 8, 1024), 'ep', 0, 0, tiled=True)]
    unnamed x10 -> x18, local copies, waits for them, and re-layouts: 0.02 us -> 17.4 us
    ppermute x6, waiting for transfers between devices: 15.1 us -> 5.18 us  [along_z(): return lax.ppermute(a, 'ep', ep_moves(s, 0, 0))]
    all_to_all x0 -> x1, starting transfers between devices: none -> 9.93 us  [layer(): lax.all_to_all(outgoing.reshape(ep_count, 8, 1024), 'ep', 0, 0, tiled=True)]
    pallas_call x3 -> x10, Pallas kernels: 4.84 us -> 11 us  [the longest x1 2.89 us: fetch_experts(): pl.pallas_call(fetch_experts_kernel, in_specs=[pl.BlockSpec(memory_space=...]
    dot_general x4 -> x0, matrix products: 6.03 us -> none  [the longest x1 3.29 us: layer(): jnp.dot(activation, expert_down[0], preferred_element_type=F32)]
    all_to_all x0 -> x1, waiting for transfers between devices: none -> 5.83 us  [layer(): lax.all_to_all(outgoing.reshape(ep_count, 8, 1024), 'ep', 0, 0, tiled=True)]
    ppermute x6, starting transfers between devices: 8.28 us -> 13 us  [along_y(): return lax.ppermute(a, 'ep', ep_moves(0, s, 0))]
  transfers between devices with their start and end apart: 26 -> 27, of which waited for: 14 -> 13; matrix products, arithmetic and copies ran while one was open for 0% -> 0% of each run, Pallas kernels for 8% -> 11%
where the time goes in v1:
time: 132 us; the launch traced here: 131 us
  starting transfers between devices  52.3 us (40%)
  waiting for transfers between devices  26.2 us (20%)
  Pallas kernels  20.2 us (15%)
  local copies, waits for them, and re-layouts  17.4 us (13%)
  blocking collectives  15.1 us (11%)
    unnamed x18, local copies, waits for them, and re-layouts  17.4 us
    ppermute x6, starting transfers between devices, along_z(): return lax.ppermute(a, 'ep', ep_moves(s, 0, 0))  16.6 us
    all_to_all x1, blocking collectives, layer(): lax.all_to_all(value.reshape(ep_count, 8, 1024), 'ep', 0, 0, tiled=True)  15.1 us
    ppermute x6, starting transfers between devices, along_y(): return lax.ppermute(a, 'ep', ep_moves(0, s, 0))  13 us
    ppermute x6, starting transfers between devices, along_tp(): return lax.ppermute(a, 'tp', [(i, (i + s) % TP) for i in range(TP)])  11.1 us
    all_to_all x1, starting transfers between devices, layer(): lax.all_to_all(outgoing.reshape(ep_count, 8, 1024), 'ep', 0, 0, tiled=True)  9.93 us
    ppermute x6, waiting for transfers between devices, along_y(): return lax.ppermute(a, 'ep', ep_moves(0, s, 0))  7.84 us
    pallas_call x1, Pallas kernels, fetch(): pl.pallas_call(fetch_kernel, in_specs=[pl.BlockSpec(memory_space=pltpu.HB...  5.94 us
  transfers between devices with their start and end apart: 27, of which 13 were waited for; matrix products, arithmetic and copies ran while one was open for 0% of the time, Pallas kernels for 11%

profile of v1, /device:TPU:0, one launch (start us, length us, event | category | flops | bytes accessed | tf_op | source)
XLA Modules:
  0.0 131.2 jit_solution(16242781928010844209)
XLA Ops:
  0.0 1.0 join.1.w0
  1.0 2.1 %collective-permute-start.3 = (bf16[64,2048]{1,0:T(8,128)(2,1)S(1)}, bf16[64,2048]{1,0:T(8,128)(2,1)S(1)}, u32[]{:S(2)}, u32[]{:S(2)}) collective-permute-start(bf16[64,2048]{1,0:T(8,128)(2,1)S(1)} %join.1.w0), channel_id=1, source_target_pairs={{0,32},{4,36},{8,40},{12,44},{16,48},{20,52},{24,56},{28,60},{32,6... | collective-permute-start | bytes 786440 | tf_op jit(solution)/shard_map/ppermute | solution.py:31
  3.1 1.8 %prepare.1 = (bf16[72,640]{1,0:T(8,128)(2,1)S(1)}, bf16[72,640]{1,0:T(8,128)(2,1)S(1)}, bf16[72,640]{1,0:T(8,128)(2,1)S(1)}, bf16[72,640]{1,0:T(8,128)(2,1)S(1)}) custom-call(bf16[16,2048]{1,0:T(8,128)(2,1)} %x.5, f32[1,2048]{1,0:T(1,128)} %bitcast.19, bf16[64,2048]{1,0:T(8,128)(2,1)} %bitcast.18, f32[1,64]{1,0:T(1,128)} %bitcast.23, f32[1,64]{1,0:T(1,128)} %bitcast.24), custom_call_target="tpu_custom_call" | custom-call | tf_op jit(solution)/shard_map/prepare/pallas_call | solution.py:119
  4.8 1.6 %collective-permute-start = (bf16[72,640]{1,0:T(8,128)(2,1)S(1)}, bf16[72,640]{1,0:T(8,128)(2,1)S(1)}, u32[]{:S(2)}, u32[]{:S(2)}) collective-permute-start(bf16[72,640]{1,0:T(8,128)(2,1)S(1)} %get-tuple-element.28), channel_id=1, source_target_pairs={{0,8},{4,12},{8,16},{12,20},{16,24},{20,28},{24,0},{28,4},{32,40},... | collective-permute-start | bytes 276488 | tf_op jit(solution)/shard_map/ppermute | solution.py:35
  6.5 3.6 %collective-permute-start.4 = (bf16[64,2048]{1,0:T(8,128)(2,1)S(1)}, bf16[64,2048]{1,0:T(8,128)(2,1)S(1)}, u32[]{:S(2)}, u32[]{:S(2)}) collective-permute-start(bf16[64,2048]{1,0:T(8,128)(2,1)S(1)} %join.1.w0), channel_id=1, source_target_pairs={{0,64},{4,68},{8,72},{12,76},{16,80},{20,84},{24,88},{28,92},{32,9... | collective-permute-start | bytes 786440 | tf_op jit(solution)/shard_map/ppermute | solution.py:31
  10.1 1.0 collective-permute-start.5
  11.1 0.0 collective-permute-start.6
  11.1 0.4 collective-permute-done.3.w1
  11.5 0.1 collective-permute-start.7
  11.6 0.0 collective-permute-done.n1.a1
  11.6 3.1 %collective-permute-start.1 = (bf16[72,640]{1,0:T(8,128)(2,1)S(1)}, bf16[72,640]{1,0:T(8,128)(2,1)S(1)}, u32[]{:S(2)}, u32[]{:S(2)}) collective-permute-start(bf16[72,640]{1,0:T(8,128)(2,1)S(1)} %get-tuple-element.29), channel_id=1, source_target_pairs={{0,16},{4,20},{8,24},{12,28},{16,0},{20,4},{24,8},{28,12},{32,48},... | collective-permute-start | bytes 276488 | tf_op jit(solution)/shard_map/ppermute | solution.py:35
  14.7 3.4 %collective-permute-done.1.n2.a2 = bf16[72,640]{1,0:T(8,128)(2,1)S(1)} collective-permute-done((bf16[72,640]{1,0:T(8,128)(2,1)S(1)}, bf16[72,640]{1,0:T(8,128)(2,1)S(1)}, u32[]{:S(2)}, u32[]{:S(2)}) %collective-permute-start.1) | collective-permute-done | bytes 92192 | tf_op jit(solution)/shard_map/ppermute | solution.py:35
  18.1 3.0 %collective-permute-start.2 = (bf16[72,640]{1,0:T(8,128)(2,1)S(1)}, bf16[72,640]{1,0:T(8,128)(2,1)S(1)}, u32[]{:S(2)}, u32[]{:S(2)}) collective-permute-start(bf16[72,640]{1,0:T(8,128)(2,1)S(1)} %get-tuple-element.30), channel_id=1, source_target_pairs={{0,24},{4,28},{8,0},{12,4},{16,8},{20,12},{24,16},{28,20},{32,56},... | collective-permute-start | bytes 276488 | tf_op jit(solution)/shard_map/ppermute | solution.py:35
  21.1 2.2 %collective-permute-done.2.n3.a3 = bf16[72,640]{1,0:T(8,128)(2,1)S(1)} collective-permute-done((bf16[72,640]{1,0:T(8,128)(2,1)S(1)}, bf16[72,640]{1,0:T(8,128)(2,1)S(1)}, u32[]{:S(2)}, u32[]{:S(2)}) %collective-permute-start.2) | collective-permute-done | bytes 92192 | tf_op jit(solution)/shard_map/ppermute | solution.py:35
  23.3 4.8 %collective-permute-start.13 = (bf16[288,512]{1,0:T(8,128)(2,1)S(1)}, bf16[288,512]{1,0:T(8,128)(2,1)S(1)}, u32[]{:S(2)}, u32[]{:S(2)}) collective-permute-start(bf16[288,512]{1,0:T(8,128)(2,1)S(1)} %stack_down.1.d0), channel_id=1, source_target_pairs={{0,32},{4,36},{8,40},{12,44},{16,48},{20,52},{24,56},{28,60},{32,6... | collective-permute-start | bytes 884744 | tf_op jit(solution)/shard_map/ppermute | solution.py:31
  28.1 2.6 %collective-permute-start.14 = (bf16[288,512]{1,0:T(8,128)(2,1)S(1)}, bf16[288,512]{1,0:T(8,128)(2,1)S(1)}, u32[]{:S(2)}, u32[]{:S(2)}) collective-permute-start(bf16[288,512]{1,0:T(8,128)(2,1)S(1)} %stack_down.1.d0), channel_id=1, source_target_pairs={{0,64},{4,68},{8,72},{12,76},{16,80},{20,84},{24,88},{28,92},{32,9... | collective-permute-start | bytes 884744 | tf_op jit(solution)/shard_map/ppermute | solution.py:31
  30.7 2.5 %collective-permute-start.15 = (bf16[288,512]{1,0:T(8,128)(2,1)S(1)}, bf16[288,512]{1,0:T(8,128)(2,1)S(1)}, u32[]{:S(2)}, u32[]{:S(2)}) collective-permute-start(bf16[288,512]{1,0:T(8,128)(2,1)S(1)} %stack_down.1.d0), channel_id=1, source_target_pairs={{0,96},{4,100},{8,104},{12,108},{16,112},{20,116},{24,120},{28,124... | collective-permute-start | bytes 884744 | tf_op jit(solution)/shard_map/ppermute | solution.py:31
  33.2 0.0 collective-permute-done.6.p0
  33.2 0.0 collective-permute-start.8
  33.2 0.0 collective-permute-done.7.p1
  33.2 0.5 collective-permute-start.9
  33.7 1.0 collective-permute-done.8.p2
  34.7 0.4 collective-permute-done.9.p3
  35.1 0.5 project.1
  35.7 1.9 %collective-permute-start.10 = (bf16[16,3072]{1,0:T(8,128)(2,1)S(1)}, bf16[16,3072]{1,0:T(8,128)(2,1)S(1)}, u32[]{:S(2)}, u32[]{:S(2)}) collective-permute-start(bf16[16,3072]{1,0:T(8,128)(2,1)S(1)} %get-tuple-element.32), channel_id=1, source_target_pairs={{0,16},{4,20},{8,24},{12,28},{16,0},{20,4},{24,8},{28,12},{32,48},... | collective-permute-start | bytes 294920 | tf_op jit(solution)/shard_map/ppermute | solution.py:35
  37.6 0.0 collective-permute-start.16
  37.6 0.0 collective-permute-done.13.d1
  37.6 0.5 collective-permute-start.17
  38.1 4.8 %collective-permute-done.14.d2 = bf16[288,512]{1,0:T(8,128)(2,1)S(1)} collective-permute-done((bf16[288,512]{1,0:T(8,128)(2,1)S(1)}, bf16[288,512]{1,0:T(8,128)(2,1)S(1)}, u32[]{:S(2)}, u32[]{:S(2)}) %collective-permute-start.14) | collective-permute-done | bytes 294944 | tf_op jit(solution)/shard_map/ppermute | solution.py:31
  42.8 0.0 collective-permute-done.15.d3
  42.8 0.5 collective-permute-start.19
  43.4 0.0 collective-permute-done.10.r1
  43.4 3.3 %collective-permute-start.11 = (bf16[16,3072]{1,0:T(8,128)(2,1)S(1)}, bf16[16,3072]{1,0:T(8,128)(2,1)S(1)}, u32[]{:S(2)}, u32[]{:S(2)}) collective-permute-start(bf16[16,3072]{1,0:T(8,128)(2,1)S(1)} %get-tuple-element.33), channel_id=1, source_target_pairs={{0,24},{4,28},{8,0},{12,4},{16,8},{20,12},{24,16},{28,20},{32,56},... | collective-permute-start | bytes 294920 | tf_op jit(solution)/shard_map/ppermute | solution.py:35
  46.7 2.3 %collective-permute-done.11.r2 = bf16[16,3072]{1,0:T(8,128)(2,1)S(1)} collective-permute-done((bf16[16,3072]{1,0:T(8,128)(2,1)S(1)}, bf16[16,3072]{1,0:T(8,128)(2,1)S(1)}, u32[]{:S(2)}, u32[]{:S(2)}) %collective-permute-start.11) | collective-permute-done | bytes 98336 | tf_op jit(solution)/shard_map/ppermute | solution.py:35
  49.0 5.9 %fetch.1.mem = f32[16,1,512,512]{3,2,1,0:T(8,128)S(1)} custom-call(f32[16,1,512,512]{3,2,1,0:T(8,128)} %memory.1), custom_call_target="tpu_custom_call" | custom-call | tf_op jit(solution)/shard_map/fetch/pallas_call | solution.py:265
  54.9 5.7 %copy-done = f32[16,1,512,512]{3,2,1,0:T(8,128)} copy-done((f32[16,1,512,512]{3,2,1,0:T(8,128)}, f32[16,1,512,512]{3,2,1,0:T(8,128)S(1)}, u32[]{:S(2)}) %copy-start) | copy-done | bytes 16777240
  60.7 1.4 %route.1 = (f32[16,128]{1,0:T(8,128)S(1)}, bf16[32,256]{1,0:T(8,128)(2,1)S(1)}, bf16[96,256]{1,0:T(8,128)(2,1)S(1)}) custom-call(bf16[16,2048]{1,0:T(8,128)(2,1)} %x.5, f32[1,2048]{1,0:T(1,128)} %bitcast.20, bf16[1,2048]{1,0:T(2,128)(2,1)} %ig.1, bf16[1,2048]{1,0:T(2,128)(2,1)} %fg.1, f32[1,16]{1,0:T(1,128)} %bitcast.25, s32[4,512]{1,0:T(4,128)} %bitcast.21, ...), custom_call_target="tpu_custom_call" | custom-call | tf_op jit(solution)/shard_map/route/pallas_call | solution.py:180
  62.1 5.8 %copy-done.1 = f32[16,1,512,512]{3,2,1,0:T(8,128)S(1)} copy-done((f32[16,1,512,512]{3,2,1,0:T(8,128)S(1)}, f32[16,1,512,512]{3,2,1,0:T(8,128)}, u32[]{:S(2)}) %copy-start.1) | copy-done | bytes 16777240
  67.8 2.2 %read.1.g = bf16[16,512]{1,0:T(8,128)(2,1)S(1)} custom-call(f32[16,2048]{1,0:T(8,128)S(1)} %get-tuple-element.31.own, bf16[16,3072]{1,0:T(8,128)(2,1)S(1)} %collective-permute-done.10.r1, bf16[16,3072]{1,0:T(8,128)(2,1)S(1)} %collective-permute-done.11.r2, bf16[16,3072]{1,0:T(8,128)(2,1)S(1)} %collective-permute-done.12.r3, ...), custom_call_target="tpu_custom_call" | custom-call | tf_op jit(solution)/shard_map/read/pallas_call | solution.py:311
  70.1 0.0 copy-start.6
  70.1 0.7 down_project.1
  70.8 3.1 %collective-permute-start.20 = (bf16[16,2048]{1,0:T(8,128)(2,1)S(1)}, bf16[16,2048]{1,0:T(8,128)(2,1)S(1)}, u32[]{:S(2)}, u32[]{:S(2)}) collective-permute-start(bf16[16,2048]{1,0:T(8,128)(2,1)S(1)} %get-tuple-element.37), channel_id=1, source_target_pairs={{0,2},{1,3},{2,0},{3,1},{4,6},{5,7},{6,4},{7,5},{8,10},{9,11},{10,... | collective-permute-start | bytes 196616 | tf_op jit(solution)/shard_map/ppermute | solution.py:43
  73.9 0.6 collective-permute-start.21
  74.5 2.6 %collective-permute-start.22 = (bf16[16,2048]{1,0:T(8,128)(2,1)S(1)}, bf16[16,2048]{1,0:T(8,128)(2,1)S(1)}, u32[]{:S(2)}, u32[]{:S(2)}) collective-permute-start(bf16[16,2048]{1,0:T(8,128)(2,1)S(1)} %get-tuple-element.37), channel_id=1, source_target_pairs={{0,3},{1,0},{2,1},{3,2},{4,7},{5,4},{6,5},{7,6},{8,11},{9,8},{10,9... | collective-permute-start | bytes 196616 | tf_op jit(solution)/shard_map/ppermute | solution.py:43
  77.2 0.3 collective-permute-done.20.r1
  77.5 1.9 %collective-permute-done.21.r2 = bf16[16,2048]{1,0:T(8,128)(2,1)S(1)} collective-permute-done((bf16[16,2048]{1,0:T(8,128)(2,1)S(1)}, bf16[16,2048]{1,0:T(8,128)(2,1)S(1)}, u32[]{:S(2)}, u32[]{:S(2)}) %collective-permute-start.21) | collective-permute-done | bytes 65568 | tf_op jit(solution)/shard_map/ppermute | solution.py:43
  79.4 1.3 dispatch.1
  80.7 9.9 %all-to-all-start = ((bf16[32,8,1024]{2,1,0:T(8,128)(2,1)}), bf16[32,8,1024]{2,1,0:T(8,128)(2,1)S(1)}, u32[]{:S(2)}, u32[]{:S(2)}) async-start(bf16[32,8,1024]{2,1,0:T(8,128)(2,1)} %bitcast.8), calls=%async_computation | async-start | bytes 1048576 | tf_op jit(solution)/shard_map/all_to_all | solution.py:543
  90.7 2.9 %fetch_experts.1 = (bf16[2048,512]{1,0:T(8,128)(2,1)S(1)}, bf16[2048,512]{1,0:T(8,128)(2,1)S(1)}, bf16[512,2048]{1,0:T(8,128)(2,1)S(1)}) custom-call(bf16[1,2048,512]{2,1,0:T(8,128)(2,1)} %g.1, bf16[1,2048,512]{2,1,0:T(8,128)(2,1)} %u.1, bf16[1,512,2048]{2,1,0:T(8,128)(2,1)} %d.1), custom_call_target="tpu_custom_call" | custom-call | tf_op jit(solution)/shard_map/fetch_experts/pallas_call | solution.py:380
  93.6 1.4 %copy-done.2 = bf16[2048,512]{1,0:T(8,128)(2,1)} copy-done((bf16[2048,512]{1,0:T(8,128)(2,1)}, bf16[2048,512]{1,0:T(8,128)(2,1)S(1)}, u32[]{:S(2)}) %copy-start.2) | copy-done | bytes 2097176
  94.9 1.3 %copy-done.4 = bf16[512,2048]{1,0:T(8,128)(2,1)} copy-done((bf16[512,2048]{1,0:T(8,128)(2,1)}, bf16[512,2048]{1,0:T(8,128)(2,1)S(1)}, u32[]{:S(2)}) %copy-start.4) | copy-done | bytes 2097176
  96.3 5.8 %all-to-all-done = bf16[32,8,1024]{2,1,0:T(8,128)(2,1)S(1)} async-done(((bf16[32,8,1024]{2,1,0:T(8,128)(2,1)}), bf16[32,8,1024]{2,1,0:T(8,128)(2,1)S(1)}, u32[]{:S(2)}, u32[]{:S(2)}) %all-to-all-start) | async-done | bytes 524320 | tf_op jit(solution)/shard_map/all_to_all | solution.py:543
  102.1 1.6 %copy-done.3 = bf16[2048,512]{1,0:T(8,128)(2,1)S(1)} copy-done((bf16[2048,512]{1,0:T(8,128)(2,1)S(1)}, bf16[2048,512]{1,0:T(8,128)(2,1)}, u32[]{:S(2)}) %copy-start.3) | copy-done | bytes 2097176
  103.7 1.6 %copy-done.5 = bf16[512,2048]{1,0:T(8,128)(2,1)S(1)} copy-done((bf16[512,2048]{1,0:T(8,128)(2,1)S(1)}, bf16[512,2048]{1,0:T(8,128)(2,1)}, u32[]{:S(2)}) %copy-start.5) | copy-done | bytes 2097176
  105.3 1.5 %experts.1 = bf16[256,1024]{1,0:T(8,128)(2,1)S(1)} custom-call(bf16[256,1024]{1,0:T(8,128)(2,1)S(1)} %bitcast.13, bf16[2048,512]{1,0:T(8,128)(2,1)S(1)} %get-tuple-element.41.gate_w, bf16[2048,512]{1,0:T(8,128)(2,1)S(1)} %copy-done.3, bf16[512,2048]{1,0:T(8,128)(2,1)S(1)} %copy-done.5), custom_call_target="tpu_custom_call" | custom-call | tf_op jit(solution)/shard_map/experts/pallas_call | solution.py:445
  106.8 15.1 %all_to_all.10 = bf16[32,8,1024]{2,1,0:T(8,128)(2,1)S(1)} all-to-all(bf16[32,8,1024]{2,1,0:T(8,128)(2,1)S(1)} %bitcast.14), channel_id=1, replica_groups=mesh['ep'=32,'tp'=4] {'ep'}, dimensions={0} | all-to-all | bytes 1048576 | tf_op jit(solution)/shard_map/all_to_all | solution.py:547
  121.8 0.2 combine.1
  122.0 1.5 %collective-permute-start.23 = (bf16[16,2048]{1,0:T(8,128)(2,1)S(1)}, bf16[16,2048]{1,0:T(8,128)(2,1)S(1)}, u32[]{:S(2)}, u32[]{:S(2)}) collective-permute-start(bf16[16,2048]{1,0:T(8,128)(2,1)S(1)} %get-tuple-element.45), channel_id=1, source_target_pairs={{0,2},{1,3},{2,0},{3,1},{4,6},{5,7},{6,4},{7,5},{8,10},{9,11},{10,... | collective-permute-start | bytes 196616 | tf_op jit(solution)/shard_map/ppermute | solution.py:43
  123.6 2.6 %collective-permute-start.24 = (bf16[16,2048]{1,0:T(8,128)(2,1)S(1)}, bf16[16,2048]{1,0:T(8,128)(2,1)S(1)}, u32[]{:S(2)}, u32[]{:S(2)}) collective-permute-start(bf16[16,2048]{1,0:T(8,128)(2,1)S(1)} %get-tuple-element.45), channel_id=1, source_target_pairs={{0,1},{1,2},{2,3},{3,0},{4,5},{5,6},{6,7},{7,4},{8,9},{9,10},{10,1... | collective-permute-start | bytes 196616 | tf_op jit(solution)/shard_map/ppermute | solution.py:43
  126.2 0.6 collective-permute-start.25
  126.8 1.4 %collective-permute-done.23.r1 = bf16[16,2048]{1,0:T(8,128)(2,1)S(1)} collective-permute-done((bf16[16,2048]{1,0:T(8,128)(2,1)S(1)}, bf16[16,2048]{1,0:T(8,128)(2,1)S(1)}, u32[]{:S(2)}, u32[]{:S(2)}) %collective-permute-start.23) | collective-permute-done | bytes 65568 | tf_op jit(solution)/shard_map/ppermute | solution.py:43
  128.2 1.1 collective-permute-done.24.r2
  129.3 1.2 collective-permute-done.25.r3
  130.5 0.7 finish.1
  (22 shorter events, 0.1 us)
Async XLA Ops:
  1.0 10.5 %collective-permute-start.3 = (bf16[64,2048]{1,0:T(8,128)(2,1)S(1)}, bf16[64,2048]{1,0:T(8,128)(2,1)S(1)}, u32[]{:S(2)}, u32[]{:S(2)}) collective-permute-start(bf16[64,2048]{1,0:T(8,128)(2,1)S(1)} %join.1.w0), channel_id=1, source_target_pairs={{0,32},{4,36},{8,40},{12,44},{16,48},{20,52},{24,56},{28,60},{32,6... | collective-permute-start | bytes 786440 | tf_op jit(solution)/shard_map/ppermute | solution.py:31
  4.8 6.8 %collective-permute-start = (bf16[72,640]{1,0:T(8,128)(2,1)S(1)}, bf16[72,640]{1,0:T(8,128)(2,1)S(1)}, u32[]{:S(2)}, u32[]{:S(2)}) collective-permute-start(bf16[72,640]{1,0:T(8,128)(2,1)S(1)} %get-tuple-element.28), channel_id=1, source_target_pairs={{0,8},{4,12},{8,16},{12,20},{16,24},{20,28},{24,0},{28,4},{32,40},... | collective-permute-start | bytes 276488 | tf_op jit(solution)/shard_map/ppermute | solution.py:35
  6.5 21.6 %collective-permute-start.4 = (bf16[64,2048]{1,0:T(8,128)(2,1)S(1)}, bf16[64,2048]{1,0:T(8,128)(2,1)S(1)}, u32[]{:S(2)}, u32[]{:S(2)}) collective-permute-start(bf16[64,2048]{1,0:T(8,128)(2,1)S(1)} %join.1.w0), channel_id=1, source_target_pairs={{0,64},{4,68},{8,72},{12,76},{16,80},{20,84},{24,88},{28,92},{32,9... | collective-permute-start | bytes 786440 | tf_op jit(solution)/shard_map/ppermute | solution.py:31
  10.1 20.6 %collective-permute-start.5 = (bf16[64,2048]{1,0:T(8,128)(2,1)S(1)}, bf16[64,2048]{1,0:T(8,128)(2,1)S(1)}, u32[]{:S(2)}, u32[]{:S(2)}) collective-permute-start(bf16[64,2048]{1,0:T(8,128)(2,1)S(1)} %join.1.w0), channel_id=1, source_target_pairs={{0,96},{4,100},{8,104},{12,108},{16,112},{20,116},{24,120},{28,124... | collective-permute-start | bytes 786440 | tf_op jit(solution)/shard_map/ppermute | solution.py:31
  11.1 22.1 %collective-permute-start.6 = (bf16[64,2048]{1,0:T(8,128)(2,1)S(1)}, bf16[64,2048]{1,0:T(8,128)(2,1)S(1)}, u32[]{:S(2)}, u32[]{:S(2)}) collective-permute-start(bf16[64,2048]{1,0:T(8,128)(2,1)S(1)} %join.1.w0), channel_id=1, source_target_pairs={{0,4},{4,0},{8,12},{12,8},{16,20},{20,16},{24,28},{28,24},{32,36},... | collective-permute-start | bytes 786440 | tf_op jit(solution)/shard_map/ppermute | solution.py:39
  11.5 21.7 %collective-permute-start.7 = (bf16[64,2048]{1,0:T(8,128)(2,1)S(1)}, bf16[64,2048]{1,0:T(8,128)(2,1)S(1)}, u32[]{:S(2)}, u32[]{:S(2)}) collective-permute-start(bf16[64,2048]{1,0:T(8,128)(2,1)S(1)} %collective-permute-done.3.w1), channel_id=1, source_target_pairs={{0,4},{4,0},{8,12},{12,8},{16,20},{20,16},{24,28},{28,24},{32,36},... | collective-permute-start | bytes 786440 | tf_op jit(solution)/shard_map/ppermute | solution.py:39
  11.6 6.5 %collective-permute-start.1 = (bf16[72,640]{1,0:T(8,128)(2,1)S(1)}, bf16[72,640]{1,0:T(8,128)(2,1)S(1)}, u32[]{:S(2)}, u32[]{:S(2)}) collective-permute-start(bf16[72,640]{1,0:T(8,128)(2,1)S(1)} %get-tuple-element.29), channel_id=1, source_target_pairs={{0,16},{4,20},{8,24},{12,28},{16,0},{20,4},{24,8},{28,12},{32,48},... | collective-permute-start | bytes 276488 | tf_op jit(solution)/shard_map/ppermute | solution.py:35
  18.1 5.2 %collective-permute-start.2 = (bf16[72,640]{1,0:T(8,128)(2,1)S(1)}, bf16[72,640]{1,0:T(8,128)(2,1)S(1)}, u32[]{:S(2)}, u32[]{:S(2)}) collective-permute-start(bf16[72,640]{1,0:T(8,128)(2,1)S(1)} %get-tuple-element.30), channel_id=1, source_target_pairs={{0,24},{4,28},{8,0},{12,4},{16,8},{20,12},{24,16},{28,20},{32,56},... | collective-permute-start | bytes 276488 | tf_op jit(solution)/shard_map/ppermute | solution.py:35
  23.3 14.3 %collective-permute-start.13 = (bf16[288,512]{1,0:T(8,128)(2,1)S(1)}, bf16[288,512]{1,0:T(8,128)(2,1)S(1)}, u32[]{:S(2)}, u32[]{:S(2)}) collective-permute-start(bf16[288,512]{1,0:T(8,128)(2,1)S(1)} %stack_down.1.d0), channel_id=1, source_target_pairs={{0,32},{4,36},{8,40},{12,44},{16,48},{20,52},{24,56},{28,60},{32,6... | collective-permute-start | bytes 884744 | tf_op jit(solution)/shard_map/ppermute | solution.py:31
  28.1 14.8 %collective-permute-start.14 = (bf16[288,512]{1,0:T(8,128)(2,1)S(1)}, bf16[288,512]{1,0:T(8,128)(2,1)S(1)}, u32[]{:S(2)}, u32[]{:S(2)}) collective-permute-start(bf16[288,512]{1,0:T(8,128)(2,1)S(1)} %stack_down.1.d0), channel_id=1, source_target_pairs={{0,64},{4,68},{8,72},{12,76},{16,80},{20,84},{24,88},{28,92},{32,9... | collective-permute-start | bytes 884744 | tf_op jit(solution)/shard_map/ppermute | solution.py:31
  30.7 12.2 %collective-permute-start.15 = (bf16[288,512]{1,0:T(8,128)(2,1)S(1)}, bf16[288,512]{1,0:T(8,128)(2,1)S(1)}, u32[]{:S(2)}, u32[]{:S(2)}) collective-permute-start(bf16[288,512]{1,0:T(8,128)(2,1)S(1)} %stack_down.1.d0), channel_id=1, source_target_pairs={{0,96},{4,100},{8,104},{12,108},{16,112},{20,116},{24,120},{28,124... | collective-permute-start | bytes 884744 | tf_op jit(solution)/shard_map/ppermute | solution.py:31
  33.2 1.5 %collective-permute-start.8 = (bf16[64,2048]{1,0:T(8,128)(2,1)S(1)}, bf16[64,2048]{1,0:T(8,128)(2,1)S(1)}, u32[]{:S(2)}, u32[]{:S(2)}) collective-permute-start(bf16[64,2048]{1,0:T(8,128)(2,1)S(1)} %collective-permute-done.4.w2), channel_id=1, source_target_pairs={{0,4},{4,0},{8,12},{12,8},{16,20},{20,16},{24,28},{28,24},{32,36},... | collective-permute-start | bytes 786440 | tf_op jit(solution)/shard_map/ppermute | solution.py:39
  33.2 1.9 %collective-permute-start.9 = (bf16[64,2048]{1,0:T(8,128)(2,1)S(1)}, bf16[64,2048]{1,0:T(8,128)(2,1)S(1)}, u32[]{:S(2)}, u32[]{:S(2)}) collective-permute-start(bf16[64,2048]{1,0:T(8,128)(2,1)S(1)} %collective-permute-done.5.w3), channel_id=1, source_target_pairs={{0,4},{4,0},{8,12},{12,8},{16,20},{20,16},{24,28},{28,24},{32,36},... | collective-permute-start | bytes 786440 | tf_op jit(solution)/shard_map/ppermute | solution.py:39
  35.7 7.7 %collective-permute-start.10 = (bf16[16,3072]{1,0:T(8,128)(2,1)S(1)}, bf16[16,3072]{1,0:T(8,128)(2,1)S(1)}, u32[]{:S(2)}, u32[]{:S(2)}) collective-permute-start(bf16[16,3072]{1,0:T(8,128)(2,1)S(1)} %get-tuple-element.32), channel_id=1, source_target_pairs={{0,16},{4,20},{8,24},{12,28},{16,0},{20,4},{24,8},{28,12},{32,48},... | collective-permute-start | bytes 294920 | tf_op jit(solution)/shard_map/ppermute | solution.py:35
  37.6 32.5 %collective-permute-start.16 = (bf16[288,512]{1,0:T(8,128)(2,1)S(1)}, bf16[288,512]{1,0:T(8,128)(2,1)S(1)}, u32[]{:S(2)}, u32[]{:S(2)}) collective-permute-start(bf16[288,512]{1,0:T(8,128)(2,1)S(1)} %stack_down.1.d0), channel_id=1, source_target_pairs={{0,4},{4,0},{8,12},{12,8},{16,20},{20,16},{24,28},{28,24},{32,36},... | collective-permute-start | bytes 884744 | tf_op jit(solution)/shard_map/ppermute | solution.py:39
  37.6 32.5 %collective-permute-start.17 = (bf16[288,512]{1,0:T(8,128)(2,1)S(1)}, bf16[288,512]{1,0:T(8,128)(2,1)S(1)}, u32[]{:S(2)}, u32[]{:S(2)}) collective-permute-start(bf16[288,512]{1,0:T(8,128)(2,1)S(1)} %collective-permute-done.13.d1), channel_id=1, source_target_pairs={{0,4},{4,0},{8,12},{12,8},{16,20},{20,16},{24,28},{28,24},{32,36},... | collective-permute-start | bytes 884744 | tf_op jit(solution)/shard_map/ppermute | solution.py:39
  42.8 27.3 %collective-permute-start.18 = (bf16[288,512]{1,0:T(8,128)(2,1)S(1)}, bf16[288,512]{1,0:T(8,128)(2,1)S(1)}, u32[]{:S(2)}, u32[]{:S(2)}) collective-permute-start(bf16[288,512]{1,0:T(8,128)(2,1)S(1)} %collective-permute-done.14.d2), channel_id=1, source_target_pairs={{0,4},{4,0},{8,12},{12,8},{16,20},{20,16},{24,28},{28,24},{32,36},... | collective-permute-start | bytes 884744 | tf_op jit(solution)/shard_map/ppermute | solution.py:39
  42.8 27.3 %collective-permute-start.19 = (bf16[288,512]{1,0:T(8,128)(2,1)S(1)}, bf16[288,512]{1,0:T(8,128)(2,1)S(1)}, u32[]{:S(2)}, u32[]{:S(2)}) collective-permute-start(bf16[288,512]{1,0:T(8,128)(2,1)S(1)} %collective-permute-done.15.d3), channel_id=1, source_target_pairs={{0,4},{4,0},{8,12},{12,8},{16,20},{20,16},{24,28},{28,24},{32,36},... | collective-permute-start | bytes 884744 | tf_op jit(solution)/shard_map/ppermute | solution.py:39
  43.4 5.6 %collective-permute-start.11 = (bf16[16,3072]{1,0:T(8,128)(2,1)S(1)}, bf16[16,3072]{1,0:T(8,128)(2,1)S(1)}, u32[]{:S(2)}, u32[]{:S(2)}) collective-permute-start(bf16[16,3072]{1,0:T(8,128)(2,1)S(1)} %get-tuple-element.33), channel_id=1, source_target_pairs={{0,24},{4,28},{8,0},{12,4},{16,8},{20,12},{24,16},{28,20},{32,56},... | collective-permute-start | bytes 294920 | tf_op jit(solution)/shard_map/ppermute | solution.py:35
  49.0 13.1 %copy-start.7 = (f32[512]{0:T(512)S(1)}, f32[512]{0:T(512)}, u32[]{:S(2)}) copy-start(f32[512]{0:T(512)} %param.30) | copy-start | bytes 6148
  49.0 13.1 %collective-permute-start.12 = (bf16[16,3072]{1,0:T(8,128)(2,1)S(1)}, bf16[16,3072]{1,0:T(8,128)(2,1)S(1)}, u32[]{:S(2)}, u32[]{:S(2)}) collective-permute-start(bf16[16,3072]{1,0:T(8,128)(2,1)S(1)} %get-tuple-element.34), channel_id=1, source_target_pairs={{0,8},{4,12},{8,16},{12,20},{16,24},{20,28},{24,0},{28,4},{32,40},... | collective-permute-start | bytes 294920 | tf_op jit(solution)/shard_map/ppermute | solution.py:35
  54.9 5.7 %copy-start = (f32[16,1,512,512]{3,2,1,0:T(8,128)}, f32[16,1,512,512]{3,2,1,0:T(8,128)S(1)}, u32[]{:S(2)}) copy-start(f32[16,1,512,512]{3,2,1,0:T(8,128)S(1)} %fetch.1.mem) | copy-start | bytes 50331652
  62.1 5.8 %copy-start.1 = (f32[16,1,512,512]{3,2,1,0:T(8,128)S(1)}, f32[16,1,512,512]{3,2,1,0:T(8,128)}, u32[]{:S(2)}) copy-start(f32[16,1,512,512]{3,2,1,0:T(8,128)} %copy-done) | copy-start | bytes 50331652
  70.1 9.4 %copy-start.6 = (bf16[16,2048]{1,0:T(8,128)(2,1)S(1)}, bf16[16,2048]{1,0:T(8,128)(2,1)}, u32[]{:S(2)}) copy-start(bf16[16,2048]{1,0:T(8,128)(2,1)} %x.5) | copy-start | bytes 196612
  70.8 6.6 %collective-permute-start.20 = (bf16[16,2048]{1,0:T(8,128)(2,1)S(1)}, bf16[16,2048]{1,0:T(8,128)(2,1)S(1)}, u32[]{:S(2)}, u32[]{:S(2)}) collective-permute-start(bf16[16,2048]{1,0:T(8,128)(2,1)S(1)} %get-tuple-element.37), channel_id=1, source_target_pairs={{0,2},{1,3},{2,0},{3,1},{4,6},{5,7},{6,4},{7,5},{8,10},{9,11},{10,... | collective-permute-start | bytes 196616 | tf_op jit(solution)/shard_map/ppermute | solution.py:43
  73.9 5.5 %collective-permute-start.21 = (bf16[16,2048]{1,0:T(8,128)(2,1)S(1)}, bf16[16,2048]{1,0:T(8,128)(2,1)S(1)}, u32[]{:S(2)}, u32[]{:S(2)}) collective-permute-start(bf16[16,2048]{1,0:T(8,128)(2,1)S(1)} %get-tuple-element.37), channel_id=1, source_target_pairs={{0,1},{1,2},{2,3},{3,0},{4,5},{5,6},{6,7},{7,4},{8,9},{9,10},{10,1... | collective-permute-start | bytes 196616 | tf_op jit(solution)/shard_map/ppermute | solution.py:43
  74.5 4.9 %collective-permute-start.22 = (bf16[16,2048]{1,0:T(8,128)(2,1)S(1)}, bf16[16,2048]{1,0:T(8,128)(2,1)S(1)}, u32[]{:S(2)}, u32[]{:S(2)}) collective-permute-start(bf16[16,2048]{1,0:T(8,128)(2,1)S(1)} %get-tuple-element.37), channel_id=1, source_target_pairs={{0,3},{1,0},{2,1},{3,2},{4,7},{5,4},{6,5},{7,6},{8,11},{9,8},{10,9... | collective-permute-start | bytes 196616 | tf_op jit(solution)/shard_map/ppermute | solution.py:43
  80.7 21.4 %all-to-all-start = ((bf16[32,8,1024]{2,1,0:T(8,128)(2,1)}), bf16[32,8,1024]{2,1,0:T(8,128)(2,1)S(1)}, u32[]{:S(2)}, u32[]{:S(2)}) async-start(bf16[32,8,1024]{2,1,0:T(8,128)(2,1)} %bitcast.8), calls=%async_computation | async-start | bytes 1048576 | tf_op jit(solution)/shard_map/all_to_all | solution.py:543
  93.6 1.4 %copy-start.2 = (bf16[2048,512]{1,0:T(8,128)(2,1)}, bf16[2048,512]{1,0:T(8,128)(2,1)S(1)}, u32[]{:S(2)}) copy-start(bf16[2048,512]{1,0:T(8,128)(2,1)S(1)} %get-tuple-element.42.up_w) | copy-start | bytes 6291460
  94.9 1.3 %copy-start.4 = (bf16[512,2048]{1,0:T(8,128)(2,1)}, bf16[512,2048]{1,0:T(8,128)(2,1)S(1)}, u32[]{:S(2)}) copy-start(bf16[512,2048]{1,0:T(8,128)(2,1)S(1)} %get-tuple-element.43.down_w) | copy-start | bytes 6291460
  102.1 1.6 %copy-start.3 = (bf16[2048,512]{1,0:T(8,128)(2,1)S(1)}, bf16[2048,512]{1,0:T(8,128)(2,1)}, u32[]{:S(2)}) copy-start(bf16[2048,512]{1,0:T(8,128)(2,1)} %copy-done.2) | copy-start | bytes 6291460
  103.7 1.6 %copy-start.5 = (bf16[512,2048]{1,0:T(8,128)(2,1)S(1)}, bf16[512,2048]{1,0:T(8,128)(2,1)}, u32[]{:S(2)}) copy-start(bf16[512,2048]{1,0:T(8,128)(2,1)} %copy-done.4) | copy-start | bytes 6291460
  105.3 25.2 %copy-start.8 = (f32[512]{0:T(512)S(1)}, f32[512]{0:T(512)}, u32[]{:S(2)}) copy-start(f32[512]{0:T(512)} %param.39) | copy-start | bytes 6148
  122.0 6.2 %collective-permute-start.23 = (bf16[16,2048]{1,0:T(8,128)(2,1)S(1)}, bf16[16,2048]{1,0:T(8,128)(2,1)S(1)}, u32[]{:S(2)}, u32[]{:S(2)}) collective-permute-start(bf16[16,2048]{1,0:T(8,128)(2,1)S(1)} %get-tuple-element.45), channel_id=1, source_target_pairs={{0,2},{1,3},{2,0},{3,1},{4,6},{5,7},{6,4},{7,5},{8,10},{9,11},{10,... | collective-permute-start | bytes 196616 | tf_op jit(solution)/shard_map/ppermute | solution.py:43
  123.6 5.7 %collective-permute-start.24 = (bf16[16,2048]{1,0:T(8,128)(2,1)S(1)}, bf16[16,2048]{1,0:T(8,128)(2,1)S(1)}, u32[]{:S(2)}, u32[]{:S(2)}) collective-permute-start(bf16[16,2048]{1,0:T(8,128)(2,1)S(1)} %get-tuple-element.45), channel_id=1, source_target_pairs={{0,1},{1,2},{2,3},{3,0},{4,5},{5,6},{6,7},{7,4},{8,9},{9,10},{10,1... | collective-permute-start | bytes 196616 | tf_op jit(solution)/shard_map/ppermute | solution.py:43
  126.2 4.3 %collective-permute-start.25 = (bf16[16,2048]{1,0:T(8,128)(2,1)S(1)}, bf16[16,2048]{1,0:T(8,128)(2,1)S(1)}, u32[]{:S(2)}, u32[]{:S(2)}) collective-permute-start(bf16[16,2048]{1,0:T(8,128)(2,1)S(1)} %get-tuple-element.45), channel_id=1, source_target_pairs={{0,3},{1,0},{2,1},{3,2},{4,7},{5,4},{6,5},{7,6},{8,11},{9,8},{10,9... | collective-permute-start | bytes 196616 | tf_op jit(solution)/shard_map/ppermute | solution.py:43

commit v2 on v1

--- a/solution.py
+++ b/solution.py
@@ -12,6 +12,7 @@
 BF = jnp.bfloat16
 F32 = jnp.float32
 Z, Y, C, TP = 4, 4, 2, 4
+EARLY, HELD = 4, 12
 
 
 def ep_at(z, y, c):
@@ -33,6 +34,16 @@
 
 def along_y(a, s):
     return lax.ppermute(a, "ep", ep_moves(0, s, 0))
+
+
+def spread(send, order):
+    came = {}
+    for s in order:
+        came[s] = send(s)
+    return [came[s] for s in (1, 2, 3)]
+
+
+NEAR_FIRST, FAR_FIRST = (1, 3, 2), (2, 1, 3)
 
 
 def other_core(a):
@@ -92,46 +103,27 @@
 TURNED = (((1,), (1,)), ((), ()))
 
 
-def prepare_kernel(x, gain, dw, mg, eg, out0, out1, out2, out3, normed, down, sem):
+def prepare_kernel(
+    x_in, gain_in, dw, mg_in, eg_in, ig_in, fg_in, stab_in, memory,
+    out0, out1, out2, out3, gates, early,
+    x, gain, mg, eg, ig, fg, stab, normed, down, sems, row_sems,
+):
     y = (lax.axis_index("ep") // C) & 3
     col = pl.multiple_of(lax.axis_index("tp") * 512, 128)
-    load = pltpu.make_async_copy(dw.at[:, pl.ds(col, 512)], down, sem)
-    load.start()
+    pairs = (
+        (x_in, x), (gain_in, gain), (mg_in, mg), (eg_in, eg), (ig_in, ig), (fg_in, fg),
+        (stab_in, stab), (dw.at[:, pl.ds(col, 512)], down),
+    )
+    loads = [pltpu.make_async_copy(a, b, sems.at[i]) for i, (a, b) in enumerate(pairs)]
+    rows = [
+        pltpu.make_async_copy(memory.at[i], early.at[i], row_sems.at[i]) for i in range(EARLY)
+    ]
+    for load in loads + rows:
+        load.start()
+    for load in loads:
+        load.wait()
     normed[...] = normed_of(x, gain)
-    row = lax.broadcasted_iota(jnp.int32, (8, 64), 0)
-    extra = jnp.zeros((8, 64), F32)
-    for i, g in enumerate((mg, eg)):
-        for j, piece in enumerate(split_in_three(g[...])):
-            extra = jnp.where(row == 3 * i + j, piece, extra)
-    extra = jnp.concatenate([extra, jnp.zeros((8, 576), F32)], axis=1).astype(BF)
-    load.wait()
-    for s, out in enumerate((out0, out1, out2, out3)):
-        out[0:64, 0:512] = down[...]
-        out[64:72] = extra
-        target = (y + s) & 3
-        for i in range(Z):
-            off = pl.multiple_of(512 * i + target * 128, 128)
-            out[16 * i : 16 * i + 16, 512:640] = normed[:, pl.ds(off, 128)]
-
-
-def prepare(tokens, mixer_gain, down_weight, mg, eg):
-    vmem = pl.BlockSpec(memory_space=pltpu.VMEM)
-    return pl.pallas_call(
-        prepare_kernel,
-        in_specs=[vmem, vmem, pl.BlockSpec(memory_space=pl.ANY), vmem, vmem],
-        out_specs=[vmem] * 4,
-        out_shape=[pltpu.VMEM((72, 640), BF)] * 4,
-        scratch_shapes=[
-            pltpu.VMEM((16, 2048), BF),
-            pltpu.VMEM((64, 512), BF),
-            pltpu.SemaphoreType.DMA,
-        ],
-        name="prepare",
-    )(tokens, mixer_gain[None], down_weight.T, mg[None], eg[None])
-
-
-def route_kernel(x, gain, ig, fg, stab, routes, weights, gates, send, take):
-    nf = normed_of(x, gain).astype(F32)
+    nf = normed[...].astype(F32)
     log_input = jnp.sum(nf * ig[...].astype(F32), axis=1, keepdims=True)
     pre = jnp.sum(nf * fg[...].astype(F32), axis=1, keepdims=True)
     log_forget = jnp.minimum(pre, 0.0) - jnp.log1p(jnp.exp(-jnp.abs(pre)))
@@ -140,6 +132,48 @@
     stab_column = jnp.sum(jnp.where(small == across, stab[...], 0.0), axis=1, keepdims=True)
     first = lax.broadcasted_iota(jnp.int32, (16, 128), 1)
     gates[...] = jnp.where(first == 0, log_input, log_forget + stab_column)
+    row = lax.broadcasted_iota(jnp.int32, (8, 64), 0)
+    extra = jnp.zeros((8, 64), F32)
+    for i, g in enumerate((mg, eg)):
+        for j, piece in enumerate(split_in_three(g[...])):
+            extra = jnp.where(row == 3 * i + j, piece, extra)
+    extra = jnp.concatenate([extra, jnp.zeros((8, 576), F32)], axis=1).astype(BF)
+    for s, out in enumerate((out0, out1, out2, out3)):
+        out[0:64, 0:512] = down[...]
+        out[64:72] = extra
+        target = (y + s) & 3
+        for i in range(Z):
+            off = pl.multiple_of(512 * i + target * 128, 128)
+            out[16 * i : 16 * i + 16, 512:640] = normed[:, pl.ds(off, 128)]
+    for load in rows:
+        load.wait()
+
+
+def prepare(tokens, mixer_gain, down_weight, mg, eg, ig, fg, stabilizer, memory):
+    vmem = pl.BlockSpec(memory_space=pltpu.VMEM)
+    ins = [tokens, mixer_gain[None], down_weight.T, mg[None], eg[None], ig, fg, stabilizer.T]
+    ins = [pltpu.with_memory_space_constraint(a, pltpu.HBM) for a in ins + [memory]]
+    return pl.pallas_call(
+        prepare_kernel,
+        in_specs=[pl.BlockSpec(memory_space=pltpu.HBM)] * 9,
+        out_specs=[vmem] * 6,
+        out_shape=[pltpu.VMEM((72, 640), BF)] * 4
+        + [pltpu.VMEM((16, 128), F32), pltpu.VMEM((EARLY, *memory.shape[1:]), F32)],
+        scratch_shapes=[pltpu.VMEM(ins[i].shape, ins[i].dtype) for i in (0, 1, 3, 4, 5, 6, 7)]
+        + [
+            pltpu.VMEM((16, 2048), BF),
+            pltpu.VMEM((64, 512), BF),
+            pltpu.SemaphoreType.DMA((8,)),
+            pltpu.SemaphoreType.DMA((EARLY,)),
+        ],
+        compiler_params=kernel_room(4),
+        name="prepare",
+    )(*ins)
+
+
+def route_kernel(routes, weights, send, take):
+    small = lax.broadcasted_iota(jnp.int32, (16, 16), 0)
+    across = lax.broadcasted_iota(jnp.int32, (16, 16), 1)
     pick = jnp.where(
         lax.broadcasted_iota(jnp.int32, (16, 512), 1)
         == lax.broadcasted_iota(jnp.int32, (16, 512), 0) + lax.axis_index("ep") * 16,
@@ -175,19 +209,19 @@
             take[at : at + 16] = piece.astype(BF)
 
 
-def route(tokens, mixer_gain, ig, fg, stabilizer, routes, weights):
+def route(routes, weights):
     vmem = pl.BlockSpec(memory_space=pltpu.VMEM)
     return pl.pallas_call(
         route_kernel,
-        in_specs=[vmem] * 7,
-        out_specs=[vmem] * 3,
+        in_specs=[vmem] * 2,
+        out_specs=[vmem] * 2,
         out_shape=[
-            pltpu.VMEM((16, 128), F32),
             pltpu.VMEM((32, 256), BF),
             pltpu.VMEM((96, 256), BF),
         ],
+        compiler_params=kernel_room(4),
         name="route",
-    )(tokens, mixer_gain[None], ig, fg, stabilizer.T, routes.T, weights.T)
+    )(routes.T, weights.T)
 
 
 def stack_kernel(a0, a1, a2, a3, out):
@@ -251,29 +285,35 @@
     )(*on_chip(*packed_by_shift, *weights, *partner))
 
 
-def fetch_kernel(memory, out, sems):
+def fetch(memory, start, stop):
+    def kernel(whole, out, sems):
+        loads = [
+            pltpu.make_async_copy(whole.at[start + i], out.at[i], sems.at[i])
+            for i in range(stop - start)
+        ]
+        for load in loads:
+            load.start()
+        for load in loads:
+            load.wait()
+
+    return pl.pallas_call(
+        kernel,
+        in_specs=[pl.BlockSpec(memory_space=pltpu.HBM)],
+        out_specs=pl.BlockSpec(memory_space=pltpu.VMEM),
+        out_shape=pltpu.VMEM((stop - start, *memory.shape[1:]), F32),
+        scratch_shapes=[pltpu.SemaphoreType.DMA((stop - start,))],
+        compiler_params=kernel_room(4),
+        name="fetch_rows",
+    )(pltpu.with_memory_space_constraint(memory, pltpu.HBM))
+
+
+def read_kernel(own, r1, r2, r3, gates, hg, early, held, memory, out, late, sems):
     loads = [
-        pltpu.make_async_copy(memory.at[n], out.at[n], sems.at[n]) for n in range(out.shape[0])
+        pltpu.make_async_copy(memory.at[HELD + i], late.at[i], sems.at[i])
+        for i in range(late.shape[0])
     ]
     for load in loads:
         load.start()
-    for load in loads:
-        load.wait()
-
-
-def fetch(memory):
-    return pl.pallas_call(
-        fetch_kernel,
-        in_specs=[pl.BlockSpec(memory_space=pltpu.HBM)],
-        out_specs=pl.BlockSpec(memory_space=pltpu.VMEM),
-        out_shape=pltpu.VMEM(memory.shape, F32),
-        scratch_shapes=[pltpu.SemaphoreType.DMA((memory.shape[0],))],
-        compiler_params=kernel_room(4),
-        name="fetch",
-    )(pltpu.with_memory_space_constraint(memory, pltpu.HBM))
-
-
-def read_kernel(own, r1, r2, r3, gates, hg, mem, out):
     parts = []
     for i in range(4):
         at_i = slice(512 * i, 512 * (i + 1))
@@ -296,9 +336,15 @@
     read_rows = []
     for n in range(16):
         column = turned[:, n : n + 1]
+        if n >= HELD:
+            loads[n - HELD].wait()
+        if n < EARLY:
+            source, at = early, n
+        else:
+            source, at = (held, n - EARLY) if n < HELD else (late, n - HELD)
         acc = jnp.zeros((8, 512), F32)
         for j in range(64):
-            acc = acc + column[8 * j : 8 * j + 8] * mem[n, 0, 8 * j : 8 * j + 8, :]
+            acc = acc + column[8 * j : 8 * j + 8] * source[at, 0, 8 * j : 8 * j + 8, :]
         read_rows.append(jnp.sum(acc, axis=0, keepdims=True))
     read = score * value + jnp.concatenate(read_rows, axis=0)
     centered = read - jnp.mean(read, axis=1, keepdims=True)
@@ -306,16 +352,24 @@
     out[...] = gated.astype(BF)
 
 
-def read(own, came, gates, head_gain, memory):
-    vmem = pl.BlockSpec(memory_space=pltpu.VMEM)
+def read(own, came, gates, head_gain, early, held, memory):
+    vmem = pl.BlockSpec(memory_space=pltpu.VMEM)
+    late = memory.shape[0] - HELD
     return pl.pallas_call(
         read_kernel,
-        in_specs=[vmem] * 7,
+        in_specs=[vmem] * 8 + [pl.BlockSpec(memory_space=pltpu.HBM)],
         out_specs=vmem,
         out_shape=pltpu.VMEM((16, 512), BF),
-        compiler_params=kernel_room(8),
+        scratch_shapes=[
+            pltpu.VMEM((late, *memory.shape[1:]), F32),
+            pltpu.SemaphoreType.DMA((late,)),
+        ],
+        compiler_params=kernel_room(16),
         name="read",
-    )(*on_chip(own, *came), gates, head_gain[None], memory)
+    )(
+        *on_chip(own, *came), gates, head_gain[None], early, held,
+        pltpu.with_memory_space_constraint(memory, pltpu.HBM),
+    )
 
 
 def paired(mine, other, c, odd):
@@ -518,26 +572,25 @@
     output_gain,
 ):
     ep_count = lax.axis_size("ep")
-    packed = prepare(tokens, mixer_gain, down_weight, mixed_gain, expert_gain)
-    by_y = [along_y(packed[s], s) for s in (2, 1, 3)]
-    by_y = [packed[0], by_y[1], by_y[0], by_y[2]]
+    *packed, gates, early = prepare(
+        tokens, mixer_gain, down_weight, mixed_gain, expert_gain, igate_weight,
+        fgate_weight, stabilizer, memory,
+    )
+    by_y = [packed[0]] + spread(lambda s: along_y(packed[s], s), FAR_FIRST)
     w0 = join((query_weight, key_weight, value_weight, outgate_weight))
-    by_z = [along_z(w0, s) for s in (2, 1, 3)]
-    by_z = [w0, by_z[1], by_z[0], by_z[2]]
-    gates, send_from, take_with = route(
-        tokens, mixer_gain, igate_weight, fgate_weight, stabilizer, routes, route_weights
-    )
+    by_z = [w0] + spread(lambda s: along_z(w0, s), NEAR_FIRST)
+    send_from, take_with = route(routes, route_weights)
     down_y = stack_down(by_y)
-    down_z = [along_z(down_y, s) for s in (2, 1, 3)]
-    down_z = [down_y, down_z[1], down_z[0], down_z[2]]
-    held = fetch(memory)
+    down_z = [down_y] + spread(lambda s: along_z(down_y, s), NEAR_FIRST)
+    held = fetch(memory, EARLY, HELD)
     partner = [other_core(w) for w in by_z]
-    own, t1, t2, t3 = project(by_y, by_z, partner)
-    came = [along_y(t, -s) for s, t in ((2, t2), (1, t1), (3, t3))]
-    down_partner = [other_core(d) for d in down_z]
-    gated = read(own, came, gates, head_gain, held)
+    own, *owed = project(by_y, by_z, partner)
+    came = spread(lambda s: along_y(owed[s - 1], -s), FAR_FIRST)
+    down_partner = [other_core(d) for d in down_z[1:]]
+    down_partner = [other_core(down_y)] + down_partner
+    gated = read(own, came, gates, head_gain, early, held, memory)
     part, send, gains = down_project(gated, down_z, down_partner)
-    mixed = [along_tp(send, s) for s in (2, 1, 3)]
+    mixed = spread(lambda s: along_tp(send, s), FAR_FIRST)
     weights = fetch_experts(gate_proj, up_proj, expert_down)
     residual, outgoing = dispatch(tokens, part, mixed, gains, send_from)
     arrived = lax.all_to_all(
@@ -548,7 +601,7 @@
         value.reshape(ep_count, 8, 1024), "ep", 0, 0, tiled=True
     ).reshape(256, 1024)
     own_sum, sent = combine(take_with, returned)
-    others = [along_tp(sent, s) for s in (2, 1, 3)]
+    others = spread(lambda s: along_tp(sent, s), FAR_FIRST)
     return finish(own_sum, others, residual, output_gain)
 
 

time: 132 us -> 117 us (0.89)
  local copies, waits for them, and re-layouts: 17.4 us -> 5.89 us
  starting transfers between devices: 52.3 us -> 49.4 us
  Pallas kernels: 20.2 us -> 17.7 us
  waiting for transfers between devices: 26.2 us -> 28.2 us
    unnamed x18, local copies, waits for them, and re-layouts: 17.4 us -> 5.89 us
    ppermute x6, waiting for transfers between devices: 7.84 us -> 11.4 us  [along_y(): return lax.ppermute(a, 'ep', ep_moves(0, s, 0))]
    all_to_all x1, starting transfers between devices: 9.93 us -> 7.14 us  [layer(): lax.all_to_all(outgoing.reshape(ep_count, 8, 1024), 'ep', 0, 0, tiled=True)]
    pallas_call x4, Pallas kernels: 11.3 us -> 8.85 us  [the longest x1 3.47 us: fetch(): pl.pallas_call(kernel, in_specs=[pl.BlockSpec(memory_space=pltpu.HBM)], o...]
    ppermute x6, waiting for transfers between devices: 5.18 us -> 3 us  [along_z(): return lax.ppermute(a, 'ep', ep_moves(s, 0, 0))]
where the time goes in v2:
time: 117 us; the launch traced here: 116 us
  starting transfers between devices  49.4 us (42%)
  waiting for transfers between devices  28.2 us (24%)
  Pallas kernels  17.7 us (15%)
  blocking collectives  15.1 us (13%)
  local copies, waits for them, and re-layouts  5.89 us (5%)
    ppermute x6, starting transfers between devices, along_z(): return lax.ppermute(a, 'ep', ep_moves(s, 0, 0))  16.6 us
    all_to_all x1, blocking collectives, layer(): lax.all_to_all(value.reshape(ep_count, 8, 1024), 'ep', 0, 0, tiled=True)  15.1 us
    ppermute x6, starting transfers between devices, along_y(): return lax.ppermute(a, 'ep', ep_moves(0, s, 0))  13.7 us
    ppermute x6, waiting for transfers between devices, along_y(): return lax.ppermute(a, 'ep', ep_moves(0, s, 0))  11.4 us
    ppermute x6, starting transfers between devices, along_tp(): return lax.ppermute(a, 'tp', [(i, (i + s) % TP) for i in range(TP)])  10 us
    all_to_all x1, starting transfers between devices, layer(): lax.all_to_all(outgoing.reshape(ep_count, 8, 1024), 'ep', 0, 0, tiled=True)  7.14 us
    ppermute x6, waiting for transfers between devices, along_tp(): return lax.ppermute(a, 'tp', [(i, (i + s) % TP) for i in range(TP)])  6.56 us
    unnamed x18, local copies, waits for them, and re-layouts  5.89 us
  transfers between devices with their start and end apart: 27, of which 13 were waited for; matrix products, arithmetic and copies ran while one was open for 0% of the time, Pallas kernels for 11%

profile of v2, /device:TPU:0, one launch (start us, length us, event | category | flops | bytes accessed | tf_op | source)
XLA Modules:
  0.0 116.5 jit_solution(4218013589890823429)
XLA Ops:
  0.0 1.0 join.1.w0
  1.0 2.1 %collective-permute-start.3 = (bf16[64,2048]{1,0:T(8,128)(2,1)S(1)}, bf16[64,2048]{1,0:T(8,128)(2,1)S(1)}, u32[]{:S(2)}, u32[]{:S(2)}) collective-permute-start(bf16[64,2048]{1,0:T(8,128)(2,1)S(1)} %join.1.w0), channel_id=1, source_target_pairs={{0,32},{4,36},{8,40},{12,44},{16,48},{20,52},{24,56},{28,60},{32,6... | collective-permute-start | bytes 786440 | tf_op jit(solution)/shard_map/ppermute | solution.py:32
  3.1 2.4 %prepare.1 = (bf16[72,640]{1,0:T(8,128)(2,1)S(1)}, bf16[72,640]{1,0:T(8,128)(2,1)S(1)}, bf16[72,640]{1,0:T(8,128)(2,1)S(1)}, bf16[72,640]{1,0:T(8,128)(2,1)S(1)}...) custom-call(bf16[16,2048]{1,0:T(8,128)(2,1)} %x.1, f32[1,2048]{1,0:T(1,128)} %bitcast.21, ...), custom_call_target="tpu_custom_call" | custom-call | tf_op jit(solution)/shard_map/prepare/pallas_call | solution.py:156
  5.5 1.6 %collective-permute-start = (bf16[72,640]{1,0:T(8,128)(2,1)S(1)}, bf16[72,640]{1,0:T(8,128)(2,1)S(1)}, u32[]{:S(2)}, u32[]{:S(2)}) collective-permute-start(bf16[72,640]{1,0:T(8,128)(2,1)S(1)} %get-tuple-element.29), channel_id=1, source_target_pairs={{0,8},{4,12},{8,16},{12,20},{16,24},{20,28},{24,0},{28,4},{32,40},... | collective-permute-start | bytes 276488 | tf_op jit(solution)/shard_map/ppermute | solution.py:36
  7.1 3.6 %collective-permute-start.4 = (bf16[64,2048]{1,0:T(8,128)(2,1)S(1)}, bf16[64,2048]{1,0:T(8,128)(2,1)S(1)}, u32[]{:S(2)}, u32[]{:S(2)}) collective-permute-start(bf16[64,2048]{1,0:T(8,128)(2,1)S(1)} %join.1.w0), channel_id=1, source_target_pairs={{0,64},{4,68},{8,72},{12,76},{16,80},{20,84},{24,88},{28,92},{32,9... | collective-permute-start | bytes 786440 | tf_op jit(solution)/shard_map/ppermute | solution.py:32
  10.7 1.0 collective-permute-start.5
  11.7 0.0 collective-permute-start.6
  11.7 0.0 collective-permute-done.3.w1
  11.7 0.5 collective-permute-start.7
  12.3 0.0 collective-permute-done.n1.a1
  12.3 2.9 %collective-permute-start.1 = (bf16[72,640]{1,0:T(8,128)(2,1)S(1)}, bf16[72,640]{1,0:T(8,128)(2,1)S(1)}, u32[]{:S(2)}, u32[]{:S(2)}) collective-permute-start(bf16[72,640]{1,0:T(8,128)(2,1)S(1)} %get-tuple-element.30), channel_id=1, source_target_pairs={{0,16},{4,20},{8,24},{12,28},{16,0},{20,4},{24,8},{28,12},{32,48},... | collective-permute-start | bytes 276488 | tf_op jit(solution)/shard_map/ppermute | solution.py:36
  15.2 3.3 %collective-permute-done.1.n2.a2 = bf16[72,640]{1,0:T(8,128)(2,1)S(1)} collective-permute-done((bf16[72,640]{1,0:T(8,128)(2,1)S(1)}, bf16[72,640]{1,0:T(8,128)(2,1)S(1)}, u32[]{:S(2)}, u32[]{:S(2)}) %collective-permute-start.1) | collective-permute-done | bytes 92192 | tf_op jit(solution)/shard_map/ppermute | solution.py:36
  18.4 2.7 %collective-permute-start.2 = (bf16[72,640]{1,0:T(8,128)(2,1)S(1)}, bf16[72,640]{1,0:T(8,128)(2,1)S(1)}, u32[]{:S(2)}, u32[]{:S(2)}) collective-permute-start(bf16[72,640]{1,0:T(8,128)(2,1)S(1)} %get-tuple-element.31), channel_id=1, source_target_pairs={{0,24},{4,28},{8,0},{12,4},{16,8},{20,12},{24,16},{28,20},{32,56},... | collective-permute-start | bytes 276488 | tf_op jit(solution)/shard_map/ppermute | solution.py:36
  21.1 2.2 %collective-permute-done.2.n3.a3 = bf16[72,640]{1,0:T(8,128)(2,1)S(1)} collective-permute-done((bf16[72,640]{1,0:T(8,128)(2,1)S(1)}, bf16[72,640]{1,0:T(8,128)(2,1)S(1)}, u32[]{:S(2)}, u32[]{:S(2)}) %collective-permute-start.2) | collective-permute-done | bytes 92192 | tf_op jit(solution)/shard_map/ppermute | solution.py:36
  23.3 0.8 collective-permute-start.13
  24.1 6.6 %collective-permute-start.14 = (bf16[288,512]{1,0:T(8,128)(2,1)S(1)}, bf16[288,512]{1,0:T(8,128)(2,1)S(1)}, u32[]{:S(2)}, u32[]{:S(2)}) collective-permute-start(bf16[288,512]{1,0:T(8,128)(2,1)S(1)} %stack_down.1.d0), channel_id=1, source_target_pairs={{0,64},{4,68},{8,72},{12,76},{16,80},{20,84},{24,88},{28,92},{32,9... | collective-permute-start | bytes 884744 | tf_op jit(solution)/shard_map/ppermute | solution.py:32
  30.7 0.0 collective-permute-done.5.w3
  30.7 2.5 %collective-permute-start.15 = (bf16[288,512]{1,0:T(8,128)(2,1)S(1)}, bf16[288,512]{1,0:T(8,128)(2,1)S(1)}, u32[]{:S(2)}, u32[]{:S(2)}) collective-permute-start(bf16[288,512]{1,0:T(8,128)(2,1)S(1)} %stack_down.1.d0), channel_id=1, source_target_pairs={{0,96},{4,100},{8,104},{12,108},{16,112},{20,116},{24,120},{28,124... | collective-permute-start | bytes 884744 | tf_op jit(solution)/shard_map/ppermute | solution.py:32
  33.2 0.0 collective-permute-done.6.p0
  33.2 0.0 collective-permute-start.8
  33.2 0.0 collective-permute-done.7.p1
  33.2 0.5 collective-permute-start.9
  33.7 1.0 collective-permute-done.8.p2
  34.7 0.4 collective-permute-done.9.p3
  35.1 0.5 project.1
  35.7 3.7 %collective-permute-start.10 = (bf16[16,3072]{1,0:T(8,128)(2,1)S(1)}, bf16[16,3072]{1,0:T(8,128)(2,1)S(1)}, u32[]{:S(2)}, u32[]{:S(2)}) collective-permute-start(bf16[16,3072]{1,0:T(8,128)(2,1)S(1)} %get-tuple-element.33), channel_id=1, source_target_pairs={{0,24},{4,28},{8,0},{12,4},{16,8},{20,12},{24,16},{28,20},{32,56},... | collective-permute-start | bytes 294920 | tf_op jit(solution)/shard_map/ppermute | solution.py:36
  39.3 0.0 collective-permute-start.16
  39.3 0.5 collective-permute-start.17
  39.8 3.0 %collective-permute-done.14.d2 = bf16[288,512]{1,0:T(8,128)(2,1)S(1)} collective-permute-done((bf16[288,512]{1,0:T(8,128)(2,1)S(1)}, bf16[288,512]{1,0:T(8,128)(2,1)S(1)}, u32[]{:S(2)}, u32[]{:S(2)}) %collective-permute-start.14) | collective-permute-done | bytes 294944 | tf_op jit(solution)/shard_map/ppermute | solution.py:32
  42.8 0.5 collective-permute-start.19
  43.4 1.8 %collective-permute-start.11 = (bf16[16,3072]{1,0:T(8,128)(2,1)S(1)}, bf16[16,3072]{1,0:T(8,128)(2,1)S(1)}, u32[]{:S(2)}, u32[]{:S(2)}) collective-permute-start(bf16[16,3072]{1,0:T(8,128)(2,1)S(1)} %get-tuple-element.34), channel_id=1, source_target_pairs={{0,16},{4,20},{8,24},{12,28},{16,0},{20,4},{24,8},{28,12},{32,48},... | collective-permute-start | bytes 294920 | tf_op jit(solution)/shard_map/ppermute | solution.py:36
  45.2 4.5 %collective-permute-done.11.r2 = bf16[16,3072]{1,0:T(8,128)(2,1)S(1)} collective-permute-done((bf16[16,3072]{1,0:T(8,128)(2,1)S(1)}, bf16[16,3072]{1,0:T(8,128)(2,1)S(1)}, u32[]{:S(2)}, u32[]{:S(2)}) %collective-permute-start.11) | collective-permute-done | bytes 98336 | tf_op jit(solution)/shard_map/ppermute | solution.py:36
  49.6 0.9 collective-permute-start.12
  50.6 3.5 %fetch_rows.1.held = f32[8,1,512,512]{3,2,1,0:T(8,128)S(1)} custom-call(f32[16,1,512,512]{3,2,1,0:T(8,128)} %memory.3), custom_call_target="tpu_custom_call" | custom-call | tf_op jit(solution)/shard_map/fetch_rows/pallas_call | solution.py:299
  54.0 1.5 %collective-permute-done.12.r3 = bf16[16,3072]{1,0:T(8,128)(2,1)S(1)} collective-permute-done((bf16[16,3072]{1,0:T(8,128)(2,1)S(1)}, bf16[16,3072]{1,0:T(8,128)(2,1)S(1)}, u32[]{:S(2)}, u32[]{:S(2)}) %collective-permute-start.12) | collective-permute-done | bytes 98336 | tf_op jit(solution)/shard_map/ppermute | solution.py:36
  55.6 2.5 %read.1.g = bf16[16,512]{1,0:T(8,128)(2,1)S(1)} custom-call(f32[16,2048]{1,0:T(8,128)S(1)} %get-tuple-element.32.own, bf16[16,3072]{1,0:T(8,128)(2,1)S(1)} %collective-permute-done.10.r1, bf16[16,3072]{1,0:T(8,128)(2,1)S(1)} %collective-permute-done.11.r2, bf16[16,3072]{1,0:T(8,128)(2,1)S(1)} %collective-permute-done.12.r3, ...), custom_call_target="tpu_custom_call" | custom-call | tf_op jit(solution)/shard_map/read/pallas_call | solution.py:358
  58.1 0.0 copy-start.5
  58.1 0.0 copy-start.6
  58.1 0.0 copy-start.4
  58.2 0.7 down_project.1
  58.9 1.6 %collective-permute-start.20 = (bf16[16,2048]{1,0:T(8,128)(2,1)S(1)}, bf16[16,2048]{1,0:T(8,128)(2,1)S(1)}, u32[]{:S(2)}, u32[]{:S(2)}) collective-permute-start(bf16[16,2048]{1,0:T(8,128)(2,1)S(1)} %get-tuple-element.39), channel_id=1, source_target_pairs={{0,1},{1,2},{2,3},{3,0},{4,5},{5,6},{6,7},{7,4},{8,9},{9,10},{10,1... | collective-permute-start | bytes 196616 | tf_op jit(solution)/shard_map/ppermute | solution.py:54
  60.5 2.7 %collective-permute-start.21 = (bf16[16,2048]{1,0:T(8,128)(2,1)S(1)}, bf16[16,2048]{1,0:T(8,128)(2,1)S(1)}, u32[]{:S(2)}, u32[]{:S(2)}) collective-permute-start(bf16[16,2048]{1,0:T(8,128)(2,1)S(1)} %get-tuple-element.39), channel_id=1, source_target_pairs={{0,2},{1,3},{2,0},{3,1},{4,6},{5,7},{6,4},{7,5},{8,10},{9,11},{10,... | collective-permute-start | bytes 196616 | tf_op jit(solution)/shard_map/ppermute | solution.py:54
  63.2 1.4 %collective-permute-start.22 = (bf16[16,2048]{1,0:T(8,128)(2,1)S(1)}, bf16[16,2048]{1,0:T(8,128)(2,1)S(1)}, u32[]{:S(2)}, u32[]{:S(2)}) collective-permute-start(bf16[16,2048]{1,0:T(8,128)(2,1)S(1)} %get-tuple-element.39), channel_id=1, source_target_pairs={{0,3},{1,0},{2,1},{3,2},{4,7},{5,4},{6,5},{7,6},{8,11},{9,8},{10,9... | collective-permute-start | bytes 196616 | tf_op jit(solution)/shard_map/ppermute | solution.py:54
  64.6 0.4 route.1
  65.1 1.2 collective-permute-done.21.r2
  66.2 1.2 %collective-permute-done.22.r3 = bf16[16,2048]{1,0:T(8,128)(2,1)S(1)} collective-permute-done((bf16[16,2048]{1,0:T(8,128)(2,1)S(1)}, bf16[16,2048]{1,0:T(8,128)(2,1)S(1)}, u32[]{:S(2)}, u32[]{:S(2)}) %collective-permute-start.22) | collective-permute-done | bytes 65568 | tf_op jit(solution)/shard_map/ppermute | solution.py:54
  67.5 1.3 %dispatch.1 = (bf16[16,2048]{1,0:T(8,128)(2,1)S(1)}, bf16[256,1024]{1,0:T(8,128)(2,1)}) custom-call(bf16[16,2048]{1,0:T(8,128)(2,1)S(1)} %copy-done.4, f32[16,2048]{1,0:T(8,128)S(1)} %get-tuple-element.38.part, bf16[16,2048]{1,0:T(8,128)(2,1)S(1)} %collective-permute-done.20.r1, bf16[16,2048]{1,0:T(8,128)(2,1)S(1)} %collective-permute-done.21.r2, ...), custom_call_target="tpu_custom_call" | custom-call | tf_op jit(solution)/shard_map/dispatch/pallas_call | solution.py:458
  68.8 7.1 %all-to-all-start = ((bf16[32,8,1024]{2,1,0:T(8,128)(2,1)}), bf16[32,8,1024]{2,1,0:T(8,128)(2,1)S(1)}, u32[]{:S(2)}, u32[]{:S(2)}) async-start(bf16[32,8,1024]{2,1,0:T(8,128)(2,1)} %bitcast.8), calls=%async_computation | async-start | bytes 1048576 | tf_op jit(solution)/shard_map/all_to_all | solution.py:596
  75.9 2.9 %fetch_experts.1 = (bf16[2048,512]{1,0:T(8,128)(2,1)S(1)}, bf16[2048,512]{1,0:T(8,128)(2,1)S(1)}, bf16[512,2048]{1,0:T(8,128)(2,1)S(1)}) custom-call(bf16[1,2048,512]{2,1,0:T(8,128)(2,1)} %g.1, bf16[1,2048,512]{2,1,0:T(8,128)(2,1)} %u.1, bf16[1,512,2048]{2,1,0:T(8,128)(2,1)} %d.1), custom_call_target="tpu_custom_call" | custom-call | tf_op jit(solution)/shard_map/fetch_experts/pallas_call | solution.py:434
  78.8 1.4 %copy-done = bf16[2048,512]{1,0:T(8,128)(2,1)} copy-done((bf16[2048,512]{1,0:T(8,128)(2,1)}, bf16[2048,512]{1,0:T(8,128)(2,1)S(1)}, u32[]{:S(2)}) %copy-start) | copy-done | bytes 2097176
  80.2 1.3 %copy-done.2 = bf16[512,2048]{1,0:T(8,128)(2,1)} copy-done((bf16[512,2048]{1,0:T(8,128)(2,1)}, bf16[512,2048]{1,0:T(8,128)(2,1)S(1)}, u32[]{:S(2)}) %copy-start.2) | copy-done | bytes 2097176
  81.5 5.8 %all-to-all-done = bf16[32,8,1024]{2,1,0:T(8,128)(2,1)S(1)} async-done(((bf16[32,8,1024]{2,1,0:T(8,128)(2,1)}), bf16[32,8,1024]{2,1,0:T(8,128)(2,1)S(1)}, u32[]{:S(2)}, u32[]{:S(2)}) %all-to-all-start) | async-done | bytes 524320 | tf_op jit(solution)/shard_map/all_to_all | solution.py:596
  87.3 1.6 %copy-done.1 = bf16[2048,512]{1,0:T(8,128)(2,1)S(1)} copy-done((bf16[2048,512]{1,0:T(8,128)(2,1)S(1)}, bf16[2048,512]{1,0:T(8,128)(2,1)}, u32[]{:S(2)}) %copy-start.1) | copy-done | bytes 2097176
  88.9 1.6 %copy-done.3 = bf16[512,2048]{1,0:T(8,128)(2,1)S(1)} copy-done((bf16[512,2048]{1,0:T(8,128)(2,1)S(1)}, bf16[512,2048]{1,0:T(8,128)(2,1)}, u32[]{:S(2)}) %copy-start.3) | copy-done | bytes 2097176
  90.5 1.5 %experts.1 = bf16[256,1024]{1,0:T(8,128)(2,1)S(1)} custom-call(bf16[256,1024]{1,0:T(8,128)(2,1)S(1)} %bitcast.13, bf16[2048,512]{1,0:T(8,128)(2,1)S(1)} %get-tuple-element.43.gate_w, bf16[2048,512]{1,0:T(8,128)(2,1)S(1)} %copy-done.1, bf16[512,2048]{1,0:T(8,128)(2,1)S(1)} %copy-done.3), custom_call_target="tpu_custom_call" | custom-call | tf_op jit(solution)/shard_map/experts/pallas_call | solution.py:499
  92.0 15.1 %all_to_all.10 = bf16[32,8,1024]{2,1,0:T(8,128)(2,1)S(1)} all-to-all(bf16[32,8,1024]{2,1,0:T(8,128)(2,1)S(1)} %bitcast.14), channel_id=1, replica_groups=mesh['ep'=32,'tp'=4] {'ep'}, dimensions={0} | all-to-all | bytes 1048576 | tf_op jit(solution)/shard_map/all_to_all | solution.py:600
  107.1 0.2 combine.1
  107.3 0.7 collective-permute-start.23
  107.9 3.5 %collective-permute-start.24 = (bf16[16,2048]{1,0:T(8,128)(2,1)S(1)}, bf16[16,2048]{1,0:T(8,128)(2,1)S(1)}, u32[]{:S(2)}, u32[]{:S(2)}) collective-permute-start(bf16[16,2048]{1,0:T(8,128)(2,1)S(1)} %get-tuple-element.47), channel_id=1, source_target_pairs={{0,2},{1,3},{2,0},{3,1},{4,6},{5,7},{6,4},{7,5},{8,10},{9,11},{10,... | collective-permute-start | bytes 196616 | tf_op jit(solution)/shard_map/ppermute | solution.py:54
  111.5 0.1 collective-permute-start.25
  111.6 1.3 %collective-permute-done.23.r1 = bf16[16,2048]{1,0:T(8,128)(2,1)S(1)} collective-permute-done((bf16[16,2048]{1,0:T(8,128)(2,1)S(1)}, bf16[16,2048]{1,0:T(8,128)(2,1)S(1)}, u32[]{:S(2)}, u32[]{:S(2)}) %collective-permute-start.23) | collective-permute-done | bytes 65568 | tf_op jit(solution)/shard_map/ppermute | solution.py:54
  112.8 2.1 %collective-permute-done.24.r2 = bf16[16,2048]{1,0:T(8,128)(2,1)S(1)} collective-permute-done((bf16[16,2048]{1,0:T(8,128)(2,1)S(1)}, bf16[16,2048]{1,0:T(8,128)(2,1)S(1)}, u32[]{:S(2)}, u32[]{:S(2)}) %collective-permute-start.24) | collective-permute-done | bytes 65568 | tf_op jit(solution)/shard_map/ppermute | solution.py:54
  115.0 0.8 collective-permute-done.25.r3
  115.7 0.7 finish.1
  (22 shorter events, 0.1 us)
Async XLA Ops:
  1.0 10.8 %collective-permute-start.3 = (bf16[64,2048]{1,0:T(8,128)(2,1)S(1)}, bf16[64,2048]{1,0:T(8,128)(2,1)S(1)}, u32[]{:S(2)}, u32[]{:S(2)}) collective-permute-start(bf16[64,2048]{1,0:T(8,128)(2,1)S(1)} %join.1.w0), channel_id=1, source_target_pairs={{0,32},{4,36},{8,40},{12,44},{16,48},{20,52},{24,56},{28,60},{32,6... | collective-permute-start | bytes 786440 | tf_op jit(solution)/shard_map/ppermute | solution.py:32
  5.5 6.8 %collective-permute-start = (bf16[72,640]{1,0:T(8,128)(2,1)S(1)}, bf16[72,640]{1,0:T(8,128)(2,1)S(1)}, u32[]{:S(2)}, u32[]{:S(2)}) collective-permute-start(bf16[72,640]{1,0:T(8,128)(2,1)S(1)} %get-tuple-element.29), channel_id=1, source_target_pairs={{0,8},{4,12},{8,16},{12,20},{16,24},{20,28},{24,0},{28,4},{32,40},... | collective-permute-start | bytes 276488 | tf_op jit(solution)/shard_map/ppermute | solution.py:36
  7.1 16.9 %collective-permute-start.4 = (bf16[64,2048]{1,0:T(8,128)(2,1)S(1)}, bf16[64,2048]{1,0:T(8,128)(2,1)S(1)}, u32[]{:S(2)}, u32[]{:S(2)}) collective-permute-start(bf16[64,2048]{1,0:T(8,128)(2,1)S(1)} %join.1.w0), channel_id=1, source_target_pairs={{0,64},{4,68},{8,72},{12,76},{16,80},{20,84},{24,88},{28,92},{32,9... | collective-permute-start | bytes 786440 | tf_op jit(solution)/shard_map/ppermute | solution.py:32
  10.7 19.9 %collective-permute-start.5 = (bf16[64,2048]{1,0:T(8,128)(2,1)S(1)}, bf16[64,2048]{1,0:T(8,128)(2,1)S(1)}, u32[]{:S(2)}, u32[]{:S(2)}) collective-permute-start(bf16[64,2048]{1,0:T(8,128)(2,1)S(1)} %join.1.w0), channel_id=1, source_target_pairs={{0,96},{4,100},{8,104},{12,108},{16,112},{20,116},{24,120},{28,124... | collective-permute-start | bytes 786440 | tf_op jit(solution)/shard_map/ppermute | solution.py:32
  11.7 21.5 %collective-permute-start.6 = (bf16[64,2048]{1,0:T(8,128)(2,1)S(1)}, bf16[64,2048]{1,0:T(8,128)(2,1)S(1)}, u32[]{:S(2)}, u32[]{:S(2)}) collective-permute-start(bf16[64,2048]{1,0:T(8,128)(2,1)S(1)} %join.1.w0), channel_id=1, source_target_pairs={{0,4},{4,0},{8,12},{12,8},{16,20},{20,16},{24,28},{28,24},{32,36},... | collective-permute-start | bytes 786440 | tf_op jit(solution)/shard_map/ppermute | solution.py:50
  11.7 21.5 %collective-permute-start.7 = (bf16[64,2048]{1,0:T(8,128)(2,1)S(1)}, bf16[64,2048]{1,0:T(8,128)(2,1)S(1)}, u32[]{:S(2)}, u32[]{:S(2)}) collective-permute-start(bf16[64,2048]{1,0:T(8,128)(2,1)S(1)} %collective-permute-done.3.w1), channel_id=1, source_target_pairs={{0,4},{4,0},{8,12},{12,8},{16,20},{20,16},{24,28},{28,24},{32,36},... | collective-permute-start | bytes 786440 | tf_op jit(solution)/shard_map/ppermute | solution.py:50
  12.3 6.2 %collective-permute-start.1 = (bf16[72,640]{1,0:T(8,128)(2,1)S(1)}, bf16[72,640]{1,0:T(8,128)(2,1)S(1)}, u32[]{:S(2)}, u32[]{:S(2)}) collective-permute-start(bf16[72,640]{1,0:T(8,128)(2,1)S(1)} %get-tuple-element.30), channel_id=1, source_target_pairs={{0,16},{4,20},{8,24},{12,28},{16,0},{20,4},{24,8},{28,12},{32,48},... | collective-permute-start | bytes 276488 | tf_op jit(solution)/shard_map/ppermute | solution.py:36
  18.4 4.8 %collective-permute-start.2 = (bf16[72,640]{1,0:T(8,128)(2,1)S(1)}, bf16[72,640]{1,0:T(8,128)(2,1)S(1)}, u32[]{:S(2)}, u32[]{:S(2)}) collective-permute-start(bf16[72,640]{1,0:T(8,128)(2,1)S(1)} %get-tuple-element.31), channel_id=1, source_target_pairs={{0,24},{4,28},{8,0},{12,4},{16,8},{20,12},{24,16},{28,20},{32,56},... | collective-permute-start | bytes 276488 | tf_op jit(solution)/shard_map/ppermute | solution.py:36
  23.3 16.1 %collective-permute-start.13 = (bf16[288,512]{1,0:T(8,128)(2,1)S(1)}, bf16[288,512]{1,0:T(8,128)(2,1)S(1)}, u32[]{:S(2)}, u32[]{:S(2)}) collective-permute-start(bf16[288,512]{1,0:T(8,128)(2,1)S(1)} %stack_down.1.d0), channel_id=1, source_target_pairs={{0,32},{4,36},{8,40},{12,44},{16,48},{20,52},{24,56},{28,60},{32,6... | collective-permute-start | bytes 884744 | tf_op jit(solution)/shard_map/ppermute | solution.py:32
  24.1 18.8 %collective-permute-start.14 = (bf16[288,512]{1,0:T(8,128)(2,1)S(1)}, bf16[288,512]{1,0:T(8,128)(2,1)S(1)}, u32[]{:S(2)}, u32[]{:S(2)}) collective-permute-start(bf16[288,512]{1,0:T(8,128)(2,1)S(1)} %stack_down.1.d0), channel_id=1, source_target_pairs={{0,64},{4,68},{8,72},{12,76},{16,80},{20,84},{24,88},{28,92},{32,9... | collective-permute-start | bytes 884744 | tf_op jit(solution)/shard_map/ppermute | solution.py:32
  30.7 12.2 %collective-permute-start.15 = (bf16[288,512]{1,0:T(8,128)(2,1)S(1)}, bf16[288,512]{1,0:T(8,128)(2,1)S(1)}, u32[]{:S(2)}, u32[]{:S(2)}) collective-permute-start(bf16[288,512]{1,0:T(8,128)(2,1)S(1)} %stack_down.1.d0), channel_id=1, source_target_pairs={{0,96},{4,100},{8,104},{12,108},{16,112},{20,116},{24,120},{28,124... | collective-permute-start | bytes 884744 | tf_op jit(solution)/shard_map/ppermute | solution.py:32
  33.2 1.5 %collective-permute-start.8 = (bf16[64,2048]{1,0:T(8,128)(2,1)S(1)}, bf16[64,2048]{1,0:T(8,128)(2,1)S(1)}, u32[]{:S(2)}, u32[]{:S(2)}) collective-permute-start(bf16[64,2048]{1,0:T(8,128)(2,1)S(1)} %collective-permute-done.4.w2), channel_id=1, source_target_pairs={{0,4},{4,0},{8,12},{12,8},{16,20},{20,16},{24,28},{28,24},{32,36},... | collective-permute-start | bytes 786440 | tf_op jit(solution)/shard_map/ppermute | solution.py:50
  33.2 1.9 %collective-permute-start.9 = (bf16[64,2048]{1,0:T(8,128)(2,1)S(1)}, bf16[64,2048]{1,0:T(8,128)(2,1)S(1)}, u32[]{:S(2)}, u32[]{:S(2)}) collective-permute-start(bf16[64,2048]{1,0:T(8,128)(2,1)S(1)} %collective-permute-done.5.w3), channel_id=1, source_target_pairs={{0,4},{4,0},{8,12},{12,8},{16,20},{20,16},{24,28},{28,24},{32,36},... | collective-permute-start | bytes 786440 | tf_op jit(solution)/shard_map/ppermute | solution.py:50
  35.7 7.7 %collective-permute-start.10 = (bf16[16,3072]{1,0:T(8,128)(2,1)S(1)}, bf16[16,3072]{1,0:T(8,128)(2,1)S(1)}, u32[]{:S(2)}, u32[]{:S(2)}) collective-permute-start(bf16[16,3072]{1,0:T(8,128)(2,1)S(1)} %get-tuple-element.33), channel_id=1, source_target_pairs={{0,24},{4,28},{8,0},{12,4},{16,8},{20,12},{24,16},{28,20},{32,56},... | collective-permute-start | bytes 294920 | tf_op jit(solution)/shard_map/ppermute | solution.py:36
  39.3 18.8 %collective-permute-start.16 = (bf16[288,512]{1,0:T(8,128)(2,1)S(1)}, bf16[288,512]{1,0:T(8,128)(2,1)S(1)}, u32[]{:S(2)}, u32[]{:S(2)}) collective-permute-start(bf16[288,512]{1,0:T(8,128)(2,1)S(1)} %stack_down.1.d0), channel_id=1, source_target_pairs={{0,4},{4,0},{8,12},{12,8},{16,20},{20,16},{24,28},{28,24},{32,36},... | collective-permute-start | bytes 884744 | tf_op jit(solution)/shard_map/ppermute | solution.py:50
  39.3 18.8 %collective-permute-start.17 = (bf16[288,512]{1,0:T(8,128)(2,1)S(1)}, bf16[288,512]{1,0:T(8,128)(2,1)S(1)}, u32[]{:S(2)}, u32[]{:S(2)}) collective-permute-start(bf16[288,512]{1,0:T(8,128)(2,1)S(1)} %collective-permute-done.13.d1), channel_id=1, source_target_pairs={{0,4},{4,0},{8,12},{12,8},{16,20},{20,16},{24,28},{28,24},{32,36},... | collective-permute-start | bytes 884744 | tf_op jit(solution)/shard_map/ppermute | solution.py:50
  42.8 15.3 %collective-permute-start.18 = (bf16[288,512]{1,0:T(8,128)(2,1)S(1)}, bf16[288,512]{1,0:T(8,128)(2,1)S(1)}, u32[]{:S(2)}, u32[]{:S(2)}) collective-permute-start(bf16[288,512]{1,0:T(8,128)(2,1)S(1)} %collective-permute-done.14.d2), channel_id=1, source_target_pairs={{0,4},{4,0},{8,12},{12,8},{16,20},{20,16},{24,28},{28,24},{32,36},... | collective-permute-start | bytes 884744 | tf_op jit(solution)/shard_map/ppermute | solution.py:50
  42.8 15.3 %collective-permute-start.19 = (bf16[288,512]{1,0:T(8,128)(2,1)S(1)}, bf16[288,512]{1,0:T(8,128)(2,1)S(1)}, u32[]{:S(2)}, u32[]{:S(2)}) collective-permute-start(bf16[288,512]{1,0:T(8,128)(2,1)S(1)} %collective-permute-done.15.d3), channel_id=1, source_target_pairs={{0,4},{4,0},{8,12},{12,8},{16,20},{20,16},{24,28},{28,24},{32,36},... | collective-permute-start | bytes 884744 | tf_op jit(solution)/shard_map/ppermute | solution.py:50
  43.4 6.3 %collective-permute-start.11 = (bf16[16,3072]{1,0:T(8,128)(2,1)S(1)}, bf16[16,3072]{1,0:T(8,128)(2,1)S(1)}, u32[]{:S(2)}, u32[]{:S(2)}) collective-permute-start(bf16[16,3072]{1,0:T(8,128)(2,1)S(1)} %get-tuple-element.34), channel_id=1, source_target_pairs={{0,16},{4,20},{8,24},{12,28},{16,0},{20,4},{24,8},{28,12},{32,48},... | collective-permute-start | bytes 294920 | tf_op jit(solution)/shard_map/ppermute | solution.py:36
  49.6 5.9 %copy-start.7 = (f32[512]{0:T(512)S(1)}, f32[512]{0:T(512)}, u32[]{:S(2)}) copy-start(f32[512]{0:T(512)} %param.30) | copy-start | bytes 6148
  49.6 5.9 %collective-permute-start.12 = (bf16[16,3072]{1,0:T(8,128)(2,1)S(1)}, bf16[16,3072]{1,0:T(8,128)(2,1)S(1)}, u32[]{:S(2)}, u32[]{:S(2)}) collective-permute-start(bf16[16,3072]{1,0:T(8,128)(2,1)S(1)} %get-tuple-element.35), channel_id=1, source_target_pairs={{0,8},{4,12},{8,16},{12,20},{16,24},{20,28},{24,0},{28,4},{32,40},... | collective-permute-start | bytes 294920 | tf_op jit(solution)/shard_map/ppermute | solution.py:36
  58.1 6.5 %copy-start.5 = (s32[512,4]{0,1:T(4,128)S(1)}, s32[512,4]{0,1:T(4,128)}, u32[]{:S(2)}) copy-start(s32[512,4]{0,1:T(4,128)} %param.34) | copy-start | bytes 24580
  58.1 6.5 %copy-start.6 = (f32[512,4]{0,1:T(4,128)S(1)}, f32[512,4]{0,1:T(4,128)}, u32[]{:S(2)}) copy-start(f32[512,4]{0,1:T(4,128)} %param.35) | copy-start | bytes 24580
  58.1 9.3 %copy-start.4 = (bf16[16,2048]{1,0:T(8,128)(2,1)S(1)}, bf16[16,2048]{1,0:T(8,128)(2,1)}, u32[]{:S(2)}) copy-start(bf16[16,2048]{1,0:T(8,128)(2,1)} %x.1) | copy-start | bytes 196612
  58.9 6.2 %collective-permute-start.20 = (bf16[16,2048]{1,0:T(8,128)(2,1)S(1)}, bf16[16,2048]{1,0:T(8,128)(2,1)S(1)}, u32[]{:S(2)}, u32[]{:S(2)}) collective-permute-start(bf16[16,2048]{1,0:T(8,128)(2,1)S(1)} %get-tuple-element.39), channel_id=1, source_target_pairs={{0,1},{1,2},{2,3},{3,0},{4,5},{5,6},{6,7},{7,4},{8,9},{9,10},{10,1... | collective-permute-start | bytes 196616 | tf_op jit(solution)/shard_map/ppermute | solution.py:54
  60.5 5.8 %collective-permute-start.21 = (bf16[16,2048]{1,0:T(8,128)(2,1)S(1)}, bf16[16,2048]{1,0:T(8,128)(2,1)S(1)}, u32[]{:S(2)}, u32[]{:S(2)}) collective-permute-start(bf16[16,2048]{1,0:T(8,128)(2,1)S(1)} %get-tuple-element.39), channel_id=1, source_target_pairs={{0,2},{1,3},{2,0},{3,1},{4,6},{5,7},{6,4},{7,5},{8,10},{9,11},{10,... | collective-permute-start | bytes 196616 | tf_op jit(solution)/shard_map/ppermute | solution.py:54
  63.2 4.3 %collective-permute-start.22 = (bf16[16,2048]{1,0:T(8,128)(2,1)S(1)}, bf16[16,2048]{1,0:T(8,128)(2,1)S(1)}, u32[]{:S(2)}, u32[]{:S(2)}) collective-permute-start(bf16[16,2048]{1,0:T(8,128)(2,1)S(1)} %get-tuple-element.39), channel_id=1, source_target_pairs={{0,3},{1,0},{2,1},{3,2},{4,7},{5,4},{6,5},{7,6},{8,11},{9,8},{10,9... | collective-permute-start | bytes 196616 | tf_op jit(solution)/shard_map/ppermute | solution.py:54
  68.8 18.6 %all-to-all-start = ((bf16[32,8,1024]{2,1,0:T(8,128)(2,1)}), bf16[32,8,1024]{2,1,0:T(8,128)(2,1)S(1)}, u32[]{:S(2)}, u32[]{:S(2)}) async-start(bf16[32,8,1024]{2,1,0:T(8,128)(2,1)} %bitcast.8), calls=%async_computation | async-start | bytes 1048576 | tf_op jit(solution)/shard_map/all_to_all | solution.py:596
  78.8 1.4 %copy-start = (bf16[2048,512]{1,0:T(8,128)(2,1)}, bf16[2048,512]{1,0:T(8,128)(2,1)S(1)}, u32[]{:S(2)}) copy-start(bf16[2048,512]{1,0:T(8,128)(2,1)S(1)} %get-tuple-element.44.up_w) | copy-start | bytes 6291460
  80.2 1.3 %copy-start.2 = (bf16[512,2048]{1,0:T(8,128)(2,1)}, bf16[512,2048]{1,0:T(8,128)(2,1)S(1)}, u32[]{:S(2)}) copy-start(bf16[512,2048]{1,0:T(8,128)(2,1)S(1)} %get-tuple-element.45.down_w) | copy-start | bytes 6291460
  87.3 1.6 %copy-start.1 = (bf16[2048,512]{1,0:T(8,128)(2,1)S(1)}, bf16[2048,512]{1,0:T(8,128)(2,1)}, u32[]{:S(2)}) copy-start(bf16[2048,512]{1,0:T(8,128)(2,1)} %copy-done) | copy-start | bytes 6291460
  88.9 1.6 %copy-start.3 = (bf16[512,2048]{1,0:T(8,128)(2,1)S(1)}, bf16[512,2048]{1,0:T(8,128)(2,1)}, u32[]{:S(2)}) copy-start(bf16[512,2048]{1,0:T(8,128)(2,1)} %copy-done.2) | copy-start | bytes 6291460
  90.5 25.2 %copy-start.8 = (f32[512]{0:T(512)S(1)}, f32[512]{0:T(512)}, u32[]{:S(2)}) copy-start(f32[512]{0:T(512)} %param.39) | copy-start | bytes 6148
  107.3 5.5 %collective-permute-start.23 = (bf16[16,2048]{1,0:T(8,128)(2,1)S(1)}, bf16[16,2048]{1,0:T(8,128)(2,1)S(1)}, u32[]{:S(2)}, u32[]{:S(2)}) collective-permute-start(bf16[16,2048]{1,0:T(8,128)(2,1)S(1)} %get-tuple-element.47), channel_id=1, source_target_pairs={{0,1},{1,2},{2,3},{3,0},{4,5},{5,6},{6,7},{7,4},{8,9},{9,10},{10,1... | collective-permute-start | bytes 196616 | tf_op jit(solution)/shard_map/ppermute | solution.py:54
  107.9 7.0 %collective-permute-start.24 = (bf16[16,2048]{1,0:T(8,128)(2,1)S(1)}, bf16[16,2048]{1,0:T(8,128)(2,1)S(1)}, u32[]{:S(2)}, u32[]{:S(2)}) collective-permute-start(bf16[16,2048]{1,0:T(8,128)(2,1)S(1)} %get-tuple-element.47), channel_id=1, source_target_pairs={{0,2},{1,3},{2,0},{3,1},{4,6},{5,7},{6,4},{7,5},{8,10},{9,11},{10,... | collective-permute-start | bytes 196616 | tf_op jit(solution)/shard_map/ppermute | solution.py:54
  111.5 4.3 %collective-permute-start.25 = (bf16[16,2048]{1,0:T(8,128)(2,1)S(1)}, bf16[16,2048]{1,0:T(8,128)(2,1)S(1)}, u32[]{:S(2)}, u32[]{:S(2)}) collective-permute-start(bf16[16,2048]{1,0:T(8,128)(2,1)S(1)} %get-tuple-element.47), channel_id=1, source_target_pairs={{0,3},{1,0},{2,1},{3,2},{4,7},{5,4},{6,5},{7,6},{8,11},{9,8},{10,9... | collective-permute-start | bytes 196616 | tf_op jit(solution)/shard_map/ppermute | solution.py:54

commit v3 on v2

--- a/solution.py
+++ b/solution.py
@@ -12,7 +12,7 @@
 BF = jnp.bfloat16
 F32 = jnp.float32
 Z, Y, C, TP = 4, 4, 2, 4
-EARLY, HELD = 4, 12
+EARLY, HELD = 5, 13
 
 
 def ep_at(z, y, c):
@@ -43,7 +43,7 @@
     return [came[s] for s in (1, 2, 3)]
 
 
-NEAR_FIRST, FAR_FIRST = (1, 3, 2), (2, 1, 3)
+FAR_FIRST = (2, 1, 3)
 
 
 def other_core(a):
@@ -225,9 +225,13 @@
 
 
 def stack_kernel(a0, a1, a2, a3, out):
+    gains = jnp.zeros((8, 256), F32)
     for i, a in enumerate((a0, a1, a2, a3)):
         out[64 * i : 64 * i + 64] = a[0:64, 0:512]
-        out[256 + 8 * i : 264 + 8 * i] = a[64:72, 0:512]
+        piece = a[64:72, 0:256].astype(F32)
+        gains = gains + (pltpu.roll(piece, 64 * i, 1) if i else piece)
+    out[256:264, 0:256] = gains.astype(BF)
+    out[256:264, 256:512] = jnp.zeros((8, 256), BF)
 
 
 def stack_down(pieces):
@@ -236,7 +240,7 @@
         stack_kernel,
         in_specs=[vmem] * 4,
         out_specs=vmem,
-        out_shape=pltpu.VMEM((288, 512), BF),
+        out_shape=pltpu.VMEM((264, 512), BF),
         compiler_params=kernel_room(4),
         name="stack_down",
     )(*on_chip(*pieces))
@@ -388,16 +392,15 @@
     for s, (d, e) in enumerate(zip((d0, d1, d2, d3), (e0, e1, e2, e3))):
         mine = lax.dot_general(gated, d[0:256], TURNED, preferred_element_type=F32)
         other = lax.dot_general(gated, e[0:256], TURNED, preferred_element_type=F32)
-        my_gains = d[256:288, 0:128].astype(F32)
-        other_gains = e[256:288, 0:128].astype(F32)
+        my_gains = d[256:264, 0:256].astype(F32)
+        other_gains = e[256:264, 0:256].astype(F32)
         for t in range(Y):
             at = slice(t // 2 * 128, t // 2 * 128 + 128)
             block = paired(mine[:, at], other[:, at], c, t % 2 == 1)
             off = pl.multiple_of(((z + (Z - s)) & 3) * 512 + ((y + (Y - t)) & 3) * 128, 128)
             part[:, pl.ds(off, 128)] = block
             send[:, pl.ds(off, 128)] = block.astype(BF)
-            at = slice(8 * t, 8 * t + 8)
-            factors[:, pl.ds(off, 128)] = paired(my_gains[at], other_gains[at], c, False)
+            factors[:, pl.ds(off, 128)] = paired(my_gains[:, at], other_gains[:, at], c, t % 2 == 1)
     gains[0:1] = factors[0:1] + factors[1:2] + factors[2:3]
     gains[1:2] = factors[3:4] + factors[4:5] + factors[5:6]
 
@@ -578,15 +581,16 @@
     )
     by_y = [packed[0]] + spread(lambda s: along_y(packed[s], s), FAR_FIRST)
     w0 = join((query_weight, key_weight, value_weight, outgate_weight))
-    by_z = [w0] + spread(lambda s: along_z(w0, s), NEAR_FIRST)
+    by_z = [w0] + spread(lambda s: along_z(w0, s), FAR_FIRST)
     send_from, take_with = route(routes, route_weights)
     down_y = stack_down(by_y)
-    down_z = [down_y] + spread(lambda s: along_z(down_y, s), NEAR_FIRST)
+    down_z = [down_y] + spread(lambda s: along_z(down_y, s), FAR_FIRST)
     held = fetch(memory, EARLY, HELD)
-    partner = [other_core(w) for w in by_z]
+    own_partner = other_core(w0)
+    partner = [own_partner] + spread(lambda s: other_core(by_z[s]), FAR_FIRST)
     own, *owed = project(by_y, by_z, partner)
     came = spread(lambda s: along_y(owed[s - 1], -s), FAR_FIRST)
-    down_partner = [other_core(d) for d in down_z[1:]]
+    down_partner = spread(lambda s: other_core(down_z[s]), FAR_FIRST)
     down_partner = [other_core(down_y)] + down_partner
     gated = read(own, came, gates, head_gain, early, held, memory)
     part, send, gains = down_project(gated, down_z, down_partner)

time: 117 us -> 115 us (0.983)
  starting transfers between devices: 49.4 us -> 44.5 us
  waiting for transfers between devices: 28.2 us -> 31.7 us
    ppermute x6, waiting for transfers between devices: 11.4 us -> 15.4 us  [along_y(): return lax.ppermute(a, 'ep', ep_moves(0, s, 0))]
    ppermute x6, starting transfers between devices: 16.6 us -> 12.9 us  [along_z(): return lax.ppermute(a, 'ep', ep_moves(s, 0, 0))]
    ppermute x8, waiting for transfers between devices: 1.41 us -> 0.02 us  [other_core(): return lax.ppermute(a, 'ep', ep_moves(0, 0, 1))]
    ppermute x6, starting transfers between devices: 13.7 us -> 12.3 us  [along_y(): return lax.ppermute(a, 'ep', ep_moves(0, s, 0))]
  transfers between devices with their start and end apart: 27 -> 27, of which waited for: 13 -> 12; matrix products, arithmetic and copies ran while one was open for 0% -> 0% of each run, Pallas kernels for 11% -> 11%
where the time goes in v3:
time: 115 us
  starting transfers between devices  44.5 us (39%)
  waiting for transfers between devices  31.7 us (28%)
  Pallas kernels  17.8 us (15%)
  blocking collectives  15.1 us (13%)
  local copies, waits for them, and re-layouts  5.89 us (5%)
    ppermute x6, waiting for transfers between devices, along_y(): return lax.ppermute(a, 'ep', ep_moves(0, s, 0))  15.4 us
    all_to_all x1, blocking collectives, layer(): lax.all_to_all(value.reshape(ep_count, 8, 1024), 'ep', 0, 0, tiled=True)  15.1 us
    ppermute x6, starting transfers between devices, along_z(): return lax.ppermute(a, 'ep', ep_moves(s, 0, 0))  12.9 us
    ppermute x6, starting transfers between devices, along_y(): return lax.ppermute(a, 'ep', ep_moves(0, s, 0))  12.3 us
    ppermute x6, starting transfers between devices, along_tp(): return lax.ppermute(a, 'tp', [(i, (i + s) % TP) for i in range(TP)])  10 us
    all_to_all x1, starting transfers between devices, layer(): lax.all_to_all(outgoing.reshape(ep_count, 8, 1024), 'ep', 0, 0, tiled=True)  7.17 us
    ppermute x6, waiting for transfers between devices, along_tp(): return lax.ppermute(a, 'tp', [(i, (i + s) % TP) for i in range(TP)])  6.55 us
    unnamed x18, local copies, waits for them, and re-layouts  5.89 us
  transfers between devices with their start and end apart: 27, of which 12 were waited for; matrix products, arithmetic and copies ran while one was open for 0% of the time, Pallas kernels for 11%

profile of v3, /device:TPU:0, one launch (start us, length us, event | category | flops | bytes accessed | tf_op | source)
XLA Modules:
  0.0 115.1 jit_solution(3349601760913847390)
XLA Ops:
  0.0 1.0 join.1.w0
  1.0 2.1 %collective-permute-start.3 = (bf16[64,2048]{1,0:T(8,128)(2,1)S(1)}, bf16[64,2048]{1,0:T(8,128)(2,1)S(1)}, u32[]{:S(2)}, u32[]{:S(2)}) collective-permute-start(bf16[64,2048]{1,0:T(8,128)(2,1)S(1)} %join.1.w0), channel_id=1, source_target_pairs={{0,32},{4,36},{8,40},{12,44},{16,48},{20,52},{24,56},{28,60},{32,6... | collective-permute-start | bytes 786440 | tf_op jit(solution)/shard_map/ppermute | solution.py:32
  3.1 3.6 %collective-permute-start.4 = (bf16[64,2048]{1,0:T(8,128)(2,1)S(1)}, bf16[64,2048]{1,0:T(8,128)(2,1)S(1)}, u32[]{:S(2)}, u32[]{:S(2)}) collective-permute-start(bf16[64,2048]{1,0:T(8,128)(2,1)S(1)} %join.1.w0), channel_id=1, source_target_pairs={{0,64},{4,68},{8,72},{12,76},{16,80},{20,84},{24,88},{28,92},{32,9... | collective-permute-start | bytes 786440 | tf_op jit(solution)/shard_map/ppermute | solution.py:32
  6.7 1.0 collective-permute-start.5
  7.7 2.7 %prepare.1 = (bf16[72,640]{1,0:T(8,128)(2,1)S(1)}, bf16[72,640]{1,0:T(8,128)(2,1)S(1)}, bf16[72,640]{1,0:T(8,128)(2,1)S(1)}, bf16[72,640]{1,0:T(8,128)(2,1)S(1)}...) custom-call(bf16[16,2048]{1,0:T(8,128)(2,1)} %x.1, f32[1,2048]{1,0:T(1,128)} %bitcast.21, ...), custom_call_target="tpu_custom_call" | custom-call | tf_op jit(solution)/shard_map/prepare/pallas_call | solution.py:156
  10.4 1.6 %collective-permute-start = (bf16[72,640]{1,0:T(8,128)(2,1)S(1)}, bf16[72,640]{1,0:T(8,128)(2,1)S(1)}, u32[]{:S(2)}, u32[]{:S(2)}) collective-permute-start(bf16[72,640]{1,0:T(8,128)(2,1)S(1)} %get-tuple-element.29), channel_id=1, source_target_pairs={{0,8},{4,12},{8,16},{12,20},{16,24},{20,28},{24,0},{28,4},{32,40},... | collective-permute-start | bytes 276488 | tf_op jit(solution)/shard_map/ppermute | solution.py:36
  12.1 0.5 collective-permute-start.7
  12.6 3.7 %collective-permute-done.n1.a1 = bf16[72,640]{1,0:T(8,128)(2,1)S(1)} collective-permute-done((bf16[72,640]{1,0:T(8,128)(2,1)S(1)}, bf16[72,640]{1,0:T(8,128)(2,1)S(1)}, u32[]{:S(2)}, u32[]{:S(2)}) %collective-permute-start) | collective-permute-done | bytes 92192 | tf_op jit(solution)/shard_map/ppermute | solution.py:36
  16.2 2.0 %collective-permute-start.1 = (bf16[72,640]{1,0:T(8,128)(2,1)S(1)}, bf16[72,640]{1,0:T(8,128)(2,1)S(1)}, u32[]{:S(2)}, u32[]{:S(2)}) collective-permute-start(bf16[72,640]{1,0:T(8,128)(2,1)S(1)} %get-tuple-element.30), channel_id=1, source_target_pairs={{0,16},{4,20},{8,24},{12,28},{16,0},{20,4},{24,8},{28,12},{32,48},... | collective-permute-start | bytes 276488 | tf_op jit(solution)/shard_map/ppermute | solution.py:36
  18.2 4.1 %collective-permute-done.1.n2.a2 = bf16[72,640]{1,0:T(8,128)(2,1)S(1)} collective-permute-done((bf16[72,640]{1,0:T(8,128)(2,1)S(1)}, bf16[72,640]{1,0:T(8,128)(2,1)S(1)}, u32[]{:S(2)}, u32[]{:S(2)}) %collective-permute-start.1) | collective-permute-done | bytes 92192 | tf_op jit(solution)/shard_map/ppermute | solution.py:36
  22.3 1.8 %collective-permute-start.2 = (bf16[72,640]{1,0:T(8,128)(2,1)S(1)}, bf16[72,640]{1,0:T(8,128)(2,1)S(1)}, u32[]{:S(2)}, u32[]{:S(2)}) collective-permute-start(bf16[72,640]{1,0:T(8,128)(2,1)S(1)} %get-tuple-element.31), channel_id=1, source_target_pairs={{0,24},{4,28},{8,0},{12,4},{16,8},{20,12},{24,16},{28,20},{32,56},... | collective-permute-start | bytes 276488 | tf_op jit(solution)/shard_map/ppermute | solution.py:36
  24.1 0.0 collective-permute-start.8
  24.1 0.0 collective-permute-done.5.w3
  24.1 0.5 collective-permute-start.9
  24.6 2.2 %collective-permute-done.2.n3.a3 = bf16[72,640]{1,0:T(8,128)(2,1)S(1)} collective-permute-done((bf16[72,640]{1,0:T(8,128)(2,1)S(1)}, bf16[72,640]{1,0:T(8,128)(2,1)S(1)}, u32[]{:S(2)}, u32[]{:S(2)}) %collective-permute-start.2) | collective-permute-done | bytes 92192 | tf_op jit(solution)/shard_map/ppermute | solution.py:36
  26.9 0.1 stack_down.1.d0
  26.9 1.1 collective-permute-start.13
  28.1 0.0 collective-permute-done.6.p0
  28.1 2.6 %collective-permute-start.14 = (bf16[264,512]{1,0:T(8,128)(2,1)S(1)}, bf16[264,512]{1,0:T(8,128)(2,1)S(1)}, u32[]{:S(2)}, u32[]{:S(2)}) collective-permute-start(bf16[264,512]{1,0:T(8,128)(2,1)S(1)} %stack_down.1.d0), channel_id=1, source_target_pairs={{0,64},{4,68},{8,72},{12,76},{16,80},{20,84},{24,88},{28,92},{32,9... | collective-permute-start | bytes 811016 | tf_op jit(solution)/shard_map/ppermute | solution.py:32
  30.7 2.5 %collective-permute-start.15 = (bf16[264,512]{1,0:T(8,128)(2,1)S(1)}, bf16[264,512]{1,0:T(8,128)(2,1)S(1)}, u32[]{:S(2)}, u32[]{:S(2)}) collective-permute-start(bf16[264,512]{1,0:T(8,128)(2,1)S(1)} %stack_down.1.d0), channel_id=1, source_target_pairs={{0,96},{4,100},{8,104},{12,108},{16,112},{20,116},{24,120},{28,124... | collective-permute-start | bytes 811016 | tf_op jit(solution)/shard_map/ppermute | solution.py:32
  33.2 0.0 collective-permute-done.8.p2
  33.2 0.0 collective-permute-done.9.p3
  33.2 0.5 project.1
  33.8 3.7 %collective-permute-start.10 = (bf16[16,3072]{1,0:T(8,128)(2,1)S(1)}, bf16[16,3072]{1,0:T(8,128)(2,1)S(1)}, u32[]{:S(2)}, u32[]{:S(2)}) collective-permute-start(bf16[16,3072]{1,0:T(8,128)(2,1)S(1)} %get-tuple-element.33), channel_id=1, source_target_pairs={{0,24},{4,28},{8,0},{12,4},{16,8},{20,12},{24,16},{28,20},{32,56},... | collective-permute-start | bytes 294920 | tf_op jit(solution)/shard_map/ppermute | solution.py:36
  37.4 0.0 collective-permute-start.16
  37.4 0.0 collective-permute-done.13.d1
  37.4 0.5 collective-permute-start.17
  37.9 3.8 %collective-permute-done.14.d2 = bf16[264,512]{1,0:T(8,128)(2,1)S(1)} collective-permute-done((bf16[264,512]{1,0:T(8,128)(2,1)S(1)}, bf16[264,512]{1,0:T(8,128)(2,1)S(1)}, u32[]{:S(2)}, u32[]{:S(2)}) %collective-permute-start.14) | collective-permute-done | bytes 270368 | tf_op jit(solution)/shard_map/ppermute | solution.py:32
  41.8 0.5 collective-permute-start.19
  42.3 2.3 %collective-permute-start.11 = (bf16[16,3072]{1,0:T(8,128)(2,1)S(1)}, bf16[16,3072]{1,0:T(8,128)(2,1)S(1)}, u32[]{:S(2)}, u32[]{:S(2)}) collective-permute-start(bf16[16,3072]{1,0:T(8,128)(2,1)S(1)} %get-tuple-element.34), channel_id=1, source_target_pairs={{0,16},{4,20},{8,24},{12,28},{16,0},{20,4},{24,8},{28,12},{32,48},... | collective-permute-start | bytes 294920 | tf_op jit(solution)/shard_map/ppermute | solution.py:36
  44.6 4.0 %collective-permute-done.11.r2 = bf16[16,3072]{1,0:T(8,128)(2,1)S(1)} collective-permute-done((bf16[16,3072]{1,0:T(8,128)(2,1)S(1)}, bf16[16,3072]{1,0:T(8,128)(2,1)S(1)}, u32[]{:S(2)}, u32[]{:S(2)}) %collective-permute-start.11) | collective-permute-done | bytes 98336 | tf_op jit(solution)/shard_map/ppermute | solution.py:36
  48.6 0.9 collective-permute-start.12
  49.5 3.5 %fetch_rows.1.held = f32[8,1,512,512]{3,2,1,0:T(8,128)S(1)} custom-call(f32[16,1,512,512]{3,2,1,0:T(8,128)} %memory.3), custom_call_target="tpu_custom_call" | custom-call | tf_op jit(solution)/shard_map/fetch_rows/pallas_call | solution.py:303
  53.0 1.5 %collective-permute-done.12.r3 = bf16[16,3072]{1,0:T(8,128)(2,1)S(1)} collective-permute-done((bf16[16,3072]{1,0:T(8,128)(2,1)S(1)}, bf16[16,3072]{1,0:T(8,128)(2,1)S(1)}, u32[]{:S(2)}, u32[]{:S(2)}) %collective-permute-start.12) | collective-permute-done | bytes 98336 | tf_op jit(solution)/shard_map/ppermute | solution.py:36
  54.5 2.2 %read.1.g = bf16[16,512]{1,0:T(8,128)(2,1)S(1)} custom-call(f32[16,2048]{1,0:T(8,128)S(1)} %get-tuple-element.32.own, bf16[16,3072]{1,0:T(8,128)(2,1)S(1)} %collective-permute-done.10.r1, bf16[16,3072]{1,0:T(8,128)(2,1)S(1)} %collective-permute-done.11.r2, bf16[16,3072]{1,0:T(8,128)(2,1)S(1)} %collective-permute-done.12.r3, ...), custom_call_target="tpu_custom_call" | custom-call | tf_op jit(solution)/shard_map/read/pallas_call | solution.py:362
  56.7 0.0 copy-start.5
  56.7 0.0 copy-start.6
  56.8 0.0 copy-start.4
  56.8 0.0 collective-permute-done.16.e0
  56.8 0.7 down_project.1
  57.5 1.6 %collective-permute-start.20 = (bf16[16,2048]{1,0:T(8,128)(2,1)S(1)}, bf16[16,2048]{1,0:T(8,128)(2,1)S(1)}, u32[]{:S(2)}, u32[]{:S(2)}) collective-permute-start(bf16[16,2048]{1,0:T(8,128)(2,1)S(1)} %get-tuple-element.39), channel_id=1, source_target_pairs={{0,1},{1,2},{2,3},{3,0},{4,5},{5,6},{6,7},{7,4},{8,9},{9,10},{10,1... | collective-permute-start | bytes 196616 | tf_op jit(solution)/shard_map/ppermute | solution.py:54
  59.1 2.7 %collective-permute-start.21 = (bf16[16,2048]{1,0:T(8,128)(2,1)S(1)}, bf16[16,2048]{1,0:T(8,128)(2,1)S(1)}, u32[]{:S(2)}, u32[]{:S(2)}) collective-permute-start(bf16[16,2048]{1,0:T(8,128)(2,1)S(1)} %get-tuple-element.39), channel_id=1, source_target_pairs={{0,2},{1,3},{2,0},{3,1},{4,6},{5,7},{6,4},{7,5},{8,10},{9,11},{10,... | collective-permute-start | bytes 196616 | tf_op jit(solution)/shard_map/ppermute | solution.py:54
  61.8 1.4 %collective-permute-start.22 = (bf16[16,2048]{1,0:T(8,128)(2,1)S(1)}, bf16[16,2048]{1,0:T(8,128)(2,1)S(1)}, u32[]{:S(2)}, u32[]{:S(2)}) collective-permute-start(bf16[16,2048]{1,0:T(8,128)(2,1)S(1)} %get-tuple-element.39), channel_id=1, source_target_pairs={{0,3},{1,0},{2,1},{3,2},{4,7},{5,4},{6,5},{7,6},{8,11},{9,8},{10,9... | collective-permute-start | bytes 196616 | tf_op jit(solution)/shard_map/ppermute | solution.py:54
  63.3 0.4 route.1
  63.7 1.2 %collective-permute-done.21.r2 = bf16[16,2048]{1,0:T(8,128)(2,1)S(1)} collective-permute-done((bf16[16,2048]{1,0:T(8,128)(2,1)S(1)}, bf16[16,2048]{1,0:T(8,128)(2,1)S(1)}, u32[]{:S(2)}, u32[]{:S(2)}) %collective-permute-start.21) | collective-permute-done | bytes 65568 | tf_op jit(solution)/shard_map/ppermute | solution.py:54
  64.9 1.2 %collective-permute-done.22.r3 = bf16[16,2048]{1,0:T(8,128)(2,1)S(1)} collective-permute-done((bf16[16,2048]{1,0:T(8,128)(2,1)S(1)}, bf16[16,2048]{1,0:T(8,128)(2,1)S(1)}, u32[]{:S(2)}, u32[]{:S(2)}) %collective-permute-start.22) | collective-permute-done | bytes 65568 | tf_op jit(solution)/shard_map/ppermute | solution.py:54
  66.1 1.3 %dispatch.1 = (bf16[16,2048]{1,0:T(8,128)(2,1)S(1)}, bf16[256,1024]{1,0:T(8,128)(2,1)}) custom-call(bf16[16,2048]{1,0:T(8,128)(2,1)S(1)} %copy-done.4, f32[16,2048]{1,0:T(8,128)S(1)} %get-tuple-element.38.part, bf16[16,2048]{1,0:T(8,128)(2,1)S(1)} %collective-permute-done.20.r1, bf16[16,2048]{1,0:T(8,128)(2,1)S(1)} %collective-permute-done.21.r2, ...), custom_call_target="tpu_custom_call" | custom-call | tf_op jit(solution)/shard_map/dispatch/pallas_call | solution.py:461
  67.4 7.2 %all-to-all-start = ((bf16[32,8,1024]{2,1,0:T(8,128)(2,1)}), bf16[32,8,1024]{2,1,0:T(8,128)(2,1)S(1)}, u32[]{:S(2)}, u32[]{:S(2)}) async-start(bf16[32,8,1024]{2,1,0:T(8,128)(2,1)} %bitcast.8), calls=%async_computation | async-start | bytes 1048576 | tf_op jit(solution)/shard_map/all_to_all | solution.py:600
  74.6 2.9 %fetch_experts.1 = (bf16[2048,512]{1,0:T(8,128)(2,1)S(1)}, bf16[2048,512]{1,0:T(8,128)(2,1)S(1)}, bf16[512,2048]{1,0:T(8,128)(2,1)S(1)}) custom-call(bf16[1,2048,512]{2,1,0:T(8,128)(2,1)} %g.1, bf16[1,2048,512]{2,1,0:T(8,128)(2,1)} %u.1, bf16[1,512,2048]{2,1,0:T(8,128)(2,1)} %d.1), custom_call_target="tpu_custom_call" | custom-call | tf_op jit(solution)/shard_map/fetch_experts/pallas_call | solution.py:437
  77.5 1.4 %copy-done = bf16[2048,512]{1,0:T(8,128)(2,1)} copy-done((bf16[2048,512]{1,0:T(8,128)(2,1)}, bf16[2048,512]{1,0:T(8,128)(2,1)S(1)}, u32[]{:S(2)}) %copy-start) | copy-done | bytes 2097176
  78.9 1.3 %copy-done.2 = bf16[512,2048]{1,0:T(8,128)(2,1)} copy-done((bf16[512,2048]{1,0:T(8,128)(2,1)}, bf16[512,2048]{1,0:T(8,128)(2,1)S(1)}, u32[]{:S(2)}) %copy-start.2) | copy-done | bytes 2097176
  80.2 5.8 %all-to-all-done = bf16[32,8,1024]{2,1,0:T(8,128)(2,1)S(1)} async-done(((bf16[32,8,1024]{2,1,0:T(8,128)(2,1)}), bf16[32,8,1024]{2,1,0:T(8,128)(2,1)S(1)}, u32[]{:S(2)}, u32[]{:S(2)}) %all-to-all-start) | async-done | bytes 524320 | tf_op jit(solution)/shard_map/all_to_all | solution.py:600
  86.0 1.6 %copy-done.1 = bf16[2048,512]{1,0:T(8,128)(2,1)S(1)} copy-done((bf16[2048,512]{1,0:T(8,128)(2,1)S(1)}, bf16[2048,512]{1,0:T(8,128)(2,1)}, u32[]{:S(2)}) %copy-start.1) | copy-done | bytes 2097176
  87.6 1.6 %copy-done.3 = bf16[512,2048]{1,0:T(8,128)(2,1)S(1)} copy-done((bf16[512,2048]{1,0:T(8,128)(2,1)S(1)}, bf16[512,2048]{1,0:T(8,128)(2,1)}, u32[]{:S(2)}) %copy-start.3) | copy-done | bytes 2097176
  89.2 1.5 %experts.1 = bf16[256,1024]{1,0:T(8,128)(2,1)S(1)} custom-call(bf16[256,1024]{1,0:T(8,128)(2,1)S(1)} %bitcast.13, bf16[2048,512]{1,0:T(8,128)(2,1)S(1)} %get-tuple-element.43.gate_w, bf16[2048,512]{1,0:T(8,128)(2,1)S(1)} %copy-done.1, bf16[512,2048]{1,0:T(8,128)(2,1)S(1)} %copy-done.3), custom_call_target="tpu_custom_call" | custom-call | tf_op jit(solution)/shard_map/experts/pallas_call | solution.py:502
  90.7 15.1 %all_to_all.10 = bf16[32,8,1024]{2,1,0:T(8,128)(2,1)S(1)} all-to-all(bf16[32,8,1024]{2,1,0:T(8,128)(2,1)S(1)} %bitcast.14), channel_id=1, replica_groups=mesh['ep'=32,'tp'=4] {'ep'}, dimensions={0} | all-to-all | bytes 1048576 | tf_op jit(solution)/shard_map/all_to_all | solution.py:604
  105.7 0.2 combine.1
  105.9 0.6 collective-permute-start.23
  106.6 3.5 %collective-permute-start.24 = (bf16[16,2048]{1,0:T(8,128)(2,1)S(1)}, bf16[16,2048]{1,0:T(8,128)(2,1)S(1)}, u32[]{:S(2)}, u32[]{:S(2)}) collective-permute-start(bf16[16,2048]{1,0:T(8,128)(2,1)S(1)} %get-tuple-element.47), channel_id=1, source_target_pairs={{0,2},{1,3},{2,0},{3,1},{4,6},{5,7},{6,4},{7,5},{8,10},{9,11},{10,... | collective-permute-start | bytes 196616 | tf_op jit(solution)/shard_map/ppermute | solution.py:54
  110.1 0.1 collective-permute-start.25
  110.2 1.3 %collective-permute-done.23.r1 = bf16[16,2048]{1,0:T(8,128)(2,1)S(1)} collective-permute-done((bf16[16,2048]{1,0:T(8,128)(2,1)S(1)}, bf16[16,2048]{1,0:T(8,128)(2,1)S(1)}, u32[]{:S(2)}, u32[]{:S(2)}) %collective-permute-start.23) | collective-permute-done | bytes 65568 | tf_op jit(solution)/shard_map/ppermute | solution.py:54
  111.5 2.1 %collective-permute-done.24.r2 = bf16[16,2048]{1,0:T(8,128)(2,1)S(1)} collective-permute-done((bf16[16,2048]{1,0:T(8,128)(2,1)S(1)}, bf16[16,2048]{1,0:T(8,128)(2,1)S(1)}, u32[]{:S(2)}, u32[]{:S(2)}) %collective-permute-start.24) | collective-permute-done | bytes 65568 | tf_op jit(solution)/shard_map/ppermute | solution.py:54
  113.6 0.8 collective-permute-done.25.r3
  114.4 0.7 finish.1
  (22 shorter events, 0.0 us)
Async XLA Ops:
  1.0 11.1 %collective-permute-start.3 = (bf16[64,2048]{1,0:T(8,128)(2,1)S(1)}, bf16[64,2048]{1,0:T(8,128)(2,1)S(1)}, u32[]{:S(2)}, u32[]{:S(2)}) collective-permute-start(bf16[64,2048]{1,0:T(8,128)(2,1)S(1)} %join.1.w0), channel_id=1, source_target_pairs={{0,32},{4,36},{8,40},{12,44},{16,48},{20,52},{24,56},{28,60},{32,6... | collective-permute-start | bytes 786440 | tf_op jit(solution)/shard_map/ppermute | solution.py:32
  3.1 21.0 %collective-permute-start.4 = (bf16[64,2048]{1,0:T(8,128)(2,1)S(1)}, bf16[64,2048]{1,0:T(8,128)(2,1)S(1)}, u32[]{:S(2)}, u32[]{:S(2)}) collective-permute-start(bf16[64,2048]{1,0:T(8,128)(2,1)S(1)} %join.1.w0), channel_id=1, source_target_pairs={{0,64},{4,68},{8,72},{12,76},{16,80},{20,84},{24,88},{28,92},{32,9... | collective-permute-start | bytes 786440 | tf_op jit(solution)/shard_map/ppermute | solution.py:32
  6.7 17.5 %collective-permute-start.5 = (bf16[64,2048]{1,0:T(8,128)(2,1)S(1)}, bf16[64,2048]{1,0:T(8,128)(2,1)S(1)}, u32[]{:S(2)}, u32[]{:S(2)}) collective-permute-start(bf16[64,2048]{1,0:T(8,128)(2,1)S(1)} %join.1.w0), channel_id=1, source_target_pairs={{0,96},{4,100},{8,104},{12,108},{16,112},{20,116},{24,120},{28,124... | collective-permute-start | bytes 786440 | tf_op jit(solution)/shard_map/ppermute | solution.py:32
  10.4 5.8 %collective-permute-start = (bf16[72,640]{1,0:T(8,128)(2,1)S(1)}, bf16[72,640]{1,0:T(8,128)(2,1)S(1)}, u32[]{:S(2)}, u32[]{:S(2)}) collective-permute-start(bf16[72,640]{1,0:T(8,128)(2,1)S(1)} %get-tuple-element.29), channel_id=1, source_target_pairs={{0,8},{4,12},{8,16},{12,20},{16,24},{20,28},{24,0},{28,4},{32,40},... | collective-permute-start | bytes 276488 | tf_op jit(solution)/shard_map/ppermute | solution.py:36
  12.1 16.0 %collective-permute-start.6 = (bf16[64,2048]{1,0:T(8,128)(2,1)S(1)}, bf16[64,2048]{1,0:T(8,128)(2,1)S(1)}, u32[]{:S(2)}, u32[]{:S(2)}) collective-permute-start(bf16[64,2048]{1,0:T(8,128)(2,1)S(1)} %join.1.w0), channel_id=1, source_target_pairs={{0,4},{4,0},{8,12},{12,8},{16,20},{20,16},{24,28},{28,24},{32,36},... | collective-permute-start | bytes 786440 | tf_op jit(solution)/shard_map/ppermute | solution.py:50
  12.1 18.6 %collective-permute-start.7 = (bf16[64,2048]{1,0:T(8,128)(2,1)S(1)}, bf16[64,2048]{1,0:T(8,128)(2,1)S(1)}, u32[]{:S(2)}, u32[]{:S(2)}) collective-permute-start(bf16[64,2048]{1,0:T(8,128)(2,1)S(1)} %collective-permute-done.3.w1), channel_id=1, source_target_pairs={{0,4},{4,0},{8,12},{12,8},{16,20},{20,16},{24,28},{28,24},{32,36},... | collective-permute-start | bytes 786440 | tf_op jit(solution)/shard_map/ppermute | solution.py:50
  16.2 6.1 %collective-permute-start.1 = (bf16[72,640]{1,0:T(8,128)(2,1)S(1)}, bf16[72,640]{1,0:T(8,128)(2,1)S(1)}, u32[]{:S(2)}, u32[]{:S(2)}) collective-permute-start(bf16[72,640]{1,0:T(8,128)(2,1)S(1)} %get-tuple-element.30), channel_id=1, source_target_pairs={{0,16},{4,20},{8,24},{12,28},{16,0},{20,4},{24,8},{28,12},{32,48},... | collective-permute-start | bytes 276488 | tf_op jit(solution)/shard_map/ppermute | solution.py:36
  22.3 4.6 %collective-permute-start.2 = (bf16[72,640]{1,0:T(8,128)(2,1)S(1)}, bf16[72,640]{1,0:T(8,128)(2,1)S(1)}, u32[]{:S(2)}, u32[]{:S(2)}) collective-permute-start(bf16[72,640]{1,0:T(8,128)(2,1)S(1)} %get-tuple-element.31), channel_id=1, source_target_pairs={{0,24},{4,28},{8,0},{12,4},{16,8},{20,12},{24,16},{28,20},{32,56},... | collective-permute-start | bytes 276488 | tf_op jit(solution)/shard_map/ppermute | solution.py:36
  24.1 9.1 %collective-permute-start.8 = (bf16[64,2048]{1,0:T(8,128)(2,1)S(1)}, bf16[64,2048]{1,0:T(8,128)(2,1)S(1)}, u32[]{:S(2)}, u32[]{:S(2)}) collective-permute-start(bf16[64,2048]{1,0:T(8,128)(2,1)S(1)} %collective-permute-done.4.w2), channel_id=1, source_target_pairs={{0,4},{4,0},{8,12},{12,8},{16,20},{20,16},{24,28},{28,24},{32,36},... | collective-permute-start | bytes 786440 | tf_op jit(solution)/shard_map/ppermute | solution.py:50
  24.1 9.1 %collective-permute-start.9 = (bf16[64,2048]{1,0:T(8,128)(2,1)S(1)}, bf16[64,2048]{1,0:T(8,128)(2,1)S(1)}, u32[]{:S(2)}, u32[]{:S(2)}) collective-permute-start(bf16[64,2048]{1,0:T(8,128)(2,1)S(1)} %collective-permute-done.5.w3), channel_id=1, source_target_pairs={{0,4},{4,0},{8,12},{12,8},{16,20},{20,16},{24,28},{28,24},{32,36},... | collective-permute-start | bytes 786440 | tf_op jit(solution)/shard_map/ppermute | solution.py:50
  26.9 10.5 %collective-permute-start.13 = (bf16[264,512]{1,0:T(8,128)(2,1)S(1)}, bf16[264,512]{1,0:T(8,128)(2,1)S(1)}, u32[]{:S(2)}, u32[]{:S(2)}) collective-permute-start(bf16[264,512]{1,0:T(8,128)(2,1)S(1)} %stack_down.1.d0), channel_id=1, source_target_pairs={{0,32},{4,36},{8,40},{12,44},{16,48},{20,52},{24,56},{28,60},{32,6... | collective-permute-start | bytes 811016 | tf_op jit(solution)/shard_map/ppermute | solution.py:32
  28.1 13.7 %collective-permute-start.14 = (bf16[264,512]{1,0:T(8,128)(2,1)S(1)}, bf16[264,512]{1,0:T(8,128)(2,1)S(1)}, u32[]{:S(2)}, u32[]{:S(2)}) collective-permute-start(bf16[264,512]{1,0:T(8,128)(2,1)S(1)} %stack_down.1.d0), channel_id=1, source_target_pairs={{0,64},{4,68},{8,72},{12,76},{16,80},{20,84},{24,88},{28,92},{32,9... | collective-permute-start | bytes 811016 | tf_op jit(solution)/shard_map/ppermute | solution.py:32
  30.7 11.1 %collective-permute-start.15 = (bf16[264,512]{1,0:T(8,128)(2,1)S(1)}, bf16[264,512]{1,0:T(8,128)(2,1)S(1)}, u32[]{:S(2)}, u32[]{:S(2)}) collective-permute-start(bf16[264,512]{1,0:T(8,128)(2,1)S(1)} %stack_down.1.d0), channel_id=1, source_target_pairs={{0,96},{4,100},{8,104},{12,108},{16,112},{20,116},{24,120},{28,124... | collective-permute-start | bytes 811016 | tf_op jit(solution)/shard_map/ppermute | solution.py:32
  33.8 8.6 %collective-permute-start.10 = (bf16[16,3072]{1,0:T(8,128)(2,1)S(1)}, bf16[16,3072]{1,0:T(8,128)(2,1)S(1)}, u32[]{:S(2)}, u32[]{:S(2)}) collective-permute-start(bf16[16,3072]{1,0:T(8,128)(2,1)S(1)} %get-tuple-element.33), channel_id=1, source_target_pairs={{0,24},{4,28},{8,0},{12,4},{16,8},{20,12},{24,16},{28,20},{32,56},... | collective-permute-start | bytes 294920 | tf_op jit(solution)/shard_map/ppermute | solution.py:36
  37.4 19.3 %collective-permute-start.16 = (bf16[264,512]{1,0:T(8,128)(2,1)S(1)}, bf16[264,512]{1,0:T(8,128)(2,1)S(1)}, u32[]{:S(2)}, u32[]{:S(2)}) collective-permute-start(bf16[264,512]{1,0:T(8,128)(2,1)S(1)} %stack_down.1.d0), channel_id=1, source_target_pairs={{0,4},{4,0},{8,12},{12,8},{16,20},{20,16},{24,28},{28,24},{32,36},... | collective-permute-start | bytes 811016 | tf_op jit(solution)/shard_map/ppermute | solution.py:50
  37.4 19.3 %collective-permute-start.17 = (bf16[264,512]{1,0:T(8,128)(2,1)S(1)}, bf16[264,512]{1,0:T(8,128)(2,1)S(1)}, u32[]{:S(2)}, u32[]{:S(2)}) collective-permute-start(bf16[264,512]{1,0:T(8,128)(2,1)S(1)} %collective-permute-done.13.d1), channel_id=1, source_target_pairs={{0,4},{4,0},{8,12},{12,8},{16,20},{20,16},{24,28},{28,24},{32,36},... | collective-permute-start | bytes 811016 | tf_op jit(solution)/shard_map/ppermute | solution.py:50
  41.8 15.0 %collective-permute-start.18 = (bf16[264,512]{1,0:T(8,128)(2,1)S(1)}, bf16[264,512]{1,0:T(8,128)(2,1)S(1)}, u32[]{:S(2)}, u32[]{:S(2)}) collective-permute-start(bf16[264,512]{1,0:T(8,128)(2,1)S(1)} %collective-permute-done.14.d2), channel_id=1, source_target_pairs={{0,4},{4,0},{8,12},{12,8},{16,20},{20,16},{24,28},{28,24},{32,36},... | collective-permute-start | bytes 811016 | tf_op jit(solution)/shard_map/ppermute | solution.py:50
  41.8 15.0 %collective-permute-start.19 = (bf16[264,512]{1,0:T(8,128)(2,1)S(1)}, bf16[264,512]{1,0:T(8,128)(2,1)S(1)}, u32[]{:S(2)}, u32[]{:S(2)}) collective-permute-start(bf16[264,512]{1,0:T(8,128)(2,1)S(1)} %collective-permute-done.15.d3), channel_id=1, source_target_pairs={{0,4},{4,0},{8,12},{12,8},{16,20},{20,16},{24,28},{28,24},{32,36},... | collective-permute-start | bytes 811016 | tf_op jit(solution)/shard_map/ppermute | solution.py:50
  42.3 6.3 %collective-permute-start.11 = (bf16[16,3072]{1,0:T(8,128)(2,1)S(1)}, bf16[16,3072]{1,0:T(8,128)(2,1)S(1)}, u32[]{:S(2)}, u32[]{:S(2)}) collective-permute-start(bf16[16,3072]{1,0:T(8,128)(2,1)S(1)} %get-tuple-element.34), channel_id=1, source_target_pairs={{0,16},{4,20},{8,24},{12,28},{16,0},{20,4},{24,8},{28,12},{32,48},... | collective-permute-start | bytes 294920 | tf_op jit(solution)/shard_map/ppermute | solution.py:36
  48.6 5.9 %copy-start.7 = (f32[512]{0:T(512)S(1)}, f32[512]{0:T(512)}, u32[]{:S(2)}) copy-start(f32[512]{0:T(512)} %param.30) | copy-start | bytes 6148
  48.6 5.9 %collective-permute-start.12 = (bf16[16,3072]{1,0:T(8,128)(2,1)S(1)}, bf16[16,3072]{1,0:T(8,128)(2,1)S(1)}, u32[]{:S(2)}, u32[]{:S(2)}) collective-permute-start(bf16[16,3072]{1,0:T(8,128)(2,1)S(1)} %get-tuple-element.35), channel_id=1, source_target_pairs={{0,8},{4,12},{8,16},{12,20},{16,24},{20,28},{24,0},{28,4},{32,40},... | collective-permute-start | bytes 294920 | tf_op jit(solution)/shard_map/ppermute | solution.py:36
  56.7 6.5 %copy-start.5 = (s32[512,4]{0,1:T(4,128)S(1)}, s32[512,4]{0,1:T(4,128)}, u32[]{:S(2)}) copy-start(s32[512,4]{0,1:T(4,128)} %param.34) | copy-start | bytes 24580
  56.7 6.5 %copy-start.6 = (f32[512,4]{0,1:T(4,128)S(1)}, f32[512,4]{0,1:T(4,128)}, u32[]{:S(2)}) copy-start(f32[512,4]{0,1:T(4,128)} %param.35) | copy-start | bytes 24580
  56.8 9.3 %copy-start.4 = (bf16[16,2048]{1,0:T(8,128)(2,1)S(1)}, bf16[16,2048]{1,0:T(8,128)(2,1)}, u32[]{:S(2)}) copy-start(bf16[16,2048]{1,0:T(8,128)(2,1)} %x.1) | copy-start | bytes 196612
  57.5 6.2 %collective-permute-start.20 = (bf16[16,2048]{1,0:T(8,128)(2,1)S(1)}, bf16[16,2048]{1,0:T(8,128)(2,1)S(1)}, u32[]{:S(2)}, u32[]{:S(2)}) collective-permute-start(bf16[16,2048]{1,0:T(8,128)(2,1)S(1)} %get-tuple-element.39), channel_id=1, source_target_pairs={{0,1},{1,2},{2,3},{3,0},{4,5},{5,6},{6,7},{7,4},{8,9},{9,10},{10,1... | collective-permute-start | bytes 196616 | tf_op jit(solution)/shard_map/ppermute | solution.py:54
  59.1 5.8 %collective-permute-start.21 = (bf16[16,2048]{1,0:T(8,128)(2,1)S(1)}, bf16[16,2048]{1,0:T(8,128)(2,1)S(1)}, u32[]{:S(2)}, u32[]{:S(2)}) collective-permute-start(bf16[16,2048]{1,0:T(8,128)(2,1)S(1)} %get-tuple-element.39), channel_id=1, source_target_pairs={{0,2},{1,3},{2,0},{3,1},{4,6},{5,7},{6,4},{7,5},{8,10},{9,11},{10,... | collective-permute-start | bytes 196616 | tf_op jit(solution)/shard_map/ppermute | solution.py:54
  61.8 4.3 %collective-permute-start.22 = (bf16[16,2048]{1,0:T(8,128)(2,1)S(1)}, bf16[16,2048]{1,0:T(8,128)(2,1)S(1)}, u32[]{:S(2)}, u32[]{:S(2)}) collective-permute-start(bf16[16,2048]{1,0:T(8,128)(2,1)S(1)} %get-tuple-element.39), channel_id=1, source_target_pairs={{0,3},{1,0},{2,1},{3,2},{4,7},{5,4},{6,5},{7,6},{8,11},{9,8},{10,9... | collective-permute-start | bytes 196616 | tf_op jit(solution)/shard_map/ppermute | solution.py:54
  67.4 18.6 %all-to-all-start = ((bf16[32,8,1024]{2,1,0:T(8,128)(2,1)}), bf16[32,8,1024]{2,1,0:T(8,128)(2,1)S(1)}, u32[]{:S(2)}, u32[]{:S(2)}) async-start(bf16[32,8,1024]{2,1,0:T(8,128)(2,1)} %bitcast.8), calls=%async_computation | async-start | bytes 1048576 | tf_op jit(solution)/shard_map/all_to_all | solution.py:600
  77.5 1.4 %copy-start = (bf16[2048,512]{1,0:T(8,128)(2,1)}, bf16[2048,512]{1,0:T(8,128)(2,1)S(1)}, u32[]{:S(2)}) copy-start(bf16[2048,512]{1,0:T(8,128)(2,1)S(1)} %get-tuple-element.44.up_w) | copy-start | bytes 6291460
  78.9 1.3 %copy-start.2 = (bf16[512,2048]{1,0:T(8,128)(2,1)}, bf16[512,2048]{1,0:T(8,128)(2,1)S(1)}, u32[]{:S(2)}) copy-start(bf16[512,2048]{1,0:T(8,128)(2,1)S(1)} %get-tuple-element.45.down_w) | copy-start | bytes 6291460
  86.0 1.6 %copy-start.1 = (bf16[2048,512]{1,0:T(8,128)(2,1)S(1)}, bf16[2048,512]{1,0:T(8,128)(2,1)}, u32[]{:S(2)}) copy-start(bf16[2048,512]{1,0:T(8,128)(2,1)} %copy-done) | copy-start | bytes 6291460
  87.6 1.6 %copy-start.3 = (bf16[512,2048]{1,0:T(8,128)(2,1)S(1)}, bf16[512,2048]{1,0:T(8,128)(2,1)}, u32[]{:S(2)}) copy-start(bf16[512,2048]{1,0:T(8,128)(2,1)} %copy-done.2) | copy-start | bytes 6291460
  89.2 25.2 %copy-start.8 = (f32[512]{0:T(512)S(1)}, f32[512]{0:T(512)}, u32[]{:S(2)}) copy-start(f32[512]{0:T(512)} %param.39) | copy-start | bytes 6148
  105.9 5.5 %collective-permute-start.23 = (bf16[16,2048]{1,0:T(8,128)(2,1)S(1)}, bf16[16,2048]{1,0:T(8,128)(2,1)S(1)}, u32[]{:S(2)}, u32[]{:S(2)}) collective-permute-start(bf16[16,2048]{1,0:T(8,128)(2,1)S(1)} %get-tuple-element.47), channel_id=1, source_target_pairs={{0,1},{1,2},{2,3},{3,0},{4,5},{5,6},{6,7},{7,4},{8,9},{9,10},{10,1... | collective-permute-start | bytes 196616 | tf_op jit(solution)/shard_map/ppermute | solution.py:54
  106.6 7.0 %collective-permute-start.24 = (bf16[16,2048]{1,0:T(8,128)(2,1)S(1)}, bf16[16,2048]{1,0:T(8,128)(2,1)S(1)}, u32[]{:S(2)}, u32[]{:S(2)}) collective-permute-start(bf16[16,2048]{1,0:T(8,128)(2,1)S(1)} %get-tuple-element.47), channel_id=1, source_target_pairs={{0,2},{1,3},{2,0},{3,1},{4,6},{5,7},{6,4},{7,5},{8,10},{9,11},{10,... | collective-permute-start | bytes 196616 | tf_op jit(solution)/shard_map/ppermute | solution.py:54
  110.1 4.3 %collective-permute-start.25 = (bf16[16,2048]{1,0:T(8,128)(2,1)S(1)}, bf16[16,2048]{1,0:T(8,128)(2,1)S(1)}, u32[]{:S(2)}, u32[]{:S(2)}) collective-permute-start(bf16[16,2048]{1,0:T(8,128)(2,1)S(1)} %get-tuple-element.47), channel_id=1, source_target_pairs={{0,3},{1,0},{2,1},{3,2},{4,7},{5,4},{6,5},{7,6},{8,11},{9,8},{10,9... | collective-permute-start | bytes 196616 | tf_op jit(solution)/shard_map/ppermute | solution.py:54
